TPU v7x, 256 devices: a 4x2x16 block of a 4x16x16 slice. The times are simulated.
256 devices in a mesh: grp: 2 (over y), sp: 16 (over z), fs: 4 (over x), tp: 2 (over core).
Axes of the slice: x: 4, y: 2, z: 16, core: 2. Of those that a mesh axis runs over, the one named last changes fastest.
The devices are a block of a 4x16x16 slice.
Arguments:
- tokens: bfloat16 [8, 8192, 2048], P(('grp', 'fs'), ('sp', 'tp')), parts along dimension 0, may hold values from -6 to 6
- norm_gain: float32 [2048], replicated, may hold values from 0.1 to 1.9
- w_bgate: bfloat16 [2048, 2048], P(('sp', 'fs'), 'tp'), may hold values from -0.125 to 0.125
- w_cgate: bfloat16 [2048, 2048], P(('sp', 'fs'), 'tp'), may hold values from -0.125 to 0.125
- w_conv_in: bfloat16 [2048, 2048], P(('sp', 'fs'), 'tp'), may hold values from -0.125 to 0.125
- conv_taps: bfloat16 [3, 2048], P(None, 'tp'), may hold values from -3.5 to 3.5
- w_query: bfloat16 [2048, 2048], P(('sp', 'fs'), 'tp'), may hold values from -0.13258252 to 0.13258252
- w_key: bfloat16 [2048, 256], P(('sp', 'fs'), 'tp'), may hold values from -4.02167 to 4.02167
- w_value: bfloat16 [2048, 256], P(('sp', 'fs'), 'tp'), may hold values from -0.125 to 0.125
- sink_logits: float32 [32], P('tp'), may hold values from 1 to 6
- conv_out_weight: bfloat16 [2048, 2048], P('tp', ('sp', 'fs')), may hold values from -0.125 to 0.125
- attn_out_weight: bfloat16 [2048, 2048], P('tp', ('sp', 'fs')), may hold values from -0.75 to 0.75
Outputs:
- mixed: bfloat16 [8, 8192, 2048], P(('grp', 'fs'), ('sp', 'tp')), parts along dimension 0
There are 2 independent parts, one for each index of `grp`. A program takes and returns all parts, laid end to end along the dimension named above; an argument that names none is the same for every part. Nothing has to cross between parts.
All inputs are finite; a program needn't handle non-finite values.
Results may differ from a plain program's by a relative error of at most 0.014.
The roundings to bfloat16 on the way count: a program that leaves them out, or rounds other values in their place, can miss the bound.
Values may be sent and summed in bfloat16 or wider, within the bound.
No kernel may reach another device: no remote copies, remote signals or barrier semaphores. Data moves between devices by JAX's collectives and lax.ppermute only.
A program may use at most 128 MiB of HBM per device.

v0:
```python
import functools

import jax
import jax.numpy as jnp
from jax import lax
from jax.experimental import pallas as pl
from jax.experimental.pallas import tpu as pltpu
from jax.sharding import PartitionSpec as P


HEAD = 64
WINDOW = 128
TAPS = 3
EPSILON = 1e-06


ANY = pl.BlockSpec(memory_space=pl.ANY)
SMEM = pl.BlockSpec(memory_space=pltpu.SMEM)
VMEM = pl.BlockSpec(memory_space=pltpu.VMEM)


def ring(array, axis, by):
    size = lax.axis_size(axis)
    return lax.ppermute(array, axis, [(i, (i + by) % size) for i in range(size)])


def pack_kernel(wq, wk, wv, conv_t, attn_t, wb, wc, wi, out):
    fs = out.shape[0]
    chans = wq.shape[1] // fs
    for f in range(fs):
        cut = slice(f * chans, (f + 1) * chans)
        head = (f * wk.shape[1]) // (fs * HEAD) * HEAD
        kv = jnp.concatenate([wk[:, head : head + HEAD], wv[:, head : head + HEAD]], axis=1)
        at = 0
        for part in (wb[:, cut], wc[:, cut], wi[:, cut], wq[:, cut], kv, conv_t[:, cut], attn_t[:, cut]):
            out[f, :, at : at + part.shape[1]] = part
            at += part.shape[1]


def turn_kernel(in_cols, mine, out):
    block, width = out.shape
    out[:, :in_cols] = mine[:, :in_cols]
    for at in range(in_cols, width, block):
        out[:, at : at + block] = mine[:, at : at + block].T


def finish_kernel(low, high, up_a, down_a, up_b, down_b, out):
    half = up_a.shape[0]
    for at, own, up, down in ((0, low, up_a, down_a), (half, high, up_b, down_b)):
        total = own[...].astype(jnp.float32) + up[...].astype(jnp.float32)
        total = total + down[...].astype(jnp.float32)
        out[at : at + half, :] = total.astype(jnp.bfloat16)


def project_kernel(wide, weights, *refs):
    opp_a, opp_b, succ, prev, own, out, edge, wout, xs, ws, sems = refs
    step = pl.program_id(0)
    half = opp_a.shape[0]
    block = weights.shape[2]
    blocks = weights.shape[0]
    in_cols = ws.shape[3]
    parts = (weights.shape[3] - in_cols) // block
    bf16, f32 = jnp.bfloat16, jnp.float32
    x_copies = [
        pltpu.make_async_copy(ref, xs.at[s, pl.ds(at, ref.shape[0]), :], sems.at[i])
        for i, (ref, s, at) in enumerate(
            ((succ, 0, 0), (prev, 1, 0), (opp_a, 2, 0), (opp_b, 2, half), (own, 3, 0))
        )
    ]
    w_copies = [
        pltpu.make_async_copy(weights.at[:, t, :, pl.ds(0, in_cols)], ws.at[t], sems.at[5 + t])
        for t in range(2)
    ]

    def out_copies(t):
        return [
            pltpu.make_async_copy(
                weights.at[j, t, :, pl.ds(in_cols + b * block, block)],
                wout.at[pl.ds((t * parts + b) * block, block), pl.ds(j * block, block)],
                sems.at[7 + (t * parts + b) * blocks + j],
            )
            for b in range(parts)
            for j in range(blocks)
        ]

    @pl.when(step == 0)
    def _():
        for c in x_copies + w_copies:
            c.start()
        for c in out_copies(0):
            c.start()
        for c in x_copies:
            c.wait()
        w_copies[0].wait()

    @pl.when(step == 1)
    def _():
        for c in out_copies(1):
            c.start()
        w_copies[1].wait()

    seqs, length, feats = xs.shape
    x = xs[...].reshape(seqs * length, feats)
    w = ws[step].reshape(feats, in_cols)
    rounded = jnp.dot(x, w, preferred_element_type=f32).astype(bf16).reshape(seqs, length, in_cols)
    out[0] = rounded
    chans = wide // 3
    for s in range(seqs):
        edge[0, s, 0:WINDOW, :] = rounded[s, length - WINDOW :, wide + chans :]
        last = rounded[s, length - 16 :, chans:wide].astype(f32)
        gated = (last[:, :chans] * last[:, chans:]).astype(bf16)
        edge[0, s, WINDOW : WINDOW + 16, :] = gated[:, : 2 * HEAD]
        edge[0, s, WINDOW + 16 : WINDOW + 32, :] = gated[:, 2 * HEAD :]

    @pl.when(step == 1)
    def _():
        for t in range(2):
            for c in out_copies(t):
                c.wait()


def mix_kernel(tasks, wide, idx, sinks, proj, edge, taps, wout, low, high, acts):
    place = idx[0]
    chans = wide // 3
    heads = chans // HEAD
    f32, bf16 = jnp.float32, jnp.bfloat16
    q_at, kv_at = wide, wide + chans
    pair = 2 * HEAD

    def iota(shape, dim):
        return lax.broadcasted_iota(jnp.int32, shape, dim)

    pick_kt = (iota((chans, pair), 1) == jnp.bitwise_and(iota((chans, pair), 0), HEAD - 1)).astype(bf16)
    pick_v = (iota((pair, pair), 0) == jnp.bitwise_and(iota((pair, pair), 1), HEAD - 1) + HEAD).astype(bf16)
    row = iota((WINDOW, chans), 0)
    lane = iota((WINDOW, chans), 1)
    left = iota((WINDOW, pair), 1) < HEAD
    qi, ki = iota((WINDOW, 2 * WINDOW), 0), iota((WINDOW, 2 * WINDOW), 1)
    band = (ki > qi) & (ki <= qi + WINDOW)
    first = band & ((ki >= WINDOW) | (place > 0))
    ones = jnp.ones((2 * WINDOW, pair), bf16)
    transposed = (((1,), (1,)), ((), ()))
    for slot, (s, n) in enumerate(tasks):
        at, to = n * WINDOW, slot * WINDOW
        for side in range(2):

            def gated_rows(start, rows):
                c = proj[side, s, start : start + rows, chans : 2 * chans].astype(f32)
                i = proj[side, s, start : start + rows, 2 * chans : 3 * chans].astype(f32)
                return (c * i).astype(bf16).astype(f32)

            t = taps[side]
            base = side * 2 * chans
            if n == 0:
                tail = jnp.concatenate(
                    [edge[side, s, WINDOW : WINDOW + 16, :], edge[side, s, WINDOW + 16 : WINDOW + 32, :]],
                    axis=1,
                ).astype(f32)
            else:
                tail = gated_rows(at - 16, 16)
            before2, before1 = tail[14:15, :], tail[15:16, :]
            g = gated_rows(at, WINDOW)
            one = jnp.where(row == 0, before1, pltpu.roll(g, 1, 0))
            two = jnp.where(row == 0, before2, jnp.where(row == 1, before1, pltpu.roll(g, 2, 0)))
            convolved = two * t[0:1] + one * t[1:2] + g * t[2:3]
            out_gate = proj[side, s, at : at + WINDOW, 0:chans].astype(f32)
            acts[to : to + WINDOW, base : base + chans] = (out_gate * convolved).astype(bf16)

            kv_here = proj[side, s, at : at + WINDOW, kv_at : kv_at + pair]
            if n == 0:
                kv_before = edge[side, s, 0:WINDOW, :]
            else:
                kv_before = proj[side, s, at - WINDOW : at, kv_at : kv_at + pair]
            kv = jnp.concatenate([kv_before, kv_here], axis=0)
            keys = lax.dot_general(pick_kt, kv, transposed, preferred_element_type=f32).astype(bf16)
            values = jnp.dot(kv, pick_v, preferred_element_type=f32).astype(bf16)
            values = jnp.concatenate([values, ones], axis=1)
            q = proj[side, s, at : at + WINDOW, q_at : q_at + chans]
            allowed = first if n == 0 else band
            outs = []
            for h in range(heads):
                qh = jnp.where((lane >= h * HEAD) & (lane < (h + 1) * HEAD), q, jnp.zeros_like(q))
                sc = jnp.dot(qh, keys, preferred_element_type=f32)
                sc = jnp.where(allowed, sc * (1.0 / 8.0), -jnp.inf)
                sink = sinks[side, h]
                m = jnp.maximum(jnp.max(sc, axis=1, keepdims=True), sink)
                e = jnp.exp(sc - m).astype(bf16)
                o = jnp.dot(e, values, preferred_element_type=f32)
                outs.append(o[:, :pair] / (o[:, pair:] + jnp.exp(sink - m)))
            for j in range(heads // 2):
                col = base + chans + j * pair
                acts[to : to + WINDOW, col : col + pair] = jnp.where(
                    left, outs[2 * j], outs[2 * j + 1]
                ).astype(bf16)

    product = jnp.dot(acts[...], wout[...], preferred_element_type=f32).astype(bf16)
    low[...] = product[:WINDOW]
    high[...] = product[WINDOW:]


def added(*parts):
    total = parts[0].astype(jnp.float32)
    for p in parts[1:]:
        total = total + p.astype(jnp.float32)
    return total.astype(jnp.bfloat16)


def layer(
    tokens,
    norm_gain,
    w_bgate,
    w_cgate,
    w_conv_in,
    conv_taps,
    w_query,
    w_key,
    w_value,
    sink_logits,
    conv_out_weight,
    attn_out_weight,
):
    fs = lax.axis_size("fs")
    sp = lax.axis_size("sp")
    tp = lax.axis_size("tp")
    bf16, f32 = jnp.bfloat16, jnp.float32
    rows_in = w_bgate.shape[0]
    chans = w_bgate.shape[1] // fs
    block = rows_in * fs
    b_width, out_cols = 3 * chans, 2 * chans
    in_cols = b_width + chans + 2 * HEAD
    width = in_cols + out_cols
    packed = pl.pallas_call(
        pack_kernel,
        out_shape=jax.ShapeDtypeStruct((fs, rows_in, width), bf16),
        in_specs=[VMEM] * 8,
        out_specs=VMEM,
        name="pack_weights",
    )(w_query, w_key, w_value, conv_out_weight.T, attn_out_weight.T, w_bgate, w_cgate, w_conv_in)
    mine = lax.all_to_all(packed, "fs", split_axis=0, concat_axis=0, tiled=True)
    mine = pl.pallas_call(
        functools.partial(turn_kernel, in_cols),
        out_shape=jax.ShapeDtypeStruct((block, width), bf16),
        in_specs=[VMEM],
        out_specs=VMEM,
        name="turn_weights",
    )(mine.reshape(block, width))
    weights = lax.all_gather(mine, ("sp", "tp"), axis=0, tiled=True)
    weights = weights.reshape(sp, tp, block, width)

    core, place, group = lax.axis_index("tp"), lax.axis_index("sp"), lax.axis_index("fs")
    heads = chans // HEAD
    idx = jnp.stack([place * tp + core, place]).astype(jnp.int32)
    taps = lax.dynamic_slice_in_dim(conv_taps, group * chans, chans, 1).astype(f32)
    sinks = lax.dynamic_slice_in_dim(sink_logits, group * heads, heads, 0)
    small = jnp.concatenate([taps, jnp.pad(sinks[None], ((0, 0), (0, chans - heads)))], axis=0)

    widened = tokens[0].astype(f32)
    normed = (
        widened
        * lax.rsqrt(jnp.mean(widened * widened, axis=-1, keepdims=True) + EPSILON)
        * norm_gain
    ).astype(bf16)
    here, feats = normed.shape
    half = here // 2
    prev = ring(normed, "fs", 1)
    succ = ring(normed, "fs", -1)
    opp_a = ring(prev[:half], "fs", 1)
    opp_b = ring(succ[half:], "fs", -1)
    theirs = lax.ppermute(small, "tp", [(0, 1), (1, 0)])
    both = jnp.where(core == 0, jnp.stack([small, theirs]), jnp.stack([theirs, small]))
    taps, sinks = both[:, :TAPS], both[:, TAPS, :heads]

    squares = out_cols // block
    proj, edge, wout = pl.pallas_call(
        functools.partial(project_kernel, b_width),
        out_shape=(
            jax.ShapeDtypeStruct((tp, fs, here, in_cols), bf16),
            jax.ShapeDtypeStruct((tp, fs, WINDOW + 32, 2 * HEAD), bf16),
            jax.ShapeDtypeStruct((tp * out_cols, feats), bf16),
        ),
        grid=(tp,),
        in_specs=[ANY] * 6,
        out_specs=(
            pl.BlockSpec((1, fs, here, in_cols), lambda t: (t, 0, 0, 0)),
            pl.BlockSpec((1, fs, WINDOW + 32, 2 * HEAD), lambda t: (t, 0, 0, 0)),
            pl.BlockSpec((tp * out_cols, feats), lambda t: (0, 0)),
        ),
        scratch_shapes=[
            pltpu.VMEM((fs, here, feats), bf16),
            pltpu.VMEM((tp, sp, block, in_cols), bf16),
            pltpu.SemaphoreType.DMA((7 + tp * squares * sp,)),
        ],
        cost_estimate=pl.CostEstimate(
            flops=2 * tp * fs * here * feats * in_cols, bytes_accessed=25_000_000, transcendentals=0
        ),
        compiler_params=pltpu.CompilerParams(dimension_semantics=("arbitrary",)),
        name="project_rows",
    )(weights, opp_a, opp_b, succ, prev, normed)
    edge = lax.ppermute(edge, ("sp", "tp"), [(i, i + 1) for i in range(sp * tp - 1)])

    def mix(first, size, tasks):
        return pl.pallas_call(
            functools.partial(mix_kernel, tasks, b_width),
            out_shape=(jax.ShapeDtypeStruct((half, feats), bf16),) * 2,
            grid=(1,),
            in_specs=[
                SMEM,
                SMEM,
                pl.BlockSpec((tp, size, here, in_cols), lambda i: (0, first, 0, 0)),
                pl.BlockSpec((tp, size, WINDOW + 32, 2 * HEAD), lambda i: (0, first, 0, 0)),
                pl.BlockSpec((tp, TAPS, chans), lambda i: (0, 0, 0)),
                pl.BlockSpec((tp * out_cols, feats), lambda i: (0, 0)),
            ],
            out_specs=(pl.BlockSpec((half, feats), lambda i: (0, 0)),) * 2,
            scratch_shapes=[pltpu.VMEM((here, tp * out_cols), bf16)],
            cost_estimate=pl.CostEstimate(
                flops=2 * here * feats * tp * out_cols + 600_000_000,
                bytes_accessed=8_000_000,
                transcendentals=600_000,
            ),
        )(idx, sinks, proj, edge, taps, wout)

    def sent(array, by):
        return ring(array, "fs", by)

    low, high = mix(2, 1, ((0, 0), (0, 1)))
    up, down = sent(low, 1), sent(high, -1)
    low, high = mix(0, 2, ((0, 1), (1, 0)))
    up_b, down_a = sent(low, 1), sent(high, -1)
    low, high = mix(0, 2, ((0, 0), (1, 1)))
    up_a, down_b = sent(added(low, up), 1), sent(added(high, down), -1)
    low, high = mix(3, 1, ((0, 0), (0, 1)))
    out = pl.pallas_call(
        finish_kernel,
        out_shape=jax.ShapeDtypeStruct((here, feats), bf16),
        in_specs=[VMEM] * 6,
        out_specs=VMEM,
        name="finish_rows",
    )(low, high, up_a, down_a, up_b, down_b)
    return out[None]


def solution(mesh):
    placed = (
        P(("grp", "fs"), ("sp", "tp"), None),
        P(),
        P(("sp", "fs"), "tp"),
        P(("sp", "fs"), "tp"),
        P(("sp", "fs"), "tp"),
        P(None, "tp"),
        P(("sp", "fs"), "tp"),
        P(("sp", "fs"), "tp"),
        P(("sp", "fs"), "tp"),
        P("tp"),
        P("tp", ("sp", "fs")),
        P("tp", ("sp", "fs")),
    )
    return jax.shard_map(
        layer,
        mesh=mesh,
        in_specs=placed,
        out_specs=P(("grp", "fs"), ("sp", "tp"), None),
        check_vma=False,
    )
```

profile of v0, /device:TPU:33, one launch (start us, length us, event | category | flops | bytes accessed | tf_op | source)
XLA Modules:
  0.0 219.9 jit_solution(13831958036724597275)
XLA Ops:
  6.5 0.0 copy-start
  6.6 0.0 all-gather.2.cloned.1.call-start
  6.6 2.0 pack_weights.1
  8.5 11.6 %all_to_all.5 = bf16[4,32,1664]{2,1,0:T(8,128)(2,1)} all-to-all(bf16[4,32,1664]{2,1,0:T(8,128)(2,1)} %pack_weights.1), channel_id=1, replica_groups=mesh['grp'=2,'sp'=16,'fs'=4,'tp'=2] {'fs'}, dimensions={0} | all-to-all | bytes 851968 | tf_op jit(solution)/shard_map/all_to_all | solution.py:239
  20.1 1.9 turn_weights.1
  22.0 0.1 all-gather.2.cloned.1.call-update
  22.1 0.3 fusion
  22.4 0.3 fusion.2.refs_4_
  22.7 1.0 collective-permute-start.3
  23.7 0.6 collective-permute-start.1
  24.3 12.9 %collective-permute-done.3.refs_2_ = bf16[256,2048]{1,0:T(8,128)(2,1)S(1)} collective-permute-done((bf16[256,2048]{1,0:T(8,128)(2,1)S(1)}, bf16[256,2048]{1,0:T(8,128)(2,1)S(1)}, u32[]{:S(2)}, u32[]{:S(2)}) %collective-permute-start.3) | collective-permute-done | bytes 1048608 | tf_op jit(solution)/shard_map/ppermute | solution.py:24
  37.3 3.6 %collective-permute-start.4 = (bf16[128,2048]{1,0:T(8,128)(2,1)S(1)}, bf16[128,2048]{1,0:T(8,128)(2,1)}, u32[]{:S(2)}, u32[]{:S(2)}) collective-permute-start(bf16[128,2048]{1,0:T(8,128)(2,1)S(1)} %slice.18), channel_id=1, source_target_pairs={{0,6},{2,0},{4,2},{6,4},{1,7},{3,1},{5,3},{7,5},{8,14},{10,8},{12,... | collective-permute-start | bytes 1572872 | tf_op jit(solution)/shard_map/ppermute | solution.py:24
  40.8 0.3 collective-permute-done.1.refs_3_
  41.2 0.1 collective-permute-start.2
  41.4 0.8 copy-done.9
  42.2 0.1 dynamic-slice_bitcast_fusion
  42.2 0.7 dynamic-slice_convert_fusion
  42.9 21.4 %collective-permute-start = (f32[4,256]{1,0:T(4,128)S(1)}, f32[4,256]{1,0:T(4,128)S(1)}, u32[]{:S(2)}, u32[]{:S(2)}) collective-permute-start(f32[4,256]{1,0:T(4,128)S(1)} %select_maximum_fusion), channel_id=1, source_target_pairs={{0,1},{1,0},{2,3},{3,2},{4,5},{5,4},{6,7},{7,6},{8,9},{9,8},{10,11... | collective-permute-start | bytes 12296 | tf_op jit(solution)/shard_map/ppermute | solution.py:269
  64.4 0.0 collective-permute-done.4.refs_1_
  64.4 0.0 collective-permute-done.2.refs_0_
  64.4 61.3 %all-gather.2.cloned.1.call-done = bf16[4096,1664]{1,0:T(8,128)(2,1)} async-done(((bf16[128,1664]{1,0:T(8,128)(2,1)}), bf16[4096,1664]{1,0:T(8,128)(2,1)}) %all-gather.2.cloned.1.call-update) | async-done | bytes 13631504 | tf_op jit(solution)/shard_map/all_gather | solution.py:247
  125.7 19.1 %project_rows.1 = (bf16[2,4,256,1152]{3,2,1,0:T(8,128)(2,1)}, bf16[2,4,160,128]{3,2,1,0:T(8,128)(2,1)}, bf16[1024,2048]{1,0:T(8,128)(2,1)}) custom-call(bf16[16,2,128,1664]{3,2,1,0:T(8,128)(2,1)} %bitcast.30, bf16[128,2048]{1,0:T(8,128)(2,1)} %collective-permute-done.2.refs_0_, bf16[128,2048]{1,0:T(8,128)(2,1)} %collective-permute-done.4.refs_1_, ...), custom_call_target="tpu_custom_call" | custom-call | flops 9663676416 | bytes 25000000 | tf_op jit(solution)/shard_map/project_rows/pallas_call | solution.py:274
  144.8 2.6 %collective-permute-start.5 = (bf16[2,4,160,128]{3,2,1,0:T(8,128)(2,1)}, bf16[2,4,160,128]{3,2,1,0:T(8,128)(2,1)S(1)}, u32[]{:S(2)}, u32[]{:S(2)}) collective-permute-start(bf16[2,4,160,128]{3,2,1,0:T(8,128)(2,1)} %get-tuple-element.17), channel_id=1, source_target_pairs={{0,1},{1,8},{8,9},{9,16},{16,17},{17,24},{24,25},{25,32},{32,33},{... | collective-permute-start | bytes 983048 | tf_op jit(solution)/shard_map/ppermute | solution.py:299
  147.4 0.6 pad_add_fusion.idx
  148.1 0.0 collective-permute-done
  148.1 0.6 slice.16
  148.6 2.9 %collective-permute-done.5.edge = bf16[2,4,160,128]{3,2,1,0:T(8,128)(2,1)S(1)} collective-permute-done((bf16[2,4,160,128]{3,2,1,0:T(8,128)(2,1)}, bf16[2,4,160,128]{3,2,1,0:T(8,128)(2,1)S(1)}, u32[]{:S(2)}, u32[]{:S(2)}) %collective-permute-start.5) | collective-permute-done | bytes 327712 | tf_op jit(solution)/shard_map/ppermute | solution.py:299
  151.6 0.7 copy-done.1
  152.3 6.7 %shard_map.120 = (bf16[128,2048]{1,0:T(8,128)(2,1)}, bf16[128,2048]{1,0:T(8,128)(2,1)}) custom-call(s32[2]{0:T(128)} %pad_add_fusion.idx, f32[2,4]{1,0:T(2,128)} %bitcast.25, bf16[2,4,256,1152]{3,2,1,0:T(8,128)(2,1)} %get-tuple-element.16.proj, bf16[2,4,160,128]{3,2,1,0:T(8,128)(2,1)} %copy-done.1, f32[2,3,256]{2,1,0:T(4,128)} %bitcast.19, ...), custom_call_target="tpu_custom_call" | custom-call | flops 1673741824 | bytes 8000000 | tf_op jit(solution)/shard_map/pallas_call | solution.py:302
  159.0 2.4 %collective-permute-start.10 = (bf16[128,2048]{1,0:T(8,128)(2,1)}, bf16[128,2048]{1,0:T(8,128)(2,1)S(1)}, u32[]{:S(2)}, u32[]{:S(2)}) collective-permute-start(bf16[128,2048]{1,0:T(8,128)(2,1)} %get-tuple-element.26), channel_id=1, source_target_pairs={{0,6},{2,0},{4,2},{6,4},{1,7},{3,1},{5,3},{7,5},{8,14},{10,8},{12,... | collective-permute-start | bytes 1572872 | tf_op jit(solution)/shard_map/ppermute | solution.py:24
  161.4 7.1 %shard_map.121 = (bf16[128,2048]{1,0:T(8,128)(2,1)}, bf16[128,2048]{1,0:T(8,128)(2,1)}) custom-call(s32[2]{0:T(128)} %pad_add_fusion.idx, f32[2,4]{1,0:T(2,128)} %bitcast.26, bf16[2,4,256,1152]{3,2,1,0:T(8,128)(2,1)} %get-tuple-element.16.proj, bf16[2,4,160,128]{3,2,1,0:T(8,128)(2,1)} %copy-done.1, f32[2,3,256]{2,1,0:T(4,128)} %bitcast.20, ...), custom_call_target="tpu_custom_call" | custom-call | flops 1673741824 | bytes 8000000 | tf_op jit(solution)/shard_map/pallas_call | solution.py:302
  168.6 0.6 collective-permute-start.8
  169.1 0.9 collective-permute-start.9
  170.0 0.0 collective-permute-start.6
  170.0 7.1 %shard_map.119 = (bf16[128,2048]{1,0:T(8,128)(2,1)}, bf16[128,2048]{1,0:T(8,128)(2,1)}) custom-call(s32[2]{0:T(128)} %pad_add_fusion.idx, f32[2,4]{1,0:T(2,128)} %bitcast.27, bf16[2,4,256,1152]{3,2,1,0:T(8,128)(2,1)} %get-tuple-element.16.proj, bf16[2,4,160,128]{3,2,1,0:T(8,128)(2,1)} %copy-done.1, f32[2,3,256]{2,1,0:T(4,128)} %bitcast.21, ...), custom_call_target="tpu_custom_call" | custom-call | flops 1673741824 | bytes 8000000 | tf_op jit(solution)/shard_map/pallas_call | solution.py:302
  177.2 0.0 collective-permute-done.10
  177.2 1.2 add_convert_fusion
  178.4 2.8 %collective-permute-start.11 = (bf16[128,2048]{1,0:T(8,128)(2,1)S(1)}, bf16[128,2048]{1,0:T(8,128)(2,1)S(1)}, u32[]{:S(2)}, u32[]{:S(2)}) collective-permute-start(bf16[128,2048]{1,0:T(8,128)(2,1)S(1)} %add_convert_fusion), channel_id=1, source_target_pairs={{0,6},{2,0},{4,2},{6,4},{1,7},{3,1},{5,3},{7,5},{8,14},{10,8},{12,... | collective-permute-start | bytes 1572872 | tf_op jit(solution)/shard_map/ppermute | solution.py:24
  181.2 12.4 %collective-permute-done.6 = bf16[128,2048]{1,0:T(8,128)(2,1)S(1)} collective-permute-done((bf16[128,2048]{1,0:T(8,128)(2,1)}, bf16[128,2048]{1,0:T(8,128)(2,1)S(1)}, u32[]{:S(2)}, u32[]{:S(2)}) %collective-permute-start.6) | collective-permute-done | bytes 524320 | tf_op jit(solution)/shard_map/ppermute | solution.py:24
  193.6 1.2 add_convert_fusion.1
  194.8 0.1 collective-permute-start.7
  195.0 6.7 %shard_map.118 = (bf16[128,2048]{1,0:T(8,128)(2,1)}, bf16[128,2048]{1,0:T(8,128)(2,1)}) custom-call(s32[2]{0:T(128)} %pad_add_fusion.idx, f32[2,4]{1,0:T(2,128)} %bitcast.28, bf16[2,4,256,1152]{3,2,1,0:T(8,128)(2,1)} %get-tuple-element.16.proj, bf16[2,4,160,128]{3,2,1,0:T(8,128)(2,1)} %copy-done.1, f32[2,3,256]{2,1,0:T(4,128)} %bitcast.22, ...), custom_call_target="tpu_custom_call" | custom-call | flops 1673741824 | bytes 8000000 | tf_op jit(solution)/shard_map/pallas_call | solution.py:302
  201.7 0.0 collective-permute-done.8.down_a
  201.7 0.0 collective-permute-done.9.up_b
  201.7 0.0 collective-permute-done.11.down_b
  201.7 7.4 %collective-permute-done.7.up_a = bf16[128,2048]{1,0:T(8,128)(2,1)S(1)} collective-permute-done((bf16[128,2048]{1,0:T(8,128)(2,1)S(1)}, bf16[128,2048]{1,0:T(8,128)(2,1)S(1)}, u32[]{:S(2)}, u32[]{:S(2)}) %collective-permute-start.7) | collective-permute-done | bytes 524320 | tf_op jit(solution)/shard_map/ppermute | solution.py:24
  209.1 0.8 copy-done.7
  209.9 3.2 %finish_rows.1 = bf16[256,2048]{1,0:T(8,128)(2,1)} custom-call(bf16[128,2048]{1,0:T(8,128)(2,1)} %get-tuple-element.19.low, bf16[128,2048]{1,0:T(8,128)(2,1)} %get-tuple-element.20.high, bf16[128,2048]{1,0:T(8,128)(2,1)} %copy-done.7, bf16[128,2048]{1,0:T(8,128)(2,1)} %copy-done.4, bf16[128,2048]{1,0:T(8,128)(2,1)} %copy-done.5, bf16[128,2048]{1,0:T(8,128)(2,1)} %copy-done.6), custom_call_target="tpu_custom_call" | custom-call | tf_op jit(solution)/shard_map/finish_rows/pallas_call | solution.py:333
  (26 shorter events, 0.2 us)
Async XLA Ops:
  6.5 35.6 %copy-start = (f32[16]{0:T(128)S(1)}, f32[16]{0:T(128)}, u32[]{:S(2)}) copy-start(f32[16]{0:T(128)} %param.21) | copy-start | bytes 196
  6.6 15.5 %copy-start.2 = (bf16[1,256,2048]{2,1,0:T(8,128)(2,1)S(1)}, bf16[1,256,2048]{2,1,0:T(8,128)(2,1)}, u32[]{:S(2)}) copy-start(bf16[1,256,2048]{2,1,0:T(8,128)(2,1)} %param.12) | copy-start | bytes 3145732
  6.6 15.8 %copy-start.11 = (f32[2048]{0:T(1024)S(1)}, f32[2048]{0:T(1024)}, u32[]{:S(2)}) copy-start(f32[2048]{0:T(1024)} %param.13) | copy-start | bytes 24580
  6.6 119.1 %all-gather.2.cloned.1.call-start = ((), (), s32[]{:S(2)}) async-start(), calls=%async_computation.1 | async-start | bytes 14057472 | tf_op jit(solution)/shard_map/all_gather | solution.py:247
  22.7 103.0 %copy-start.3 = (bf16[256,2048]{1,0:T(8,128)(2,1)}, bf16[256,2048]{1,0:T(8,128)(2,1)S(1)}, u32[]{:S(2)}) copy-start(bf16[256,2048]{1,0:T(8,128)(2,1)S(1)} %fusion.2.refs_4_) | copy-start | bytes 3145732
  22.7 14.5 %collective-permute-start.3 = (bf16[256,2048]{1,0:T(8,128)(2,1)S(1)}, bf16[256,2048]{1,0:T(8,128)(2,1)S(1)}, u32[]{:S(2)}, u32[]{:S(2)}) collective-permute-start(bf16[256,2048]{1,0:T(8,128)(2,1)S(1)} %fusion.2.refs_4_), channel_id=1, source_target_pairs={{0,6},{2,0},{4,2},{6,4},{1,7},{3,1},{5,3},{7,5},{8,14},{10,8},{12,... | collective-permute-start | bytes 3145736 | tf_op jit(solution)/shard_map/ppermute | solution.py:24
  23.7 17.5 %collective-permute-start.1 = (bf16[256,2048]{1,0:T(8,128)(2,1)S(1)}, bf16[256,2048]{1,0:T(8,128)(2,1)S(1)}, u32[]{:S(2)}, u32[]{:S(2)}) collective-permute-start(bf16[256,2048]{1,0:T(8,128)(2,1)S(1)} %fusion.2.refs_4_), channel_id=1, source_target_pairs={{0,2},{2,4},{4,6},{6,0},{1,3},{3,5},{5,7},{7,1},{8,10},{10,12},{12... | collective-permute-start | bytes 3145736 | tf_op jit(solution)/shard_map/ppermute | solution.py:24
  37.2 88.5 %copy-start.8 = (bf16[256,2048]{1,0:T(8,128)(2,1)}, bf16[256,2048]{1,0:T(8,128)(2,1)S(1)}, u32[]{:S(2)}) copy-start(bf16[256,2048]{1,0:T(8,128)(2,1)S(1)} %collective-permute-done.3.refs_2_) | copy-start | bytes 3145732
  37.3 27.1 %collective-permute-start.4 = (bf16[128,2048]{1,0:T(8,128)(2,1)S(1)}, bf16[128,2048]{1,0:T(8,128)(2,1)}, u32[]{:S(2)}, u32[]{:S(2)}) collective-permute-start(bf16[128,2048]{1,0:T(8,128)(2,1)S(1)} %slice.18), channel_id=1, source_target_pairs={{0,6},{2,0},{4,2},{6,4},{1,7},{3,1},{5,3},{7,5},{8,14},{10,8},{12,... | collective-permute-start | bytes 1572872 | tf_op jit(solution)/shard_map/ppermute | solution.py:24
  41.2 1.0 copy-start.9
  41.2 23.2 %collective-permute-start.2 = (bf16[128,2048]{1,0:T(8,128)(2,1)S(1)}, bf16[128,2048]{1,0:T(8,128)(2,1)}, u32[]{:S(2)}, u32[]{:S(2)}) collective-permute-start(bf16[128,2048]{1,0:T(8,128)(2,1)S(1)} %slice.17), channel_id=1, source_target_pairs={{0,2},{2,4},{4,6},{6,0},{1,3},{3,5},{5,7},{7,1},{8,10},{10,12},{12... | collective-permute-start | bytes 1572872 | tf_op jit(solution)/shard_map/ppermute | solution.py:24
  42.9 105.1 %collective-permute-start = (f32[4,256]{1,0:T(4,128)S(1)}, f32[4,256]{1,0:T(4,128)S(1)}, u32[]{:S(2)}, u32[]{:S(2)}) collective-permute-start(f32[4,256]{1,0:T(4,128)S(1)} %select_maximum_fusion), channel_id=1, source_target_pairs={{0,1},{1,0},{2,3},{3,2},{4,5},{5,4},{6,7},{7,6},{8,9},{9,8},{10,11... | collective-permute-start | bytes 12296 | tf_op jit(solution)/shard_map/ppermute | solution.py:269
  144.8 6.8 %collective-permute-start.5 = (bf16[2,4,160,128]{3,2,1,0:T(8,128)(2,1)}, bf16[2,4,160,128]{3,2,1,0:T(8,128)(2,1)S(1)}, u32[]{:S(2)}, u32[]{:S(2)}) collective-permute-start(bf16[2,4,160,128]{3,2,1,0:T(8,128)(2,1)} %get-tuple-element.17), channel_id=1, source_target_pairs={{0,1},{1,8},{8,9},{9,16},{16,17},{17,24},{24,25},{25,32},{32,33},{... | collective-permute-start | bytes 983048 | tf_op jit(solution)/shard_map/ppermute | solution.py:299
  148.1 3.5 %copy-start.10 = (f32[2,4,256]{2,1,0:T(4,128)}, f32[2,4,256]{2,1,0:T(4,128)S(1)}, u32[]{:S(2)}) copy-start(f32[2,4,256]{2,1,0:T(4,128)S(1)} %maximum_select_fusion) | copy-start | bytes 24580
  151.6 0.7 copy-start.1
  159.0 18.2 %collective-permute-start.10 = (bf16[128,2048]{1,0:T(8,128)(2,1)}, bf16[128,2048]{1,0:T(8,128)(2,1)S(1)}, u32[]{:S(2)}, u32[]{:S(2)}) collective-permute-start(bf16[128,2048]{1,0:T(8,128)(2,1)} %get-tuple-element.26), channel_id=1, source_target_pairs={{0,6},{2,0},{4,2},{6,4},{1,7},{3,1},{5,3},{7,5},{8,14},{10,8},{12,... | collective-permute-start | bytes 1572872 | tf_op jit(solution)/shard_map/ppermute | solution.py:24
  168.6 33.1 %collective-permute-start.8 = (bf16[128,2048]{1,0:T(8,128)(2,1)}, bf16[128,2048]{1,0:T(8,128)(2,1)S(1)}, u32[]{:S(2)}, u32[]{:S(2)}) collective-permute-start(bf16[128,2048]{1,0:T(8,128)(2,1)} %get-tuple-element.23), channel_id=1, source_target_pairs={{0,6},{2,0},{4,2},{6,4},{1,7},{3,1},{5,3},{7,5},{8,14},{10,8},{12,... | collective-permute-start | bytes 1572872 | tf_op jit(solution)/shard_map/ppermute | solution.py:24
  169.1 32.6 %collective-permute-start.9 = (bf16[128,2048]{1,0:T(8,128)(2,1)}, bf16[128,2048]{1,0:T(8,128)(2,1)S(1)}, u32[]{:S(2)}, u32[]{:S(2)}) collective-permute-start(bf16[128,2048]{1,0:T(8,128)(2,1)} %get-tuple-element.24), channel_id=1, source_target_pairs={{0,2},{2,4},{4,6},{6,0},{1,3},{3,5},{5,7},{7,1},{8,10},{10,12},{12... | collective-permute-start | bytes 1572872 | tf_op jit(solution)/shard_map/ppermute | solution.py:24
  170.0 23.6 %collective-permute-start.6 = (bf16[128,2048]{1,0:T(8,128)(2,1)}, bf16[128,2048]{1,0:T(8,128)(2,1)S(1)}, u32[]{:S(2)}, u32[]{:S(2)}) collective-permute-start(bf16[128,2048]{1,0:T(8,128)(2,1)} %get-tuple-element.22), channel_id=1, source_target_pairs={{0,2},{2,4},{4,6},{6,0},{1,3},{3,5},{5,7},{7,1},{8,10},{10,12},{12... | collective-permute-start | bytes 1572872 | tf_op jit(solution)/shard_map/ppermute | solution.py:24
  178.4 23.3 %collective-permute-start.11 = (bf16[128,2048]{1,0:T(8,128)(2,1)S(1)}, bf16[128,2048]{1,0:T(8,128)(2,1)S(1)}, u32[]{:S(2)}, u32[]{:S(2)}) collective-permute-start(bf16[128,2048]{1,0:T(8,128)(2,1)S(1)} %add_convert_fusion), channel_id=1, source_target_pairs={{0,6},{2,0},{4,2},{6,4},{1,7},{3,1},{5,3},{7,5},{8,14},{10,8},{12,... | collective-permute-start | bytes 1572872 | tf_op jit(solution)/shard_map/ppermute | solution.py:24
  194.8 14.3 %collective-permute-start.7 = (bf16[128,2048]{1,0:T(8,128)(2,1)S(1)}, bf16[128,2048]{1,0:T(8,128)(2,1)S(1)}, u32[]{:S(2)}, u32[]{:S(2)}) collective-permute-start(bf16[128,2048]{1,0:T(8,128)(2,1)S(1)} %add_convert_fusion.1), channel_id=1, source_target_pairs={{0,2},{2,4},{4,6},{6,0},{1,3},{3,5},{5,7},{7,1},{8,10},{10,12},{12... | collective-permute-start | bytes 1572872 | tf_op jit(solution)/shard_map/ppermute | solution.py:24
  201.7 7.4 %copy-start.4 = (bf16[128,2048]{1,0:T(8,128)(2,1)}, bf16[128,2048]{1,0:T(8,128)(2,1)S(1)}, u32[]{:S(2)}) copy-start(bf16[128,2048]{1,0:T(8,128)(2,1)S(1)} %collective-permute-done.8.down_a) | copy-start | bytes 1572868
  201.7 7.4 %copy-start.5 = (bf16[128,2048]{1,0:T(8,128)(2,1)}, bf16[128,2048]{1,0:T(8,128)(2,1)S(1)}, u32[]{:S(2)}) copy-start(bf16[128,2048]{1,0:T(8,128)(2,1)S(1)} %collective-permute-done.9.up_b) | copy-start | bytes 1572868
  201.7 7.4 %copy-start.6 = (bf16[128,2048]{1,0:T(8,128)(2,1)}, bf16[128,2048]{1,0:T(8,128)(2,1)S(1)}, u32[]{:S(2)}) copy-start(bf16[128,2048]{1,0:T(8,128)(2,1)S(1)} %collective-permute-done.11.down_b) | copy-start | bytes 1572868
  209.1 0.8 copy-start.7
Sparse Core Ops, SparseCore 0:
  22.2 103.4 all-gather.1
where the time goes:
time: 220 us
  waiting for transfers between devices  97.3 us (44%)
  Pallas kernels  53.8 us (24%)
  starting transfers between devices  36.2 us (16%)
  between operations  13.6 us (6%)
  blocking collectives  11.6 us (5%)
  other arithmetic  4.37 us (2%)
  local copies, waits for them, and re-layouts  3.1 us (1%)
    all_gather x1, waiting for transfers between devices, layer(): weights = lax.all_gather(mine, ('sp', 'tp'), axis=0, tiled=True)  61.3 us
    ppermute x10, waiting for transfers between devices, ring(): lax.ppermute(array, axis, [(i, (i + by) % size) for i in range(size)])  33.1 us
    pallas_call x4, Pallas kernels, mix(): pl.pallas_call(functools.partial(mix_kernel, tasks, b_width), out_shape=(...  27.7 us
    ppermute x1, starting transfers between devices, layer(): theirs = lax.ppermute(small, 'tp', [(0, 1), (1, 0)])  21.4 us
    pallas_call x1, Pallas kernels, layer(): pl.pallas_call(functools.partial(project_kernel, b_width), out_shape=(jax...  19.1 us
    ppermute x10, starting transfers between devices, ring(): lax.ppermute(array, axis, [(i, (i + by) % size) for i in range(size)])  12.1 us
    all_to_all x1, blocking collectives, layer(): mine = lax.all_to_all(packed, 'fs', split_axis=0, concat_axis=0, tiled=True)  11.6 us
  transfers between devices with their start and end apart: 13, of which 6 were waited for; matrix products, arithmetic and copies ran while one was open for 2% of the time, Pallas kernels for 18%

commit v1 on v0

--- a/solution.py
+++ b/solution.py
@@ -53,7 +53,7 @@
 
 
 def project_kernel(wide, weights, *refs):
-    opp_a, opp_b, succ, prev, own, out, edge, wout, xs, ws, sems = refs
+    opp_a, opp_b, succ, prev, own, out, edge, wout, xs, ws, wo, sems = refs
     step = pl.program_id(0)
     half = opp_a.shape[0]
     block = weights.shape[2]
@@ -76,28 +76,33 @@
         return [
             pltpu.make_async_copy(
                 weights.at[j, t, :, pl.ds(in_cols + b * block, block)],
-                wout.at[pl.ds((t * parts + b) * block, block), pl.ds(j * block, block)],
+                wo.at[pl.ds((t * parts + b) * block, block), pl.ds(j * block, block)],
                 sems.at[7 + (t * parts + b) * blocks + j],
             )
             for b in range(parts)
             for j in range(blocks)
         ]
 
+    laid_out = pltpu.make_async_copy(wo, wout, sems.at[7 + 2 * parts * blocks])
+
     @pl.when(step == 0)
     def _():
-        for c in x_copies + w_copies:
+        for c in x_copies + w_copies[:1]:
             c.start()
-        for c in out_copies(0):
-            c.start()
-        for c in x_copies:
+        for c in x_copies + w_copies[:1]:
             c.wait()
-        w_copies[0].wait()
+        w_copies[1].start()
+        for t in range(2):
+            for c in out_copies(t):
+                c.start()
 
     @pl.when(step == 1)
     def _():
-        for c in out_copies(1):
-            c.start()
         w_copies[1].wait()
+        for t in range(2):
+            for c in out_copies(t):
+                c.wait()
+        laid_out.start()
 
     seqs, length, feats = xs.shape
     x = xs[...].reshape(seqs * length, feats)
@@ -114,12 +119,12 @@
 
     @pl.when(step == 1)
     def _():
-        for t in range(2):
-            for c in out_copies(t):
-                c.wait()
-
-
-def mix_kernel(tasks, wide, idx, sinks, proj, edge, taps, wout, low, high, acts):
+        laid_out.wait()
+
+
+def mix_kernel(blocks, wide, idx, sinks, taps, wout, *refs):
+    projs, edges = refs[:2], refs[2:-3]
+    low, high, acts = refs[-3:]
     place = idx[0]
     chans = wide // 3
     heads = chans // HEAD
@@ -140,20 +145,21 @@
     first = band & ((ki >= WINDOW) | (place > 0))
     ones = jnp.ones((2 * WINDOW, pair), bf16)
     transposed = (((1,), (1,)), ((), ()))
-    for slot, (s, n) in enumerate(tasks):
+    for slot, n in enumerate(blocks):
         at, to = n * WINDOW, slot * WINDOW
+        proj, edge = projs[slot], edges[slot] if n == 0 else None
         for side in range(2):
 
             def gated_rows(start, rows):
-                c = proj[side, s, start : start + rows, chans : 2 * chans].astype(f32)
-                i = proj[side, s, start : start + rows, 2 * chans : 3 * chans].astype(f32)
+                c = proj[side, 0, start : start + rows, chans : 2 * chans].astype(f32)
+                i = proj[side, 0, start : start + rows, 2 * chans : 3 * chans].astype(f32)
                 return (c * i).astype(bf16).astype(f32)
 
             t = taps[side]
             base = side * 2 * chans
             if n == 0:
                 tail = jnp.concatenate(
-                    [edge[side, s, WINDOW : WINDOW + 16, :], edge[side, s, WINDOW + 16 : WINDOW + 32, :]],
+                    [edge[side, 0, WINDOW : WINDOW + 16, :], edge[side, 0, WINDOW + 16 : WINDOW + 32, :]],
                     axis=1,
                 ).astype(f32)
             else:
@@ -163,19 +169,19 @@
             one = jnp.where(row == 0, before1, pltpu.roll(g, 1, 0))
             two = jnp.where(row == 0, before2, jnp.where(row == 1, before1, pltpu.roll(g, 2, 0)))
             convolved = two * t[0:1] + one * t[1:2] + g * t[2:3]
-            out_gate = proj[side, s, at : at + WINDOW, 0:chans].astype(f32)
+            out_gate = proj[side, 0, at : at + WINDOW, 0:chans].astype(f32)
             acts[to : to + WINDOW, base : base + chans] = (out_gate * convolved).astype(bf16)
 
-            kv_here = proj[side, s, at : at + WINDOW, kv_at : kv_at + pair]
+            kv_here = proj[side, 0, at : at + WINDOW, kv_at : kv_at + pair]
             if n == 0:
-                kv_before = edge[side, s, 0:WINDOW, :]
+                kv_before = edge[side, 0, 0:WINDOW, :]
             else:
-                kv_before = proj[side, s, at - WINDOW : at, kv_at : kv_at + pair]
+                kv_before = proj[side, 0, at - WINDOW : at, kv_at : kv_at + pair]
             kv = jnp.concatenate([kv_before, kv_here], axis=0)
             keys = lax.dot_general(pick_kt, kv, transposed, preferred_element_type=f32).astype(bf16)
             values = jnp.dot(kv, pick_v, preferred_element_type=f32).astype(bf16)
             values = jnp.concatenate([values, ones], axis=1)
-            q = proj[side, s, at : at + WINDOW, q_at : q_at + chans]
+            q = proj[side, 0, at : at + WINDOW, q_at : q_at + chans]
             allowed = first if n == 0 else band
             outs = []
             for h in range(heads):
@@ -269,6 +275,7 @@
     theirs = lax.ppermute(small, "tp", [(0, 1), (1, 0)])
     both = jnp.where(core == 0, jnp.stack([small, theirs]), jnp.stack([theirs, small]))
     taps, sinks = both[:, :TAPS], both[:, TAPS, :heads]
+    weights, idx, taps, sinks = lax.optimization_barrier((weights, idx, taps, sinks))
 
     squares = out_cols // block
     proj, edge, wout = pl.pallas_call(
@@ -283,12 +290,13 @@
         out_specs=(
             pl.BlockSpec((1, fs, here, in_cols), lambda t: (t, 0, 0, 0)),
             pl.BlockSpec((1, fs, WINDOW + 32, 2 * HEAD), lambda t: (t, 0, 0, 0)),
-            pl.BlockSpec((tp * out_cols, feats), lambda t: (0, 0)),
+            ANY,
         ),
         scratch_shapes=[
             pltpu.VMEM((fs, here, feats), bf16),
             pltpu.VMEM((tp, sp, block, in_cols), bf16),
-            pltpu.SemaphoreType.DMA((7 + tp * squares * sp,)),
+            pltpu.VMEM((tp * out_cols, feats), bf16),
+            pltpu.SemaphoreType.DMA((8 + tp * squares * sp,)),
         ],
         cost_estimate=pl.CostEstimate(
             flops=2 * tp * fs * here * feats * in_cols, bytes_accessed=25_000_000, transcendentals=0
@@ -298,19 +306,25 @@
     )(weights, opp_a, opp_b, succ, prev, normed)
     edge = lax.ppermute(edge, ("sp", "tp"), [(i, i + 1) for i in range(sp * tp - 1)])
 
-    def mix(first, size, tasks):
+    def mix(tasks):
+        seqs, blocks = zip(*tasks)
+        edged = [q for q, n in tasks if n == 0]
+
+        def part(shape, q):
+            return pl.BlockSpec((tp, 1) + shape, lambda i, q=q: (0, q, 0, 0))
+
         return pl.pallas_call(
-            functools.partial(mix_kernel, tasks, b_width),
+            functools.partial(mix_kernel, blocks, b_width),
             out_shape=(jax.ShapeDtypeStruct((half, feats), bf16),) * 2,
             grid=(1,),
             in_specs=[
                 SMEM,
                 SMEM,
-                pl.BlockSpec((tp, size, here, in_cols), lambda i: (0, first, 0, 0)),
-                pl.BlockSpec((tp, size, WINDOW + 32, 2 * HEAD), lambda i: (0, first, 0, 0)),
                 pl.BlockSpec((tp, TAPS, chans), lambda i: (0, 0, 0)),
                 pl.BlockSpec((tp * out_cols, feats), lambda i: (0, 0)),
-            ],
+            ]
+            + [part((here, in_cols), q) for q in seqs]
+            + [part((WINDOW + 32, 2 * HEAD), q) for q in (seqs if edged else ())],
             out_specs=(pl.BlockSpec((half, feats), lambda i: (0, 0)),) * 2,
             scratch_shapes=[pltpu.VMEM((here, tp * out_cols), bf16)],
             cost_estimate=pl.CostEstimate(
@@ -318,18 +332,19 @@
                 bytes_accessed=8_000_000,
                 transcendentals=600_000,
             ),
-        )(idx, sinks, proj, edge, taps, wout)
+        )(idx, sinks, taps, wout, proj, proj, *((edge, edge) if edged else ()))
 
     def sent(array, by):
         return ring(array, "fs", by)
 
-    low, high = mix(2, 1, ((0, 0), (0, 1)))
-    up, down = sent(low, 1), sent(high, -1)
-    low, high = mix(0, 2, ((0, 1), (1, 0)))
-    up_b, down_a = sent(low, 1), sent(high, -1)
-    low, high = mix(0, 2, ((0, 0), (1, 1)))
-    up_a, down_b = sent(added(low, up), 1), sent(added(high, down), -1)
-    low, high = mix(3, 1, ((0, 0), (0, 1)))
+    succ_q, prev_q, opp_q, own_q = range(4)
+    low, high = mix(((succ_q, 1), (opp_q, 1)))
+    down, up_b = sent(high, -1), sent(low, 1)
+    low, high = mix(((opp_q, 0), (prev_q, 0)))
+    up, down_a = sent(low, 1), sent(high, -1)
+    low, high = mix(((succ_q, 0), (prev_q, 1)))
+    down_b, up_a = sent(added(high, down), -1), sent(added(low, up), 1)
+    low, high = mix(((own_q, 0), (own_q, 1)))
     out = pl.pallas_call(
         finish_kernel,
         out_shape=jax.ShapeDtypeStruct((here, feats), bf16),

time: 220 us -> 208 us (0.945)
  waiting for transfers between devices: 97.3 us -> 84.4 us
    ppermute x10, waiting for transfers between devices: 33.1 us -> 24.9 us  [ring(): lax.ppermute(array, axis, [(i, (i + by) % size) for i in range(size)])]
    ppermute x1, waiting for transfers between devices: 2.91 us -> 0.01 us  [layer(): lax.ppermute(edge, ('sp', 'tp'), [(i, i + 1) for i in range(sp * tp - 1)])]
  transfers between devices with their start and end apart: 13 -> 13, of which waited for: 6 -> 6; matrix products, arithmetic and copies ran while one was open for 2% -> 3% of each run, Pallas kernels for 18% -> 14%
where the time goes in v1:
time: 208 us
  waiting for transfers between devices  84.4 us (41%)
  Pallas kernels  53.1 us (26%)
  starting transfers between devices  37.5 us (18%)
  between operations  13.6 us (7%)
  blocking collectives  11.6 us (6%)
  other arithmetic  4.31 us (2%)
  local copies, waits for them, and re-layouts  3.33 us (2%)
    all_gather x1, waiting for transfers between devices, layer(): weights = lax.all_gather(mine, ('sp', 'tp'), axis=0, tiled=True)  59.2 us
    pallas_call x4, Pallas kernels, mix(): pl.pallas_call(functools.partial(mix_kernel, blocks, b_width), out_shape=...  28.2 us
    ppermute x10, waiting for transfers between devices, ring(): lax.ppermute(array, axis, [(i, (i + by) % size) for i in range(size)])  24.9 us
    ppermute x1, starting transfers between devices, layer(): theirs = lax.ppermute(small, 'tp', [(0, 1), (1, 0)])  22.6 us
    pallas_call x1, Pallas kernels, layer(): pl.pallas_call(functools.partial(project_kernel, b_width), out_shape=(jax...  17.9 us
    ppermute x10, starting transfers between devices, ring(): lax.ppermute(array, axis, [(i, (i + by) % size) for i in range(size)])  12.5 us
    all_to_all x1, blocking collectives, layer(): mine = lax.all_to_all(packed, 'fs', split_axis=0, concat_axis=0, tiled=True)  11.6 us
  transfers between devices with their start and end apart: 13, of which 6 were waited for; matrix products, arithmetic and copies ran while one was open for 3% of the time, Pallas kernels for 14%

profile of v1, /device:TPU:33, one launch (start us, length us, event | category | flops | bytes accessed | tf_op | source)
XLA Modules:
  0.0 207.9 jit_solution(1157843908407261422)
XLA Ops:
  6.5 0.0 copy-start
  6.6 0.0 all-gather.2.cloned.1.call-start
  6.6 2.0 pack_weights.1
  8.5 11.6 %all_to_all.5 = bf16[4,32,1664]{2,1,0:T(8,128)(2,1)} all-to-all(bf16[4,32,1664]{2,1,0:T(8,128)(2,1)} %pack_weights.1), channel_id=1, replica_groups=mesh['grp'=2,'sp'=16,'fs'=4,'tp'=2] {'fs'}, dimensions={0} | all-to-all | bytes 851968 | tf_op jit(solution)/shard_map/all_to_all | solution.py:245
  20.1 1.8 turn_weights.1
  22.0 0.1 all-gather.2.cloned.1.call-update
  22.1 0.3 fusion
  22.4 0.3 fusion.2.refs_4_
  22.7 1.0 collective-permute-start.3
  23.7 0.6 collective-permute-start.1
  24.3 0.7 dynamic-slice_convert_fusion
  25.0 12.2 %collective-permute-done.3.refs_2_ = bf16[256,2048]{1,0:T(8,128)(2,1)S(1)} collective-permute-done((bf16[256,2048]{1,0:T(8,128)(2,1)S(1)}, bf16[256,2048]{1,0:T(8,128)(2,1)S(1)}, u32[]{:S(2)}, u32[]{:S(2)}) %collective-permute-start.3) | collective-permute-done | bytes 1048608 | tf_op jit(solution)/shard_map/ppermute | solution.py:24
  37.2 3.6 %collective-permute-start.4 = (bf16[128,2048]{1,0:T(8,128)(2,1)S(1)}, bf16[128,2048]{1,0:T(8,128)(2,1)}, u32[]{:S(2)}, u32[]{:S(2)}) collective-permute-start(bf16[128,2048]{1,0:T(8,128)(2,1)S(1)} %slice.19), channel_id=1, source_target_pairs={{0,6},{2,0},{4,2},{6,4},{1,7},{3,1},{5,3},{7,5},{8,14},{10,8},{12,... | collective-permute-start | bytes 1572872 | tf_op jit(solution)/shard_map/ppermute | solution.py:24
  40.8 0.4 collective-permute-done.1.refs_3_
  41.2 1.1 slice.18
  42.2 0.1 collective-permute-start.2
  42.4 0.1 dynamic-slice_bitcast_fusion
  42.5 22.6 %collective-permute-start = (f32[4,256]{1,0:T(4,128)S(1)}, f32[4,256]{1,0:T(4,128)S(1)}, u32[]{:S(2)}, u32[]{:S(2)}) collective-permute-start(f32[4,256]{1,0:T(4,128)S(1)} %select_maximum_fusion), channel_id=1, source_target_pairs={{0,1},{1,0},{2,3},{3,2},{4,5},{5,4},{6,7},{7,6},{8,9},{9,8},{10,11... | collective-permute-start | bytes 12296 | tf_op jit(solution)/shard_map/ppermute | solution.py:275
  65.1 0.6 pad_add_fusion.idx
  65.6 0.3 collective-permute-done
  65.9 0.5 slice.17
  66.4 59.2 %all-gather.2.cloned.1.call-done = bf16[4096,1664]{1,0:T(8,128)(2,1)} async-done(((bf16[128,1664]{1,0:T(8,128)(2,1)}), bf16[4096,1664]{1,0:T(8,128)(2,1)}) %all-gather.2.cloned.1.call-update) | async-done | bytes 13631504 | tf_op jit(solution)/shard_map/all_gather | solution.py:253
  125.6 0.0 collective-permute-done.4.refs_1_
  125.6 0.0 collective-permute-done.2.refs_0_
  125.7 17.9 %project_rows.1 = (bf16[2,4,256,1152]{3,2,1,0:T(8,128)(2,1)}, bf16[2,4,160,128]{3,2,1,0:T(8,128)(2,1)}, bf16[1024,2048]{1,0:T(8,128)(2,1)}) custom-call(bf16[16,2,128,1664]{3,2,1,0:T(8,128)(2,1)} %bitcast.30, bf16[128,2048]{1,0:T(8,128)(2,1)} %collective-permute-done.2.refs_0_, bf16[128,2048]{1,0:T(8,128)(2,1)} %collective-permute-done.4.refs_1_, ...), custom_call_target="tpu_custom_call" | custom-call | flops 9663676416 | bytes 25000000 | tf_op jit(solution)/shard_map/project_rows/pallas_call | solution.py:281
  143.6 2.4 %collective-permute-start.5 = (bf16[2,4,160,128]{3,2,1,0:T(8,128)(2,1)}, bf16[2,4,160,128]{3,2,1,0:T(8,128)(2,1)S(1)}, u32[]{:S(2)}, u32[]{:S(2)}) collective-permute-start(bf16[2,4,160,128]{3,2,1,0:T(8,128)(2,1)} %get-tuple-element.26), channel_id=1, source_target_pairs={{0,1},{1,8},{8,9},{9,16},{16,17},{17,24},{24,25},{25,32},{32,33},{... | collective-permute-start | bytes 983048 | tf_op jit(solution)/shard_map/ppermute | solution.py:307
  146.1 7.0 %shard_map.121 = (bf16[128,2048]{1,0:T(8,128)(2,1)}, bf16[128,2048]{1,0:T(8,128)(2,1)}) custom-call(s32[2]{0:T(128)} %pad_add_fusion.idx, f32[2,4]{1,0:T(2,128)} %bitcast.25, f32[2,3,256]{2,1,0:T(4,128)} %bitcast.19, bf16[1024,2048]{1,0:T(8,128)(2,1)} %get-tuple-element.24.wout, bf16[2,4,256,1152]{3,2,1,0:T(8,128)(2,1)} %get-tuple-element.25.refs_0_.refs_1_, ...), custom_call_target="tpu_custom_call" | custom-call | flops 1673741824 | bytes 8000000 | tf_op jit(solution)/shard_map/pallas_call | solution.py:316
  153.1 2.6 %collective-permute-start.10 = (bf16[128,2048]{1,0:T(8,128)(2,1)}, bf16[128,2048]{1,0:T(8,128)(2,1)S(1)}, u32[]{:S(2)}, u32[]{:S(2)}) collective-permute-start(bf16[128,2048]{1,0:T(8,128)(2,1)} %get-tuple-element.34), channel_id=1, source_target_pairs={{0,6},{2,0},{4,2},{6,4},{1,7},{3,1},{5,3},{7,5},{8,14},{10,8},{12,... | collective-permute-start | bytes 1572872 | tf_op jit(solution)/shard_map/ppermute | solution.py:24
  155.7 0.0 collective-permute-start.9
  155.7 0.0 collective-permute-done.5.refs_2_.refs_3_
  155.7 0.8 copy-done.1
  156.5 7.0 %shard_map.120 = (bf16[128,2048]{1,0:T(8,128)(2,1)}, bf16[128,2048]{1,0:T(8,128)(2,1)}) custom-call(s32[2]{0:T(128)} %pad_add_fusion.idx, f32[2,4]{1,0:T(2,128)} %bitcast.26, f32[2,3,256]{2,1,0:T(4,128)} %bitcast.20, bf16[1024,2048]{1,0:T(8,128)(2,1)} %get-tuple-element.24.wout, bf16[2,4,256,1152]{3,2,1,0:T(8,128)(2,1)} %get-tuple-element.25.refs_0_.refs_1_, ...), custom_call_target="tpu_custom_call" | custom-call | flops 1673741824 | bytes 8000000 | tf_op jit(solution)/shard_map/pallas_call | solution.py:316
  163.5 0.2 collective-permute-start.6
  163.7 2.5 %collective-permute-start.8 = (bf16[128,2048]{1,0:T(8,128)(2,1)}, bf16[128,2048]{1,0:T(8,128)(2,1)S(1)}, u32[]{:S(2)}, u32[]{:S(2)}) collective-permute-start(bf16[128,2048]{1,0:T(8,128)(2,1)} %get-tuple-element.31), channel_id=1, source_target_pairs={{0,6},{2,0},{4,2},{6,4},{1,7},{3,1},{5,3},{7,5},{8,14},{10,8},{12,... | collective-permute-start | bytes 1572872 | tf_op jit(solution)/shard_map/ppermute | solution.py:24
  166.2 7.0 %shard_map.119 = (bf16[128,2048]{1,0:T(8,128)(2,1)}, bf16[128,2048]{1,0:T(8,128)(2,1)}) custom-call(s32[2]{0:T(128)} %pad_add_fusion.idx, f32[2,4]{1,0:T(2,128)} %bitcast.27, f32[2,3,256]{2,1,0:T(4,128)} %bitcast.21, bf16[1024,2048]{1,0:T(8,128)(2,1)} %get-tuple-element.24.wout, bf16[2,4,256,1152]{3,2,1,0:T(8,128)(2,1)} %get-tuple-element.25.refs_0_.refs_1_, ...), custom_call_target="tpu_custom_call" | custom-call | flops 1673741824 | bytes 8000000 | tf_op jit(solution)/shard_map/pallas_call | solution.py:316
  173.2 0.0 collective-permute-done.10
  173.2 1.2 add_convert_fusion
  174.5 1.6 collective-permute-start.11
  176.1 5.7 %collective-permute-done.6 = bf16[128,2048]{1,0:T(8,128)(2,1)S(1)} collective-permute-done((bf16[128,2048]{1,0:T(8,128)(2,1)}, bf16[128,2048]{1,0:T(8,128)(2,1)S(1)}, u32[]{:S(2)}, u32[]{:S(2)}) %collective-permute-start.6) | collective-permute-done | bytes 524320 | tf_op jit(solution)/shard_map/ppermute | solution.py:24
  181.8 1.2 add_convert_fusion.1
  183.0 0.4 collective-permute-start.7
  183.3 7.1 %shard_map.118 = (bf16[128,2048]{1,0:T(8,128)(2,1)}, bf16[128,2048]{1,0:T(8,128)(2,1)}) custom-call(s32[2]{0:T(128)} %pad_add_fusion.idx, f32[2,4]{1,0:T(2,128)} %bitcast.28, f32[2,3,256]{2,1,0:T(4,128)} %bitcast.22, bf16[1024,2048]{1,0:T(8,128)(2,1)} %get-tuple-element.24.wout, bf16[2,4,256,1152]{3,2,1,0:T(8,128)(2,1)} %get-tuple-element.25.refs_0_.refs_1_, ...), custom_call_target="tpu_custom_call" | custom-call | flops 1673741824 | bytes 8000000 | tf_op jit(solution)/shard_map/pallas_call | solution.py:316
  190.4 0.0 collective-permute-done.9.up_b
  190.5 0.0 collective-permute-done.8.down_a
  190.5 0.0 collective-permute-done.11.down_b
  190.5 6.5 %collective-permute-done.7.up_a = bf16[128,2048]{1,0:T(8,128)(2,1)S(1)} collective-permute-done((bf16[128,2048]{1,0:T(8,128)(2,1)S(1)}, bf16[128,2048]{1,0:T(8,128)(2,1)S(1)}, u32[]{:S(2)}, u32[]{:S(2)}) %collective-permute-start.7) | collective-permute-done | bytes 524320 | tf_op jit(solution)/shard_map/ppermute | solution.py:24
  197.1 0.8 copy-done.7
  197.9 3.2 %finish_rows.1 = bf16[256,2048]{1,0:T(8,128)(2,1)} custom-call(bf16[128,2048]{1,0:T(8,128)(2,1)} %get-tuple-element.27.low, bf16[128,2048]{1,0:T(8,128)(2,1)} %get-tuple-element.28.high, bf16[128,2048]{1,0:T(8,128)(2,1)} %copy-done.7, bf16[128,2048]{1,0:T(8,128)(2,1)} %copy-done.5, bf16[128,2048]{1,0:T(8,128)(2,1)} %copy-done.4, bf16[128,2048]{1,0:T(8,128)(2,1)} %copy-done.6), custom_call_target="tpu_custom_call" | custom-call | tf_op jit(solution)/shard_map/finish_rows/pallas_call | solution.py:348
  (24 shorter events, 0.1 us)
Async XLA Ops:
  6.5 35.8 %copy-start = (f32[16]{0:T(128)S(1)}, f32[16]{0:T(128)}, u32[]{:S(2)}) copy-start(f32[16]{0:T(128)} %param.21) | copy-start | bytes 196
  6.6 15.5 %copy-start.2 = (bf16[1,256,2048]{2,1,0:T(8,128)(2,1)S(1)}, bf16[1,256,2048]{2,1,0:T(8,128)(2,1)}, u32[]{:S(2)}) copy-start(bf16[1,256,2048]{2,1,0:T(8,128)(2,1)} %param.12) | copy-start | bytes 3145732
  6.6 15.8 %copy-start.10 = (f32[2048]{0:T(1024)S(1)}, f32[2048]{0:T(1024)}, u32[]{:S(2)}) copy-start(f32[2048]{0:T(1024)} %param.13) | copy-start | bytes 24580
  6.6 119.1 %all-gather.2.cloned.1.call-start = ((), (), s32[]{:S(2)}) async-start(), calls=%async_computation.1 | async-start | bytes 14057472 | tf_op jit(solution)/shard_map/all_gather | solution.py:253
  22.7 103.0 %copy-start.3 = (bf16[256,2048]{1,0:T(8,128)(2,1)}, bf16[256,2048]{1,0:T(8,128)(2,1)S(1)}, u32[]{:S(2)}) copy-start(bf16[256,2048]{1,0:T(8,128)(2,1)S(1)} %fusion.2.refs_4_) | copy-start | bytes 3145732
  22.7 14.5 %collective-permute-start.3 = (bf16[256,2048]{1,0:T(8,128)(2,1)S(1)}, bf16[256,2048]{1,0:T(8,128)(2,1)S(1)}, u32[]{:S(2)}, u32[]{:S(2)}) collective-permute-start(bf16[256,2048]{1,0:T(8,128)(2,1)S(1)} %fusion.2.refs_4_), channel_id=1, source_target_pairs={{0,6},{2,0},{4,2},{6,4},{1,7},{3,1},{5,3},{7,5},{8,14},{10,8},{12,... | collective-permute-start | bytes 3145736 | tf_op jit(solution)/shard_map/ppermute | solution.py:24
  23.7 17.5 %collective-permute-start.1 = (bf16[256,2048]{1,0:T(8,128)(2,1)S(1)}, bf16[256,2048]{1,0:T(8,128)(2,1)}, u32[]{:S(2)}, u32[]{:S(2)}) collective-permute-start(bf16[256,2048]{1,0:T(8,128)(2,1)S(1)} %fusion.2.refs_4_), channel_id=1, source_target_pairs={{0,2},{2,4},{4,6},{6,0},{1,3},{3,5},{5,7},{7,1},{8,10},{10,12},{12... | collective-permute-start | bytes 3145736 | tf_op jit(solution)/shard_map/ppermute | solution.py:24
  37.2 88.5 %copy-start.8 = (bf16[256,2048]{1,0:T(8,128)(2,1)}, bf16[256,2048]{1,0:T(8,128)(2,1)S(1)}, u32[]{:S(2)}) copy-start(bf16[256,2048]{1,0:T(8,128)(2,1)S(1)} %collective-permute-done.3.refs_2_) | copy-start | bytes 3145732
  37.2 88.4 %collective-permute-start.4 = (bf16[128,2048]{1,0:T(8,128)(2,1)S(1)}, bf16[128,2048]{1,0:T(8,128)(2,1)}, u32[]{:S(2)}, u32[]{:S(2)}) collective-permute-start(bf16[128,2048]{1,0:T(8,128)(2,1)S(1)} %slice.19), channel_id=1, source_target_pairs={{0,6},{2,0},{4,2},{6,4},{1,7},{3,1},{5,3},{7,5},{8,14},{10,8},{12,... | collective-permute-start | bytes 1572872 | tf_op jit(solution)/shard_map/ppermute | solution.py:24
  42.2 83.4 %collective-permute-start.2 = (bf16[128,2048]{1,0:T(8,128)(2,1)S(1)}, bf16[128,2048]{1,0:T(8,128)(2,1)}, u32[]{:S(2)}, u32[]{:S(2)}) collective-permute-start(bf16[128,2048]{1,0:T(8,128)(2,1)S(1)} %slice.18), channel_id=1, source_target_pairs={{0,2},{2,4},{4,6},{6,0},{1,3},{3,5},{5,7},{7,1},{8,10},{10,12},{12... | collective-permute-start | bytes 1572872 | tf_op jit(solution)/shard_map/ppermute | solution.py:24
  42.5 23.4 %collective-permute-start = (f32[4,256]{1,0:T(4,128)S(1)}, f32[4,256]{1,0:T(4,128)S(1)}, u32[]{:S(2)}, u32[]{:S(2)}) collective-permute-start(f32[4,256]{1,0:T(4,128)S(1)} %select_maximum_fusion), channel_id=1, source_target_pairs={{0,1},{1,0},{2,3},{3,2},{4,5},{5,4},{6,7},{7,6},{8,9},{9,8},{10,11... | collective-permute-start | bytes 12296 | tf_op jit(solution)/shard_map/ppermute | solution.py:275
  65.9 77.7 %copy-start.9 = (f32[2,4,256]{2,1,0:T(4,128)}, f32[2,4,256]{2,1,0:T(4,128)S(1)}, u32[]{:S(2)}) copy-start(f32[2,4,256]{2,1,0:T(4,128)S(1)} %maximum_select_fusion) | copy-start | bytes 24580
  143.6 12.1 %collective-permute-start.5 = (bf16[2,4,160,128]{3,2,1,0:T(8,128)(2,1)}, bf16[2,4,160,128]{3,2,1,0:T(8,128)(2,1)S(1)}, u32[]{:S(2)}, u32[]{:S(2)}) collective-permute-start(bf16[2,4,160,128]{3,2,1,0:T(8,128)(2,1)} %get-tuple-element.26), channel_id=1, source_target_pairs={{0,1},{1,8},{8,9},{9,16},{16,17},{17,24},{24,25},{25,32},{32,33},{... | collective-permute-start | bytes 983048 | tf_op jit(solution)/shard_map/ppermute | solution.py:307
  153.1 20.1 %collective-permute-start.10 = (bf16[128,2048]{1,0:T(8,128)(2,1)}, bf16[128,2048]{1,0:T(8,128)(2,1)S(1)}, u32[]{:S(2)}, u32[]{:S(2)}) collective-permute-start(bf16[128,2048]{1,0:T(8,128)(2,1)} %get-tuple-element.34), channel_id=1, source_target_pairs={{0,6},{2,0},{4,2},{6,4},{1,7},{3,1},{5,3},{7,5},{8,14},{10,8},{12,... | collective-permute-start | bytes 1572872 | tf_op jit(solution)/shard_map/ppermute | solution.py:24
  155.7 34.7 %collective-permute-start.9 = (bf16[128,2048]{1,0:T(8,128)(2,1)}, bf16[128,2048]{1,0:T(8,128)(2,1)S(1)}, u32[]{:S(2)}, u32[]{:S(2)}) collective-permute-start(bf16[128,2048]{1,0:T(8,128)(2,1)} %get-tuple-element.32), channel_id=1, source_target_pairs={{0,2},{2,4},{4,6},{6,0},{1,3},{3,5},{5,7},{7,1},{8,10},{10,12},{12... | collective-permute-start | bytes 1572872 | tf_op jit(solution)/shard_map/ppermute | solution.py:24
  155.7 0.8 copy-start.1
  163.5 18.2 %collective-permute-start.6 = (bf16[128,2048]{1,0:T(8,128)(2,1)}, bf16[128,2048]{1,0:T(8,128)(2,1)S(1)}, u32[]{:S(2)}, u32[]{:S(2)}) collective-permute-start(bf16[128,2048]{1,0:T(8,128)(2,1)} %get-tuple-element.30), channel_id=1, source_target_pairs={{0,2},{2,4},{4,6},{6,0},{1,3},{3,5},{5,7},{7,1},{8,10},{10,12},{12... | collective-permute-start | bytes 1572872 | tf_op jit(solution)/shard_map/ppermute | solution.py:24
  163.7 26.7 %collective-permute-start.8 = (bf16[128,2048]{1,0:T(8,128)(2,1)}, bf16[128,2048]{1,0:T(8,128)(2,1)S(1)}, u32[]{:S(2)}, u32[]{:S(2)}) collective-permute-start(bf16[128,2048]{1,0:T(8,128)(2,1)} %get-tuple-element.31), channel_id=1, source_target_pairs={{0,6},{2,0},{4,2},{6,4},{1,7},{3,1},{5,3},{7,5},{8,14},{10,8},{12,... | collective-permute-start | bytes 1572872 | tf_op jit(solution)/shard_map/ppermute | solution.py:24
  174.5 16.0 %collective-permute-start.11 = (bf16[128,2048]{1,0:T(8,128)(2,1)S(1)}, bf16[128,2048]{1,0:T(8,128)(2,1)S(1)}, u32[]{:S(2)}, u32[]{:S(2)}) collective-permute-start(bf16[128,2048]{1,0:T(8,128)(2,1)S(1)} %add_convert_fusion), channel_id=1, source_target_pairs={{0,6},{2,0},{4,2},{6,4},{1,7},{3,1},{5,3},{7,5},{8,14},{10,8},{12,... | collective-permute-start | bytes 1572872 | tf_op jit(solution)/shard_map/ppermute | solution.py:24
  183.0 14.1 %collective-permute-start.7 = (bf16[128,2048]{1,0:T(8,128)(2,1)S(1)}, bf16[128,2048]{1,0:T(8,128)(2,1)S(1)}, u32[]{:S(2)}, u32[]{:S(2)}) collective-permute-start(bf16[128,2048]{1,0:T(8,128)(2,1)S(1)} %add_convert_fusion.1), channel_id=1, source_target_pairs={{0,2},{2,4},{4,6},{6,0},{1,3},{3,5},{5,7},{7,1},{8,10},{10,12},{12... | collective-permute-start | bytes 1572872 | tf_op jit(solution)/shard_map/ppermute | solution.py:24
  190.4 6.6 %copy-start.4 = (bf16[128,2048]{1,0:T(8,128)(2,1)}, bf16[128,2048]{1,0:T(8,128)(2,1)S(1)}, u32[]{:S(2)}) copy-start(bf16[128,2048]{1,0:T(8,128)(2,1)S(1)} %collective-permute-done.9.up_b) | copy-start | bytes 1572868
  190.5 6.6 %copy-start.5 = (bf16[128,2048]{1,0:T(8,128)(2,1)}, bf16[128,2048]{1,0:T(8,128)(2,1)S(1)}, u32[]{:S(2)}) copy-start(bf16[128,2048]{1,0:T(8,128)(2,1)S(1)} %collective-permute-done.8.down_a) | copy-start | bytes 1572868
  190.5 6.6 %copy-start.6 = (bf16[128,2048]{1,0:T(8,128)(2,1)}, bf16[128,2048]{1,0:T(8,128)(2,1)S(1)}, u32[]{:S(2)}) copy-start(bf16[128,2048]{1,0:T(8,128)(2,1)S(1)} %collective-permute-done.11.down_b) | copy-start | bytes 1572868
  197.0 0.8 copy-start.7
Sparse Core Ops, SparseCore 0:
  22.2 103.4 all-gather.1

commit v2 on v1

--- a/solution.py
+++ b/solution.py
@@ -42,14 +42,6 @@
     out[:, :in_cols] = mine[:, :in_cols]
     for at in range(in_cols, width, block):
         out[:, at : at + block] = mine[:, at : at + block].T
-
-
-def finish_kernel(low, high, up_a, down_a, up_b, down_b, out):
-    half = up_a.shape[0]
-    for at, own, up, down in ((0, low, up_a, down_a), (half, high, up_b, down_b)):
-        total = own[...].astype(jnp.float32) + up[...].astype(jnp.float32)
-        total = total + down[...].astype(jnp.float32)
-        out[at : at + half, :] = total.astype(jnp.bfloat16)
 
 
 def project_kernel(wide, weights, *refs):
@@ -67,38 +59,39 @@
             ((succ, 0, 0), (prev, 1, 0), (opp_a, 2, 0), (opp_b, 2, half), (own, 3, 0))
         )
     ]
-    w_copies = [
-        pltpu.make_async_copy(weights.at[:, t, :, pl.ds(0, in_cols)], ws.at[t], sems.at[5 + t])
-        for t in range(2)
-    ]
+    cuts = ((0, 4 * block), (4 * block, in_cols - 4 * block))
+
+    def w_copy(t, k):
+        cols = pl.ds(*cuts[k])
+        return pltpu.make_async_copy(weights.at[:, t, :, cols], ws.at[t, :, :, cols], sems.at[5 + 2 * t + k])
 
     def out_copies(t):
         return [
             pltpu.make_async_copy(
                 weights.at[j, t, :, pl.ds(in_cols + b * block, block)],
                 wo.at[pl.ds((t * parts + b) * block, block), pl.ds(j * block, block)],
-                sems.at[7 + (t * parts + b) * blocks + j],
+                sems.at[9 + (t * parts + b) * blocks + j],
             )
             for b in range(parts)
             for j in range(blocks)
         ]
 
-    laid_out = pltpu.make_async_copy(wo, wout, sems.at[7 + 2 * parts * blocks])
+    laid_out = pltpu.make_async_copy(wo, wout, sems.at[9 + 2 * parts * blocks])
 
     @pl.when(step == 0)
     def _():
-        for c in x_copies + w_copies[:1]:
+        for c in x_copies:
             c.start()
-        for c in x_copies + w_copies[:1]:
+        w_copy(0, 0).start()
+        w_copy(0, 1).start()
+        for c in x_copies:
             c.wait()
-        w_copies[1].start()
-        for t in range(2):
-            for c in out_copies(t):
-                c.start()
+        w_copy(0, 0).wait()
 
     @pl.when(step == 1)
     def _():
-        w_copies[1].wait()
+        w_copy(1, 0).wait()
+        w_copy(1, 1).wait()
         for t in range(2):
             for c in out_copies(t):
                 c.wait()
@@ -106,13 +99,29 @@
 
     seqs, length, feats = xs.shape
     x = xs[...].reshape(seqs * length, feats)
-    w = ws[step].reshape(feats, in_cols)
-    rounded = jnp.dot(x, w, preferred_element_type=f32).astype(bf16).reshape(seqs, length, in_cols)
-    out[0] = rounded
+
+    def project(k):
+        cols = slice(cuts[k][0], cuts[k][0] + cuts[k][1])
+        w = ws[step, :, :, cols].reshape(feats, cuts[k][1])
+        product = jnp.dot(x, w, preferred_element_type=f32).astype(bf16)
+        out[0, :, :, cols] = product.reshape(seqs, length, cuts[k][1])
+
+    project(0)
+
+    @pl.when(step == 0)
+    def _():
+        w_copy(0, 1).wait()
+        w_copy(1, 0).start()
+        w_copy(1, 1).start()
+        for t in range(2):
+            for c in out_copies(t):
+                c.start()
+
+    project(1)
     chans = wide // 3
     for s in range(seqs):
-        edge[0, s, 0:WINDOW, :] = rounded[s, length - WINDOW :, wide + chans :]
-        last = rounded[s, length - 16 :, chans:wide].astype(f32)
+        edge[0, s, 0:WINDOW, :] = out[0, s, length - WINDOW :, wide + chans :]
+        last = out[0, s, length - 16 :, chans:wide].astype(f32)
         gated = (last[:, :chans] * last[:, chans:]).astype(bf16)
         edge[0, s, WINDOW : WINDOW + 16, :] = gated[:, : 2 * HEAD]
         edge[0, s, WINDOW + 16 : WINDOW + 32, :] = gated[:, 2 * HEAD :]
@@ -122,9 +131,15 @@
         laid_out.wait()
 
 
-def mix_kernel(blocks, wide, idx, sinks, taps, wout, *refs):
-    projs, edges = refs[:2], refs[2:-3]
-    low, high, acts = refs[-3:]
+def mix_kernel(blocks, pieces, wide, idx, sinks, taps, wout, *refs):
+    acts, wo, sem = refs[-3:]
+    outs_at = len(refs) - 3 - len(pieces)
+    results = refs[outs_at:-3]
+    first_edge = 2 if 0 in blocks else 0
+    projs, edges = refs[:2], refs[2 : 2 + first_edge]
+    arrived = refs[2 + first_edge : outs_at]
+    wanted = pltpu.make_async_copy(wout, wo, sem)
+    wanted.start()
     place = idx[0]
     chans = wide // 3
     heads = chans // HEAD
@@ -199,9 +214,15 @@
                     left, outs[2 * j], outs[2 * j + 1]
                 ).astype(bf16)
 
-    product = jnp.dot(acts[...], wout[...], preferred_element_type=f32).astype(bf16)
-    low[...] = product[:WINDOW]
-    high[...] = product[WINDOW:]
+    wanted.wait()
+    product = jnp.dot(acts[...], wo[...], preferred_element_type=f32)
+    if arrived:
+        product = product + jnp.concatenate([a[...] for a in arrived], axis=0).astype(f32)
+    product = product.astype(bf16)
+    at = 0
+    for ref in results:
+        ref[...] = product[at : at + ref.shape[0]]
+        at += ref.shape[0]
 
 
 def added(*parts):
@@ -296,7 +317,7 @@
             pltpu.VMEM((fs, here, feats), bf16),
             pltpu.VMEM((tp, sp, block, in_cols), bf16),
             pltpu.VMEM((tp * out_cols, feats), bf16),
-            pltpu.SemaphoreType.DMA((8 + tp * squares * sp,)),
+            pltpu.SemaphoreType.DMA((10 + tp * squares * sp,)),
         ],
         cost_estimate=pl.CostEstimate(
             flops=2 * tp * fs * here * feats * in_cols, bytes_accessed=25_000_000, transcendentals=0
@@ -306,7 +327,7 @@
     )(weights, opp_a, opp_b, succ, prev, normed)
     edge = lax.ppermute(edge, ("sp", "tp"), [(i, i + 1) for i in range(sp * tp - 1)])
 
-    def mix(tasks):
+    def mix(tasks, pieces, arrived=()):
         seqs, blocks = zip(*tasks)
         edged = [q for q, n in tasks if n == 0]
 
@@ -314,45 +335,41 @@
             return pl.BlockSpec((tp, 1) + shape, lambda i, q=q: (0, q, 0, 0))
 
         return pl.pallas_call(
-            functools.partial(mix_kernel, blocks, b_width),
-            out_shape=(jax.ShapeDtypeStruct((half, feats), bf16),) * 2,
+            functools.partial(mix_kernel, blocks, pieces, b_width),
+            out_shape=tuple(jax.ShapeDtypeStruct((n, feats), bf16) for n in pieces),
             grid=(1,),
-            in_specs=[
-                SMEM,
-                SMEM,
-                pl.BlockSpec((tp, TAPS, chans), lambda i: (0, 0, 0)),
-                pl.BlockSpec((tp * out_cols, feats), lambda i: (0, 0)),
-            ]
+            in_specs=[SMEM, SMEM, pl.BlockSpec((tp, TAPS, chans), lambda i: (0, 0, 0)), ANY]
             + [part((here, in_cols), q) for q in seqs]
-            + [part((WINDOW + 32, 2 * HEAD), q) for q in (seqs if edged else ())],
-            out_specs=(pl.BlockSpec((half, feats), lambda i: (0, 0)),) * 2,
-            scratch_shapes=[pltpu.VMEM((here, tp * out_cols), bf16)],
+            + [part((WINDOW + 32, 2 * HEAD), q) for q in (seqs if edged else ())]
+            + [pl.BlockSpec(a.shape, lambda i: (0, 0)) for a in arrived],
+            out_specs=tuple(pl.BlockSpec((n, feats), lambda i: (0, 0)) for n in pieces),
+            scratch_shapes=[
+                pltpu.VMEM((here, tp * out_cols), bf16),
+                pltpu.VMEM((tp * out_cols, feats), bf16),
+                pltpu.SemaphoreType.DMA,
+            ],
             cost_estimate=pl.CostEstimate(
                 flops=2 * here * feats * tp * out_cols + 600_000_000,
                 bytes_accessed=8_000_000,
                 transcendentals=600_000,
             ),
-        )(idx, sinks, taps, wout, proj, proj, *((edge, edge) if edged else ()))
+        )(idx, sinks, taps, wout, proj, proj, *((edge, edge) if edged else ()), *arrived)
 
     def sent(array, by):
         return ring(array, "fs", by)
 
     succ_q, prev_q, opp_q, own_q = range(4)
-    low, high = mix(((succ_q, 1), (opp_q, 1)))
+    low, high = mix(((succ_q, 1), (opp_q, 1)), (half, half))
     down, up_b = sent(high, -1), sent(low, 1)
-    low, high = mix(((opp_q, 0), (prev_q, 0)))
-    up, down_a = sent(low, 1), sent(high, -1)
-    low, high = mix(((succ_q, 0), (prev_q, 1)))
-    down_b, up_a = sent(added(high, down), -1), sent(added(low, up), 1)
-    low, high = mix(((own_q, 0), (own_q, 1)))
-    out = pl.pallas_call(
-        finish_kernel,
-        out_shape=jax.ShapeDtypeStruct((here, feats), bf16),
-        in_specs=[VMEM] * 6,
-        out_specs=VMEM,
-        name="finish_rows",
-    )(low, high, up_a, down_a, up_b, down_b)
-    return out[None]
+    quarter = half // 2
+    low_1, low_2, high = mix(((opp_q, 0), (prev_q, 0)), (quarter, quarter, half))
+    up_1, up_2 = sent(low_1, 1), sent(low_2, 1)
+    down_a = sent(high, -1)
+    low_1, low_2, high = mix(((succ_q, 0), (prev_q, 1)), (quarter, quarter, half))
+    down_b = sent(added(high, down), -1)
+    up_a1, up_a2 = sent(added(low_1, up_1), 1), sent(added(low_2, up_2), 1)
+    (own,) = mix(((own_q, 0), (own_q, 1)), (here,), (down_a, up_b))
+    return added(own, jnp.concatenate([up_a1, up_a2, down_b], 0))[None]
 
 
 def solution(mesh):

time: 208 us -> 206 us (level)
  waiting for transfers between devices: 84.4 us -> 80.8 us
  Pallas kernels: 53.1 us -> 50.5 us
  other arithmetic: 4.31 us -> 6.81 us
    pallas_call x5 -> x4, Pallas kernels: 31.4 us -> 24.8 us  [mix(): pl.pallas_call(functools.partial(mix_kernel, blocks, pieces, b_width), ou...]
    pallas_call x1, Pallas kernels: 17.9 us -> 21.9 us  [layer(): pl.pallas_call(functools.partial(project_kernel, b_width), out_shape=(jax...]
    ppermute x10 -> x12, waiting for transfers between devices: 24.9 us -> 21.2 us  [ring(): lax.ppermute(array, axis, [(i, (i + by) % size) for i in range(size)])]
    broadcast_in_dim x0 -> x1, other arithmetic: none -> 2.59 us  [layer(): return added(own, jnp.concatenate([up_a1, up_a2, down_b], 0))[None]]
    ppermute x10 -> x12, starting transfers between devices: 12.5 us -> 12.8 us  [ring(): lax.ppermute(array, axis, [(i, (i + by) % size) for i in range(size)])]
  transfers between devices with their start and end apart: 13 -> 15, of which waited for: 6 -> 7; matrix products, arithmetic and copies ran while one was open for 3% -> 3% of each run, Pallas kernels for 14% -> 12%
where the time goes in v2:
time: 206 us; the launch traced here: 205 us
  waiting for transfers between devices  80.8 us (39%)
  Pallas kernels  50.5 us (25%)
  starting transfers between devices  38 us (18%)
  between operations  13.6 us (7%)
  blocking collectives  11.6 us (6%)
  other arithmetic  6.81 us (3%)
  local copies, waits for them, and re-layouts  4.14 us (2%)
    all_gather x1, waiting for transfers between devices, layer(): weights = lax.all_gather(mine, ('sp', 'tp'), axis=0, tiled=True)  59.2 us
    pallas_call x4, Pallas kernels, mix(): pl.pallas_call(functools.partial(mix_kernel, blocks, pieces, b_width), ou...  24.8 us
    ppermute x1, starting transfers between devices, layer(): theirs = lax.ppermute(small, 'tp', [(0, 1), (1, 0)])  22.6 us
    pallas_call x1, Pallas kernels, layer(): pl.pallas_call(functools.partial(project_kernel, b_width), out_shape=(jax...  21.9 us
    ppermute x12, waiting for transfers between devices, ring(): lax.ppermute(array, axis, [(i, (i + by) % size) for i in range(size)])  21.2 us
    ppermute x12, starting transfers between devices, ring(): lax.ppermute(array, axis, [(i, (i + by) % size) for i in range(size)])  12.8 us
    all_to_all x1, blocking collectives, layer(): mine = lax.all_to_all(packed, 'fs', split_axis=0, concat_axis=0, tiled=True)  11.6 us
  transfers between devices with their start and end apart: 15, of which 7 were waited for; matrix products, arithmetic and copies ran while one was open for 3% of the time, Pallas kernels for 12%

profile of v2, /device:TPU:33, one launch (start us, length us, event | category | flops | bytes accessed | tf_op | source)
XLA Modules:
  0.0 205.5 jit_solution(6518366446096492016)
XLA Ops:
  6.6 2.0 pack_weights.1
  8.5 11.6 %all_to_all.5 = bf16[4,32,1664]{2,1,0:T(8,128)(2,1)} all-to-all(bf16[4,32,1664]{2,1,0:T(8,128)(2,1)} %pack_weights.1), channel_id=1, replica_groups=mesh['grp'=2,'sp'=16,'fs'=4,'tp'=2] {'fs'}, dimensions={0} | all-to-all | bytes 851968 | tf_op jit(solution)/shard_map/all_to_all | solution.py:266
  20.1 1.8 turn_weights.1
  22.0 0.1 all-gather.2.cloned.1.call-update
  22.1 0.3 fusion
  22.4 0.3 fusion.2.refs_4_
  22.7 1.0 collective-permute-start.3
  23.7 0.6 collective-permute-start.1
  24.3 0.7 dynamic-slice_convert_fusion
  25.0 12.2 %collective-permute-done.3.refs_2_ = bf16[256,2048]{1,0:T(8,128)(2,1)S(1)} collective-permute-done((bf16[256,2048]{1,0:T(8,128)(2,1)S(1)}, bf16[256,2048]{1,0:T(8,128)(2,1)S(1)}, u32[]{:S(2)}, u32[]{:S(2)}) %collective-permute-start.3) | collective-permute-done | bytes 1048608 | tf_op jit(solution)/shard_map/ppermute | solution.py:24
  37.2 3.6 %collective-permute-start.4 = (bf16[128,2048]{1,0:T(8,128)(2,1)S(1)}, bf16[128,2048]{1,0:T(8,128)(2,1)}, u32[]{:S(2)}, u32[]{:S(2)}) collective-permute-start(bf16[128,2048]{1,0:T(8,128)(2,1)S(1)} %slice.19), channel_id=1, source_target_pairs={{0,6},{2,0},{4,2},{6,4},{1,7},{3,1},{5,3},{7,5},{8,14},{10,8},{12,... | collective-permute-start | bytes 1572872 | tf_op jit(solution)/shard_map/ppermute | solution.py:24
  40.8 0.4 collective-permute-done.1.refs_3_
  41.2 1.1 slice.18
  42.2 0.1 collective-permute-start.2
  42.4 0.1 dynamic-slice_bitcast_fusion
  42.5 22.6 %collective-permute-start = (f32[4,256]{1,0:T(4,128)S(1)}, f32[4,256]{1,0:T(4,128)S(1)}, u32[]{:S(2)}, u32[]{:S(2)}) collective-permute-start(f32[4,256]{1,0:T(4,128)S(1)} %select_maximum_fusion), channel_id=1, source_target_pairs={{0,1},{1,0},{2,3},{3,2},{4,5},{5,4},{6,7},{7,6},{8,9},{9,8},{10,11... | collective-permute-start | bytes 12296 | tf_op jit(solution)/shard_map/ppermute | solution.py:296
  65.1 0.6 pad_add_fusion.idx
  65.6 0.3 collective-permute-done
  65.9 0.5 slice.17
  66.4 59.2 %all-gather.2.cloned.1.call-done = bf16[4096,1664]{1,0:T(8,128)(2,1)} async-done(((bf16[128,1664]{1,0:T(8,128)(2,1)}), bf16[4096,1664]{1,0:T(8,128)(2,1)}) %all-gather.2.cloned.1.call-update) | async-done | bytes 13631504 | tf_op jit(solution)/shard_map/all_gather | solution.py:274
  125.6 0.0 collective-permute-done.4.refs_1_
  125.6 0.0 collective-permute-done.2.refs_0_
  125.7 21.9 %project_rows.1 = (bf16[2,4,256,1152]{3,2,1,0:T(8,128)(2,1)}, bf16[2,4,160,128]{3,2,1,0:T(8,128)(2,1)}, bf16[1024,2048]{1,0:T(8,128)(2,1)}) custom-call(bf16[16,2,128,1664]{3,2,1,0:T(8,128)(2,1)} %bitcast.31, bf16[128,2048]{1,0:T(8,128)(2,1)} %collective-permute-done.2.refs_0_, bf16[128,2048]{1,0:T(8,128)(2,1)} %collective-permute-done.4.refs_1_, ...), custom_call_target="tpu_custom_call" | custom-call | flops 9663676416 | bytes 25000000 | tf_op jit(solution)/shard_map/project_rows/pallas_call | solution.py:302
  147.6 2.6 %collective-permute-start.5 = (bf16[2,4,160,128]{3,2,1,0:T(8,128)(2,1)}, bf16[2,4,160,128]{3,2,1,0:T(8,128)(2,1)S(1)}, u32[]{:S(2)}, u32[]{:S(2)}) collective-permute-start(bf16[2,4,160,128]{3,2,1,0:T(8,128)(2,1)} %get-tuple-element.26), channel_id=1, source_target_pairs={{0,1},{1,8},{8,9},{9,16},{16,17},{17,24},{24,25},{25,32},{32,33},{... | collective-permute-start | bytes 983048 | tf_op jit(solution)/shard_map/ppermute | solution.py:328
  150.2 6.1 %shard_map.119 = (bf16[128,2048]{1,0:T(8,128)(2,1)}, bf16[128,2048]{1,0:T(8,128)(2,1)}) custom-call(s32[2]{0:T(128)} %pad_add_fusion.idx, f32[2,4]{1,0:T(2,128)} %bitcast.26, f32[2,3,256]{2,1,0:T(4,128)} %bitcast.20, bf16[1024,2048]{1,0:T(8,128)(2,1)} %get-tuple-element.24.wout, bf16[2,4,256,1152]{3,2,1,0:T(8,128)(2,1)} %get-tuple-element.25.refs_0_.refs_1_, ...), custom_call_target="tpu_custom_call" | custom-call | flops 1673741824 | bytes 8000000 | tf_op jit(solution)/shard_map/pallas_call | solution.py:337
  156.3 2.7 %collective-permute-start.12 = (bf16[128,2048]{1,0:T(8,128)(2,1)}, bf16[128,2048]{1,0:T(8,128)(2,1)S(1)}, u32[]{:S(2)}, u32[]{:S(2)}) collective-permute-start(bf16[128,2048]{1,0:T(8,128)(2,1)} %get-tuple-element.34), channel_id=1, source_target_pairs={{0,6},{2,0},{4,2},{6,4},{1,7},{3,1},{5,3},{7,5},{8,14},{10,8},{12,... | collective-permute-start | bytes 1572872 | tf_op jit(solution)/shard_map/ppermute | solution.py:24
  159.1 0.0 collective-permute-start.7
  159.1 0.0 collective-permute-done.5.refs_2_.refs_3_
  159.1 0.8 copy-done.1
  159.8 6.0 %shard_map.118 = (bf16[64,2048]{1,0:T(8,128)(2,1)}, bf16[64,2048]{1,0:T(8,128)(2,1)}, bf16[128,2048]{1,0:T(8,128)(2,1)}) custom-call(s32[2]{0:T(128)} %pad_add_fusion.idx, f32[2,4]{1,0:T(2,128)} %bitcast.27, f32[2,3,256]{2,1,0:T(4,128)} %bitcast.21, bf16[1024,2048]{1,0:T(8,128)(2,1)} %get-tuple-element.24.wout, ...), custom_call_target="tpu_custom_call" | custom-call | flops 1673741824 | bytes 8000000 | tf_op jit(solution)/shard_map/pallas_call | solution.py:337
  165.9 0.3 collective-permute-start.8
  166.2 1.1 collective-permute-start.10
  167.2 1.9 collective-permute-start.6
  169.2 6.1 %shard_map.121 = (bf16[64,2048]{1,0:T(8,128)(2,1)}, bf16[64,2048]{1,0:T(8,128)(2,1)}, bf16[128,2048]{1,0:T(8,128)(2,1)}) custom-call(s32[2]{0:T(128)} %pad_add_fusion.idx, f32[2,4]{1,0:T(2,128)} %bitcast.28, f32[2,3,256]{2,1,0:T(4,128)} %bitcast.22, bf16[1024,2048]{1,0:T(8,128)(2,1)} %get-tuple-element.24.wout, ...), custom_call_target="tpu_custom_call" | custom-call | flops 1673741824 | bytes 8000000 | tf_op jit(solution)/shard_map/pallas_call | solution.py:337
  175.2 1.3 add_convert_fusion.1
  176.5 1.2 collective-permute-start.13
  177.7 1.7 collective-permute-done.8
  179.5 1.0 add_convert_fusion.3
  180.5 0.1 collective-permute-start.9
  180.6 4.4 %collective-permute-done.10 = bf16[64,2048]{1,0:T(8,128)(2,1)S(1)} collective-permute-done((bf16[64,2048]{1,0:T(8,128)(2,1)}, bf16[64,2048]{1,0:T(8,128)(2,1)S(1)}, u32[]{:S(2)}, u32[]{:S(2)}) %collective-permute-start.10) | collective-permute-done | bytes 262176 | tf_op jit(solution)/shard_map/ppermute | solution.py:24
  185.1 0.1 add_convert_fusion.2
  185.2 0.1 collective-permute-start.11
  185.3 0.0 collective-permute-done.7.refs_5_
  185.3 0.8 copy-done.4
  186.1 0.8 copy-done.5
  186.9 6.6 %shard_map.120 = bf16[256,2048]{1,0:T(8,128)(2,1)} custom-call(s32[2]{0:T(128)} %pad_add_fusion.idx, f32[2,4]{1,0:T(2,128)} %bitcast.29, f32[2,3,256]{2,1,0:T(4,128)} %bitcast.23, bf16[1024,2048]{1,0:T(8,128)(2,1)} %get-tuple-element.24.wout, bf16[2,4,256,1152]{3,2,1,0:T(8,128)(2,1)} %get-tuple-element.25.refs_0_.refs_1_, ...), custom_call_target="tpu_custom_call" | custom-call | flops 1673741824 | bytes 8000000 | tf_op jit(solution)/shard_map/pallas_call | solution.py:337
  193.6 2.4 %collective-permute-done.11 = bf16[64,2048]{1,0:T(8,128)(2,1)S(1)} collective-permute-done((bf16[64,2048]{1,0:T(8,128)(2,1)S(1)}, bf16[64,2048]{1,0:T(8,128)(2,1)S(1)}, u32[]{:S(2)}, u32[]{:S(2)}) %collective-permute-start.11) | collective-permute-done | bytes 262176 | tf_op jit(solution)/shard_map/ppermute | solution.py:24
  196.0 2.6 %fusion.3 = bf16[1,256,2048]{2,1,0:T(8,128)(2,1)} fusion(bf16[256,2048]{1,0:T(8,128)(2,1)} %shard_map.120, bf16[128,2048]{1,0:T(8,128)(2,1)S(1)} %collective-permute-done.13, bf16[64,2048]{1,0:T(8,128)(2,1)S(1)} %collective-permute-done.11, bf16[64,2048]{1,0:T(8,128)(2,1)S(1)} %collective-permute-done.9), kind=kLoop, calls=%fused_computation.6 | loop fusion | flops 4718592 | bytes 3145728 | tf_op jit(solution)/shard_map/broadcast_in_dim | solution.py:372
  (27 shorter events, 0.1 us)
Async XLA Ops:
  6.5 35.8 %copy-start = (f32[16]{0:T(128)S(1)}, f32[16]{0:T(128)}, u32[]{:S(2)}) copy-start(f32[16]{0:T(128)} %param.21) | copy-start | bytes 196
  6.6 15.5 %copy-start.2 = (bf16[1,256,2048]{2,1,0:T(8,128)(2,1)S(1)}, bf16[1,256,2048]{2,1,0:T(8,128)(2,1)}, u32[]{:S(2)}) copy-start(bf16[1,256,2048]{2,1,0:T(8,128)(2,1)} %param.12) | copy-start | bytes 3145732
  6.6 15.8 %copy-start.9 = (f32[2048]{0:T(1024)S(1)}, f32[2048]{0:T(1024)}, u32[]{:S(2)}) copy-start(f32[2048]{0:T(1024)} %param.13) | copy-start | bytes 24580
  6.6 119.1 %all-gather.2.cloned.1.call-start = ((), (), s32[]{:S(2)}) async-start(), calls=%async_computation.1 | async-start | bytes 14057472 | tf_op jit(solution)/shard_map/all_gather | solution.py:274
  22.7 103.0 %copy-start.3 = (bf16[256,2048]{1,0:T(8,128)(2,1)}, bf16[256,2048]{1,0:T(8,128)(2,1)S(1)}, u32[]{:S(2)}) copy-start(bf16[256,2048]{1,0:T(8,128)(2,1)S(1)} %fusion.2.refs_4_) | copy-start | bytes 3145732
  22.7 14.5 %collective-permute-start.3 = (bf16[256,2048]{1,0:T(8,128)(2,1)S(1)}, bf16[256,2048]{1,0:T(8,128)(2,1)S(1)}, u32[]{:S(2)}, u32[]{:S(2)}) collective-permute-start(bf16[256,2048]{1,0:T(8,128)(2,1)S(1)} %fusion.2.refs_4_), channel_id=1, source_target_pairs={{0,6},{2,0},{4,2},{6,4},{1,7},{3,1},{5,3},{7,5},{8,14},{10,8},{12,... | collective-permute-start | bytes 3145736 | tf_op jit(solution)/shard_map/ppermute | solution.py:24
  23.7 17.5 %collective-permute-start.1 = (bf16[256,2048]{1,0:T(8,128)(2,1)S(1)}, bf16[256,2048]{1,0:T(8,128)(2,1)}, u32[]{:S(2)}, u32[]{:S(2)}) collective-permute-start(bf16[256,2048]{1,0:T(8,128)(2,1)S(1)} %fusion.2.refs_4_), channel_id=1, source_target_pairs={{0,2},{2,4},{4,6},{6,0},{1,3},{3,5},{5,7},{7,1},{8,10},{10,12},{12... | collective-permute-start | bytes 3145736 | tf_op jit(solution)/shard_map/ppermute | solution.py:24
  37.2 88.5 %copy-start.7 = (bf16[256,2048]{1,0:T(8,128)(2,1)}, bf16[256,2048]{1,0:T(8,128)(2,1)S(1)}, u32[]{:S(2)}) copy-start(bf16[256,2048]{1,0:T(8,128)(2,1)S(1)} %collective-permute-done.3.refs_2_) | copy-start | bytes 3145732
  37.2 88.4 %collective-permute-start.4 = (bf16[128,2048]{1,0:T(8,128)(2,1)S(1)}, bf16[128,2048]{1,0:T(8,128)(2,1)}, u32[]{:S(2)}, u32[]{:S(2)}) collective-permute-start(bf16[128,2048]{1,0:T(8,128)(2,1)S(1)} %slice.19), channel_id=1, source_target_pairs={{0,6},{2,0},{4,2},{6,4},{1,7},{3,1},{5,3},{7,5},{8,14},{10,8},{12,... | collective-permute-start | bytes 1572872 | tf_op jit(solution)/shard_map/ppermute | solution.py:24
  42.2 83.4 %collective-permute-start.2 = (bf16[128,2048]{1,0:T(8,128)(2,1)S(1)}, bf16[128,2048]{1,0:T(8,128)(2,1)}, u32[]{:S(2)}, u32[]{:S(2)}) collective-permute-start(bf16[128,2048]{1,0:T(8,128)(2,1)S(1)} %slice.18), channel_id=1, source_target_pairs={{0,2},{2,4},{4,6},{6,0},{1,3},{3,5},{5,7},{7,1},{8,10},{10,12},{12... | collective-permute-start | bytes 1572872 | tf_op jit(solution)/shard_map/ppermute | solution.py:24
  42.5 23.4 %collective-permute-start = (f32[4,256]{1,0:T(4,128)S(1)}, f32[4,256]{1,0:T(4,128)S(1)}, u32[]{:S(2)}, u32[]{:S(2)}) collective-permute-start(f32[4,256]{1,0:T(4,128)S(1)} %select_maximum_fusion), channel_id=1, source_target_pairs={{0,1},{1,0},{2,3},{3,2},{4,5},{5,4},{6,7},{7,6},{8,9},{9,8},{10,11... | collective-permute-start | bytes 12296 | tf_op jit(solution)/shard_map/ppermute | solution.py:296
  65.9 81.7 %copy-start.8 = (f32[2,4,256]{2,1,0:T(4,128)}, f32[2,4,256]{2,1,0:T(4,128)S(1)}, u32[]{:S(2)}) copy-start(f32[2,4,256]{2,1,0:T(4,128)S(1)} %maximum_select_fusion) | copy-start | bytes 24580
  147.6 11.4 %collective-permute-start.5 = (bf16[2,4,160,128]{3,2,1,0:T(8,128)(2,1)}, bf16[2,4,160,128]{3,2,1,0:T(8,128)(2,1)S(1)}, u32[]{:S(2)}, u32[]{:S(2)}) collective-permute-start(bf16[2,4,160,128]{3,2,1,0:T(8,128)(2,1)} %get-tuple-element.26), channel_id=1, source_target_pairs={{0,1},{1,8},{8,9},{9,16},{16,17},{17,24},{24,25},{25,32},{32,33},{... | collective-permute-start | bytes 983048 | tf_op jit(solution)/shard_map/ppermute | solution.py:328
  156.3 18.9 %collective-permute-start.12 = (bf16[128,2048]{1,0:T(8,128)(2,1)}, bf16[128,2048]{1,0:T(8,128)(2,1)S(1)}, u32[]{:S(2)}, u32[]{:S(2)}) collective-permute-start(bf16[128,2048]{1,0:T(8,128)(2,1)} %get-tuple-element.34), channel_id=1, source_target_pairs={{0,6},{2,0},{4,2},{6,4},{1,7},{3,1},{5,3},{7,5},{8,14},{10,8},{12,... | collective-permute-start | bytes 1572872 | tf_op jit(solution)/shard_map/ppermute | solution.py:24
  159.1 26.2 %collective-permute-start.7 = (bf16[128,2048]{1,0:T(8,128)(2,1)}, bf16[128,2048]{1,0:T(8,128)(2,1)S(1)}, u32[]{:S(2)}, u32[]{:S(2)}) collective-permute-start(bf16[128,2048]{1,0:T(8,128)(2,1)} %get-tuple-element.28), channel_id=1, source_target_pairs={{0,2},{2,4},{4,6},{6,0},{1,3},{3,5},{5,7},{7,1},{8,10},{10,12},{12... | collective-permute-start | bytes 1572872 | tf_op jit(solution)/shard_map/ppermute | solution.py:24
  159.1 0.8 copy-start.1
  165.9 13.6 %collective-permute-start.8 = (bf16[64,2048]{1,0:T(8,128)(2,1)}, bf16[64,2048]{1,0:T(8,128)(2,1)S(1)}, u32[]{:S(2)}, u32[]{:S(2)}) collective-permute-start(bf16[64,2048]{1,0:T(8,128)(2,1)} %get-tuple-element.30), channel_id=1, source_target_pairs={{0,2},{2,4},{4,6},{6,0},{1,3},{3,5},{5,7},{7,1},{8,10},{10,12},{12... | collective-permute-start | bytes 786440 | tf_op jit(solution)/shard_map/ppermute | solution.py:24
  166.2 18.9 %collective-permute-start.10 = (bf16[64,2048]{1,0:T(8,128)(2,1)}, bf16[64,2048]{1,0:T(8,128)(2,1)S(1)}, u32[]{:S(2)}, u32[]{:S(2)}) collective-permute-start(bf16[64,2048]{1,0:T(8,128)(2,1)} %get-tuple-element.32), channel_id=1, source_target_pairs={{0,2},{2,4},{4,6},{6,0},{1,3},{3,5},{5,7},{7,1},{8,10},{10,12},{12... | collective-permute-start | bytes 786440 | tf_op jit(solution)/shard_map/ppermute | solution.py:24
  167.2 18.1 %collective-permute-start.6 = (bf16[128,2048]{1,0:T(8,128)(2,1)}, bf16[128,2048]{1,0:T(8,128)(2,1)S(1)}, u32[]{:S(2)}, u32[]{:S(2)}) collective-permute-start(bf16[128,2048]{1,0:T(8,128)(2,1)} %get-tuple-element.27), channel_id=1, source_target_pairs={{0,6},{2,0},{4,2},{6,4},{1,7},{3,1},{5,3},{7,5},{8,14},{10,8},{12,... | collective-permute-start | bytes 1572872 | tf_op jit(solution)/shard_map/ppermute | solution.py:24
  175.2 9.9 %copy-start.6 = (bf16[64,2048]{1,0:T(8,128)(2,1)S(1)}, bf16[64,2048]{1,0:T(8,128)(2,1)}, u32[]{:S(2)}) copy-start(bf16[64,2048]{1,0:T(8,128)(2,1)} %get-tuple-element.31) | copy-start | bytes 786436
  176.5 19.5 %collective-permute-start.13 = (bf16[128,2048]{1,0:T(8,128)(2,1)S(1)}, bf16[128,2048]{1,0:T(8,128)(2,1)S(1)}, u32[]{:S(2)}, u32[]{:S(2)}) collective-permute-start(bf16[128,2048]{1,0:T(8,128)(2,1)S(1)} %add_convert_fusion.1), channel_id=1, source_target_pairs={{0,6},{2,0},{4,2},{6,4},{1,7},{3,1},{5,3},{7,5},{8,14},{10,8},{12,... | collective-permute-start | bytes 1572872 | tf_op jit(solution)/shard_map/ppermute | solution.py:24
  180.5 13.1 %collective-permute-start.9 = (bf16[64,2048]{1,0:T(8,128)(2,1)S(1)}, bf16[64,2048]{1,0:T(8,128)(2,1)S(1)}, u32[]{:S(2)}, u32[]{:S(2)}) collective-permute-start(bf16[64,2048]{1,0:T(8,128)(2,1)S(1)} %add_convert_fusion.3), channel_id=1, source_target_pairs={{0,2},{2,4},{4,6},{6,0},{1,3},{3,5},{5,7},{7,1},{8,10},{10,12},{12... | collective-permute-start | bytes 786440 | tf_op jit(solution)/shard_map/ppermute | solution.py:24
  185.2 10.9 %collective-permute-start.11 = (bf16[64,2048]{1,0:T(8,128)(2,1)S(1)}, bf16[64,2048]{1,0:T(8,128)(2,1)S(1)}, u32[]{:S(2)}, u32[]{:S(2)}) collective-permute-start(bf16[64,2048]{1,0:T(8,128)(2,1)S(1)} %add_convert_fusion.2), channel_id=1, source_target_pairs={{0,2},{2,4},{4,6},{6,0},{1,3},{3,5},{5,7},{7,1},{8,10},{10,12},{12... | collective-permute-start | bytes 786440 | tf_op jit(solution)/shard_map/ppermute | solution.py:24
  185.3 0.8 copy-start.4
  186.1 0.8 copy-start.5
Sparse Core Ops, SparseCore 0:
  22.2 103.4 all-gather.1

commit v3 on v2

--- a/solution.py
+++ b/solution.py
@@ -45,13 +45,14 @@
 
 
 def project_kernel(wide, weights, *refs):
-    opp_a, opp_b, succ, prev, own, out, edge, wout, xs, ws, wo, sems = refs
+    opp_a, opp_b, succ, prev, own, out, kvs, edge, wout, xs, ws, wkv, wo, sems = refs
     step = pl.program_id(0)
     half = opp_a.shape[0]
     block = weights.shape[2]
     blocks = weights.shape[0]
-    in_cols = ws.shape[3]
-    parts = (weights.shape[3] - in_cols) // block
+    main = ws.shape[3]
+    pair = wkv.shape[2] // 2
+    parts = (weights.shape[3] - main - pair) // block
     bf16, f32 = jnp.bfloat16, jnp.float32
     x_copies = [
         pltpu.make_async_copy(ref, xs.at[s, pl.ds(at, ref.shape[0]), :], sems.at[i])
@@ -59,75 +60,63 @@
             ((succ, 0, 0), (prev, 1, 0), (opp_a, 2, 0), (opp_b, 2, half), (own, 3, 0))
         )
     ]
-    cuts = ((0, 4 * block), (4 * block, in_cols - 4 * block))
-
-    def w_copy(t, k):
-        cols = pl.ds(*cuts[k])
-        return pltpu.make_async_copy(weights.at[:, t, :, cols], ws.at[t, :, :, cols], sems.at[5 + 2 * t + k])
-
-    def out_copies(t):
-        return [
-            pltpu.make_async_copy(
-                weights.at[j, t, :, pl.ds(in_cols + b * block, block)],
-                wo.at[pl.ds((t * parts + b) * block, block), pl.ds(j * block, block)],
-                sems.at[9 + (t * parts + b) * blocks + j],
-            )
-            for b in range(parts)
-            for j in range(blocks)
-        ]
-
+    w_copies = [
+        pltpu.make_async_copy(weights.at[:, t, :, pl.ds(0, main)], ws.at[t], sems.at[5 + t])
+        for t in range(2)
+    ]
+    kv_copies = [
+        pltpu.make_async_copy(
+            weights.at[:, t, :, pl.ds(main, pair)], wkv.at[:, :, pl.ds(t * pair, pair)], sems.at[7 + t]
+        )
+        for t in range(2)
+    ]
+    out_copies = [
+        pltpu.make_async_copy(
+            weights.at[j, t, :, pl.ds(main + pair + b * block, block)],
+            wo.at[pl.ds((t * parts + b) * block, block), pl.ds(j * block, block)],
+            sems.at[9 + (t * parts + b) * blocks + j],
+        )
+        for t in range(2)
+        for b in range(parts)
+        for j in range(blocks)
+    ]
     laid_out = pltpu.make_async_copy(wo, wout, sems.at[9 + 2 * parts * blocks])
 
     @pl.when(step == 0)
     def _():
-        for c in x_copies:
+        for c in x_copies + w_copies[:1]:
             c.start()
-        w_copy(0, 0).start()
-        w_copy(0, 1).start()
-        for c in x_copies:
+        for c in x_copies + w_copies[:1]:
             c.wait()
-        w_copy(0, 0).wait()
+        for c in w_copies[1:] + kv_copies + out_copies:
+            c.start()
 
     @pl.when(step == 1)
     def _():
-        w_copy(1, 0).wait()
-        w_copy(1, 1).wait()
-        for t in range(2):
-            for c in out_copies(t):
-                c.wait()
+        for c in w_copies[1:] + kv_copies + out_copies:
+            c.wait()
         laid_out.start()
 
     seqs, length, feats = xs.shape
     x = xs[...].reshape(seqs * length, feats)
-
-    def project(k):
-        cols = slice(cuts[k][0], cuts[k][0] + cuts[k][1])
-        w = ws[step, :, :, cols].reshape(feats, cuts[k][1])
-        product = jnp.dot(x, w, preferred_element_type=f32).astype(bf16)
-        out[0, :, :, cols] = product.reshape(seqs, length, cuts[k][1])
-
-    project(0)
-
-    @pl.when(step == 0)
-    def _():
-        w_copy(0, 1).wait()
-        w_copy(1, 0).start()
-        w_copy(1, 1).start()
-        for t in range(2):
-            for c in out_copies(t):
-                c.start()
-
-    project(1)
+    w = ws[step].reshape(feats, main)
+    rounded = jnp.dot(x, w, preferred_element_type=f32).astype(bf16).reshape(seqs, length, main)
+    out[0] = rounded
     chans = wide // 3
     for s in range(seqs):
-        edge[0, s, 0:WINDOW, :] = out[0, s, length - WINDOW :, wide + chans :]
-        last = out[0, s, length - 16 :, chans:wide].astype(f32)
+        last = rounded[s, length - 16 :, chans:wide].astype(f32)
         gated = (last[:, :chans] * last[:, chans:]).astype(bf16)
-        edge[0, s, WINDOW : WINDOW + 16, :] = gated[:, : 2 * HEAD]
-        edge[0, s, WINDOW + 16 : WINDOW + 32, :] = gated[:, 2 * HEAD :]
+        edge[step, s, WINDOW : WINDOW + 16, :] = gated[:, : 2 * HEAD]
+        edge[step, s, WINDOW + 16 : WINDOW + 32, :] = gated[:, 2 * HEAD :]
 
     @pl.when(step == 1)
     def _():
+        k = wkv[...].reshape(feats, 2 * pair)
+        both = jnp.dot(x, k, preferred_element_type=f32).astype(bf16).reshape(seqs, length, 2 * pair)
+        kvs[...] = both
+        for t in range(2):
+            for s in range(seqs):
+                edge[t, s, 0:WINDOW, :] = both[s, length - WINDOW :, t * pair : (t + 1) * pair]
         laid_out.wait()
 
 
@@ -135,16 +124,16 @@
     acts, wo, sem = refs[-3:]
     outs_at = len(refs) - 3 - len(pieces)
     results = refs[outs_at:-3]
-    first_edge = 2 if 0 in blocks else 0
-    projs, edges = refs[:2], refs[2 : 2 + first_edge]
-    arrived = refs[2 + first_edge : outs_at]
+    has_edge = 2 if 0 in blocks else 0
+    projs, kvs, edges = refs[:2], refs[2:4], refs[4 : 4 + has_edge]
+    arrived = refs[4 + has_edge : outs_at]
     wanted = pltpu.make_async_copy(wout, wo, sem)
     wanted.start()
     place = idx[0]
     chans = wide // 3
     heads = chans // HEAD
     f32, bf16 = jnp.float32, jnp.bfloat16
-    q_at, kv_at = wide, wide + chans
+    q_at = wide
     pair = 2 * HEAD
 
     def iota(shape, dim):
@@ -162,7 +151,7 @@
     transposed = (((1,), (1,)), ((), ()))
     for slot, n in enumerate(blocks):
         at, to = n * WINDOW, slot * WINDOW
-        proj, edge = projs[slot], edges[slot] if n == 0 else None
+        proj, kv_rows, edge = projs[slot], kvs[slot], edges[slot] if n == 0 else None
         for side in range(2):
 
             def gated_rows(start, rows):
@@ -187,11 +176,12 @@
             out_gate = proj[side, 0, at : at + WINDOW, 0:chans].astype(f32)
             acts[to : to + WINDOW, base : base + chans] = (out_gate * convolved).astype(bf16)
 
-            kv_here = proj[side, 0, at : at + WINDOW, kv_at : kv_at + pair]
+            kv_cols = slice(side * pair, (side + 1) * pair)
+            kv_here = kv_rows[0, at : at + WINDOW, kv_cols]
             if n == 0:
                 kv_before = edge[side, 0, 0:WINDOW, :]
             else:
-                kv_before = proj[side, 0, at - WINDOW : at, kv_at : kv_at + pair]
+                kv_before = kv_rows[0, at - WINDOW : at, kv_cols]
             kv = jnp.concatenate([kv_before, kv_here], axis=0)
             keys = lax.dot_general(pick_kt, kv, transposed, preferred_element_type=f32).astype(bf16)
             values = jnp.dot(kv, pick_v, preferred_element_type=f32).astype(bf16)
@@ -299,23 +289,27 @@
     weights, idx, taps, sinks = lax.optimization_barrier((weights, idx, taps, sinks))
 
     squares = out_cols // block
-    proj, edge, wout = pl.pallas_call(
+    pair = 2 * HEAD
+    proj, kvs, edge, wout = pl.pallas_call(
         functools.partial(project_kernel, b_width),
         out_shape=(
-            jax.ShapeDtypeStruct((tp, fs, here, in_cols), bf16),
+            jax.ShapeDtypeStruct((tp, fs, here, in_cols - pair), bf16),
+            jax.ShapeDtypeStruct((fs, here, tp * pair), bf16),
             jax.ShapeDtypeStruct((tp, fs, WINDOW + 32, 2 * HEAD), bf16),
             jax.ShapeDtypeStruct((tp * out_cols, feats), bf16),
         ),
         grid=(tp,),
         in_specs=[ANY] * 6,
         out_specs=(
-            pl.BlockSpec((1, fs, here, in_cols), lambda t: (t, 0, 0, 0)),
-            pl.BlockSpec((1, fs, WINDOW + 32, 2 * HEAD), lambda t: (t, 0, 0, 0)),
+            pl.BlockSpec((1, fs, here, in_cols - pair), lambda t: (t, 0, 0, 0)),
+            pl.BlockSpec((fs, here, tp * pair), lambda t: (0, 0, 0)),
+            pl.BlockSpec((tp, fs, WINDOW + 32, pair), lambda t: (0, 0, 0, 0)),
             ANY,
         ),
         scratch_shapes=[
             pltpu.VMEM((fs, here, feats), bf16),
-            pltpu.VMEM((tp, sp, block, in_cols), bf16),
+            pltpu.VMEM((tp, sp, block, in_cols - pair), bf16),
+            pltpu.VMEM((sp, block, tp * pair), bf16),
             pltpu.VMEM((tp * out_cols, feats), bf16),
             pltpu.SemaphoreType.DMA((10 + tp * squares * sp,)),
         ],
@@ -339,7 +333,8 @@
             out_shape=tuple(jax.ShapeDtypeStruct((n, feats), bf16) for n in pieces),
             grid=(1,),
             in_specs=[SMEM, SMEM, pl.BlockSpec((tp, TAPS, chans), lambda i: (0, 0, 0)), ANY]
-            + [part((here, in_cols), q) for q in seqs]
+            + [part((here, in_cols - pair), q) for q in seqs]
+            + [pl.BlockSpec((1, here, tp * pair), lambda i, q=q: (q, 0, 0)) for q in seqs]
             + [part((WINDOW + 32, 2 * HEAD), q) for q in (seqs if edged else ())]
             + [pl.BlockSpec(a.shape, lambda i: (0, 0)) for a in arrived],
             out_specs=tuple(pl.BlockSpec((n, feats), lambda i: (0, 0)) for n in pieces),
@@ -353,7 +348,7 @@
                 bytes_accessed=8_000_000,
                 transcendentals=600_000,
             ),
-        )(idx, sinks, taps, wout, proj, proj, *((edge, edge) if edged else ()), *arrived)
+        )(idx, sinks, taps, wout, proj, proj, kvs, kvs, *((edge, edge) if edged else ()), *arrived)
 
     def sent(array, by):
         return ring(array, "fs", by)

time: 206 us -> 201 us (0.976)
  Pallas kernels: 50.5 us -> 45.5 us
    pallas_call x1, Pallas kernels: 21.9 us -> 17.1 us  [layer(): pl.pallas_call(functools.partial(project_kernel, b_width), out_shape=(jax...]
where the time goes in v3:
time: 201 us
  waiting for transfers between devices  80.9 us (40%)
  Pallas kernels  45.5 us (23%)
  starting transfers between devices  38 us (19%)
  between operations  13.6 us (7%)
  blocking collectives  11.6 us (6%)
  other arithmetic  6.81 us (3%)
  local copies, waits for them, and re-layouts  4.11 us (2%)
    all_gather x1, waiting for transfers between devices, layer(): weights = lax.all_gather(mine, ('sp', 'tp'), axis=0, tiled=True)  59.2 us
    pallas_call x4, Pallas kernels, mix(): pl.pallas_call(functools.partial(mix_kernel, blocks, pieces, b_width), ou...  24.6 us
    ppermute x1, starting transfers between devices, layer(): theirs = lax.ppermute(small, 'tp', [(0, 1), (1, 0)])  22.6 us
    ppermute x12, waiting for transfers between devices, ring(): lax.ppermute(array, axis, [(i, (i + by) % size) for i in range(size)])  21.4 us
    pallas_call x1, Pallas kernels, layer(): pl.pallas_call(functools.partial(project_kernel, b_width), out_shape=(jax...  17.1 us
    ppermute x12, starting transfers between devices, ring(): lax.ppermute(array, axis, [(i, (i + by) % size) for i in range(size)])  12.8 us
    all_to_all x1, blocking collectives, layer(): mine = lax.all_to_all(packed, 'fs', split_axis=0, concat_axis=0, tiled=True)  11.6 us
  transfers between devices with their start and end apart: 15, of which 7 were waited for; matrix products, arithmetic and copies ran while one was open for 3% of the time, Pallas kernels for 12%

profile of v3, /device:TPU:33, one launch (start us, length us, event | category | flops | bytes accessed | tf_op | source)
XLA Modules:
  0.0 200.6 jit_solution(9477142280310545538)
XLA Ops:
  6.6 2.0 pack_weights.1
  8.5 11.6 %all_to_all.5 = bf16[4,32,1664]{2,1,0:T(8,128)(2,1)} all-to-all(bf16[4,32,1664]{2,1,0:T(8,128)(2,1)} %pack_weights.1), channel_id=1, replica_groups=mesh['grp'=2,'sp'=16,'fs'=4,'tp'=2] {'fs'}, dimensions={0} | all-to-all | bytes 851968 | tf_op jit(solution)/shard_map/all_to_all | solution.py:256
  20.1 1.9 turn_weights.1
  22.0 0.1 all-gather.2.cloned.1.call-update
  22.1 0.3 fusion
  22.4 0.3 fusion.2.refs_4_
  22.7 1.0 collective-permute-start.3
  23.7 0.6 collective-permute-start.1
  24.3 0.7 dynamic-slice_convert_fusion
  25.0 12.2 %collective-permute-done.3.refs_2_ = bf16[256,2048]{1,0:T(8,128)(2,1)S(1)} collective-permute-done((bf16[256,2048]{1,0:T(8,128)(2,1)S(1)}, bf16[256,2048]{1,0:T(8,128)(2,1)S(1)}, u32[]{:S(2)}, u32[]{:S(2)}) %collective-permute-start.3) | collective-permute-done | bytes 1048608 | tf_op jit(solution)/shard_map/ppermute | solution.py:24
  37.3 3.6 %collective-permute-start.4 = (bf16[128,2048]{1,0:T(8,128)(2,1)S(1)}, bf16[128,2048]{1,0:T(8,128)(2,1)}, u32[]{:S(2)}, u32[]{:S(2)}) collective-permute-start(bf16[128,2048]{1,0:T(8,128)(2,1)S(1)} %slice.19), channel_id=1, source_target_pairs={{0,6},{2,0},{4,2},{6,4},{1,7},{3,1},{5,3},{7,5},{8,14},{10,8},{12,... | collective-permute-start | bytes 1572872 | tf_op jit(solution)/shard_map/ppermute | solution.py:24
  40.8 0.3 collective-permute-done.1.refs_3_
  41.2 1.1 slice.18
  42.2 0.1 collective-permute-start.2
  42.4 0.1 dynamic-slice_bitcast_fusion
  42.5 22.6 %collective-permute-start = (f32[4,256]{1,0:T(4,128)S(1)}, f32[4,256]{1,0:T(4,128)S(1)}, u32[]{:S(2)}, u32[]{:S(2)}) collective-permute-start(f32[4,256]{1,0:T(4,128)S(1)} %select_maximum_fusion), channel_id=1, source_target_pairs={{0,1},{1,0},{2,3},{3,2},{4,5},{5,4},{6,7},{7,6},{8,9},{9,8},{10,11... | collective-permute-start | bytes 12296 | tf_op jit(solution)/shard_map/ppermute | solution.py:286
  65.1 0.6 pad_add_fusion.idx
  65.6 0.3 collective-permute-done
  65.9 0.5 slice.17
  66.4 59.2 %all-gather.2.cloned.1.call-done = bf16[4096,1664]{1,0:T(8,128)(2,1)} async-done(((bf16[128,1664]{1,0:T(8,128)(2,1)}), bf16[4096,1664]{1,0:T(8,128)(2,1)}) %all-gather.2.cloned.1.call-update) | async-done | bytes 13631504 | tf_op jit(solution)/shard_map/all_gather | solution.py:264
  125.6 0.0 collective-permute-done.4.refs_1_
  125.7 0.0 collective-permute-done.2.refs_0_
  125.7 17.1 %project_rows.1 = (bf16[2,4,256,1024]{3,2,1,0:T(8,128)(2,1)}, bf16[4,256,256]{2,1,0:T(8,128)(2,1)}, bf16[2,4,160,128]{3,2,1,0:T(8,128)(2,1)}, bf16[1024,2048]{1,0:T(8,128)(2,1)}) custom-call(bf16[16,2,128,1664]{3,2,1,0:T(8,128)(2,1)} %bitcast.31, bf16[128,2048]{1,0:T(8,128)(2,1)} %collective-permute-done.2.refs_0_, ...), custom_call_target="tpu_custom_call" | custom-call | flops 9663676416 | bytes 25000000 | tf_op jit(solution)/shard_map/project_rows/pallas_call | solution.py:293
  142.8 2.6 %collective-permute-start.5 = (bf16[2,4,160,128]{3,2,1,0:T(8,128)(2,1)}, bf16[2,4,160,128]{3,2,1,0:T(8,128)(2,1)S(1)}, u32[]{:S(2)}, u32[]{:S(2)}) collective-permute-start(bf16[2,4,160,128]{3,2,1,0:T(8,128)(2,1)} %get-tuple-element.28), channel_id=1, source_target_pairs={{0,1},{1,8},{8,9},{9,16},{16,17},{17,24},{24,25},{25,32},{32,33},{... | collective-permute-start | bytes 983048 | tf_op jit(solution)/shard_map/ppermute | solution.py:322
  145.4 6.0 %shard_map.119 = (bf16[128,2048]{1,0:T(8,128)(2,1)}, bf16[128,2048]{1,0:T(8,128)(2,1)}) custom-call(s32[2]{0:T(128)} %pad_add_fusion.idx, f32[2,4]{1,0:T(2,128)} %bitcast.26, f32[2,3,256]{2,1,0:T(4,128)} %bitcast.20, bf16[1024,2048]{1,0:T(8,128)(2,1)} %get-tuple-element.25.wout, bf16[2,4,256,1024]{3,2,1,0:T(8,128)(2,1)} %get-tuple-element.26.refs_0_.refs_1_, ...), custom_call_target="tpu_custom_call" | custom-call | flops 1673741824 | bytes 8000000 | tf_op jit(solution)/shard_map/pallas_call | solution.py:331
  151.5 2.7 %collective-permute-start.12 = (bf16[128,2048]{1,0:T(8,128)(2,1)}, bf16[128,2048]{1,0:T(8,128)(2,1)S(1)}, u32[]{:S(2)}, u32[]{:S(2)}) collective-permute-start(bf16[128,2048]{1,0:T(8,128)(2,1)} %get-tuple-element.36), channel_id=1, source_target_pairs={{0,6},{2,0},{4,2},{6,4},{1,7},{3,1},{5,3},{7,5},{8,14},{10,8},{12,... | collective-permute-start | bytes 1572872 | tf_op jit(solution)/shard_map/ppermute | solution.py:24
  154.2 0.0 collective-permute-start.7
  154.2 0.0 collective-permute-done.5.refs_4_.refs_5_
  154.2 0.7 copy-done.1
  154.9 6.0 %shard_map.118 = (bf16[64,2048]{1,0:T(8,128)(2,1)}, bf16[64,2048]{1,0:T(8,128)(2,1)}, bf16[128,2048]{1,0:T(8,128)(2,1)}) custom-call(s32[2]{0:T(128)} %pad_add_fusion.idx, f32[2,4]{1,0:T(2,128)} %bitcast.27, f32[2,3,256]{2,1,0:T(4,128)} %bitcast.21, bf16[1024,2048]{1,0:T(8,128)(2,1)} %get-tuple-element.25.wout, ...), custom_call_target="tpu_custom_call" | custom-call | flops 1673741824 | bytes 8000000 | tf_op jit(solution)/shard_map/pallas_call | solution.py:331
  160.9 0.3 collective-permute-start.8
  161.3 1.0 collective-permute-start.10
  162.3 1.9 collective-permute-start.6
  164.2 6.1 %shard_map.121 = (bf16[64,2048]{1,0:T(8,128)(2,1)}, bf16[64,2048]{1,0:T(8,128)(2,1)}, bf16[128,2048]{1,0:T(8,128)(2,1)}) custom-call(s32[2]{0:T(128)} %pad_add_fusion.idx, f32[2,4]{1,0:T(2,128)} %bitcast.28, f32[2,3,256]{2,1,0:T(4,128)} %bitcast.22, bf16[1024,2048]{1,0:T(8,128)(2,1)} %get-tuple-element.25.wout, ...), custom_call_target="tpu_custom_call" | custom-call | flops 1673741824 | bytes 8000000 | tf_op jit(solution)/shard_map/pallas_call | solution.py:331
  170.3 0.0 collective-permute-done.12
  170.3 1.3 add_convert_fusion.1
  171.6 1.2 collective-permute-start.13
  172.8 1.8 collective-permute-done.8
  174.6 1.0 add_convert_fusion.3
  175.6 0.1 collective-permute-start.9
  175.8 4.4 %collective-permute-done.10 = bf16[64,2048]{1,0:T(8,128)(2,1)S(1)} collective-permute-done((bf16[64,2048]{1,0:T(8,128)(2,1)}, bf16[64,2048]{1,0:T(8,128)(2,1)S(1)}, u32[]{:S(2)}, u32[]{:S(2)}) %collective-permute-start.10) | collective-permute-done | bytes 262176 | tf_op jit(solution)/shard_map/ppermute | solution.py:24
  180.2 0.1 add_convert_fusion.2
  180.3 0.1 collective-permute-start.11
  180.4 0.8 copy-done.4
  181.3 0.8 copy-done.5
  182.1 6.5 %shard_map.120 = bf16[256,2048]{1,0:T(8,128)(2,1)} custom-call(s32[2]{0:T(128)} %pad_add_fusion.idx, f32[2,4]{1,0:T(2,128)} %bitcast.29, f32[2,3,256]{2,1,0:T(4,128)} %bitcast.23, bf16[1024,2048]{1,0:T(8,128)(2,1)} %get-tuple-element.25.wout, bf16[2,4,256,1024]{3,2,1,0:T(8,128)(2,1)} %get-tuple-element.26.refs_0_.refs_1_, ...), custom_call_target="tpu_custom_call" | custom-call | flops 1673741824 | bytes 8000000 | tf_op jit(solution)/shard_map/pallas_call | solution.py:331
  188.6 2.6 %collective-permute-done.11 = bf16[64,2048]{1,0:T(8,128)(2,1)S(1)} collective-permute-done((bf16[64,2048]{1,0:T(8,128)(2,1)S(1)}, bf16[64,2048]{1,0:T(8,128)(2,1)S(1)}, u32[]{:S(2)}, u32[]{:S(2)}) %collective-permute-start.11) | collective-permute-done | bytes 262176 | tf_op jit(solution)/shard_map/ppermute | solution.py:24
  191.1 2.6 %fusion.3 = bf16[1,256,2048]{2,1,0:T(8,128)(2,1)} fusion(bf16[256,2048]{1,0:T(8,128)(2,1)} %shard_map.120, bf16[128,2048]{1,0:T(8,128)(2,1)S(1)} %collective-permute-done.13, bf16[64,2048]{1,0:T(8,128)(2,1)S(1)} %collective-permute-done.11, bf16[64,2048]{1,0:T(8,128)(2,1)S(1)} %collective-permute-done.9), kind=kLoop, calls=%fused_computation.6 | loop fusion | flops 4718592 | bytes 3145728 | tf_op jit(solution)/shard_map/broadcast_in_dim | solution.py:367
  (27 shorter events, 0.1 us)
Async XLA Ops:
  6.5 35.8 %copy-start = (f32[16]{0:T(128)S(1)}, f32[16]{0:T(128)}, u32[]{:S(2)}) copy-start(f32[16]{0:T(128)} %param.21) | copy-start | bytes 196
  6.6 15.5 %copy-start.2 = (bf16[1,256,2048]{2,1,0:T(8,128)(2,1)S(1)}, bf16[1,256,2048]{2,1,0:T(8,128)(2,1)}, u32[]{:S(2)}) copy-start(bf16[1,256,2048]{2,1,0:T(8,128)(2,1)} %param.12) | copy-start | bytes 3145732
  6.6 15.8 %copy-start.9 = (f32[2048]{0:T(1024)S(1)}, f32[2048]{0:T(1024)}, u32[]{:S(2)}) copy-start(f32[2048]{0:T(1024)} %param.13) | copy-start | bytes 24580
  6.6 119.1 %all-gather.2.cloned.1.call-start = ((), (), s32[]{:S(2)}) async-start(), calls=%async_computation.1 | async-start | bytes 14057472 | tf_op jit(solution)/shard_map/all_gather | solution.py:264
  22.7 103.0 %copy-start.3 = (bf16[256,2048]{1,0:T(8,128)(2,1)}, bf16[256,2048]{1,0:T(8,128)(2,1)S(1)}, u32[]{:S(2)}) copy-start(bf16[256,2048]{1,0:T(8,128)(2,1)S(1)} %fusion.2.refs_4_) | copy-start | bytes 3145732
  22.7 14.5 %collective-permute-start.3 = (bf16[256,2048]{1,0:T(8,128)(2,1)S(1)}, bf16[256,2048]{1,0:T(8,128)(2,1)S(1)}, u32[]{:S(2)}, u32[]{:S(2)}) collective-permute-start(bf16[256,2048]{1,0:T(8,128)(2,1)S(1)} %fusion.2.refs_4_), channel_id=1, source_target_pairs={{0,6},{2,0},{4,2},{6,4},{1,7},{3,1},{5,3},{7,5},{8,14},{10,8},{12,... | collective-permute-start | bytes 3145736 | tf_op jit(solution)/shard_map/ppermute | solution.py:24
  23.7 17.5 %collective-permute-start.1 = (bf16[256,2048]{1,0:T(8,128)(2,1)S(1)}, bf16[256,2048]{1,0:T(8,128)(2,1)}, u32[]{:S(2)}, u32[]{:S(2)}) collective-permute-start(bf16[256,2048]{1,0:T(8,128)(2,1)S(1)} %fusion.2.refs_4_), channel_id=1, source_target_pairs={{0,2},{2,4},{4,6},{6,0},{1,3},{3,5},{5,7},{7,1},{8,10},{10,12},{12... | collective-permute-start | bytes 3145736 | tf_op jit(solution)/shard_map/ppermute | solution.py:24
  37.2 88.5 %copy-start.7 = (bf16[256,2048]{1,0:T(8,128)(2,1)}, bf16[256,2048]{1,0:T(8,128)(2,1)S(1)}, u32[]{:S(2)}) copy-start(bf16[256,2048]{1,0:T(8,128)(2,1)S(1)} %collective-permute-done.3.refs_2_) | copy-start | bytes 3145732
  37.3 88.4 %collective-permute-start.4 = (bf16[128,2048]{1,0:T(8,128)(2,1)S(1)}, bf16[128,2048]{1,0:T(8,128)(2,1)}, u32[]{:S(2)}, u32[]{:S(2)}) collective-permute-start(bf16[128,2048]{1,0:T(8,128)(2,1)S(1)} %slice.19), channel_id=1, source_target_pairs={{0,6},{2,0},{4,2},{6,4},{1,7},{3,1},{5,3},{7,5},{8,14},{10,8},{12,... | collective-permute-start | bytes 1572872 | tf_op jit(solution)/shard_map/ppermute | solution.py:24
  42.2 83.4 %collective-permute-start.2 = (bf16[128,2048]{1,0:T(8,128)(2,1)S(1)}, bf16[128,2048]{1,0:T(8,128)(2,1)}, u32[]{:S(2)}, u32[]{:S(2)}) collective-permute-start(bf16[128,2048]{1,0:T(8,128)(2,1)S(1)} %slice.18), channel_id=1, source_target_pairs={{0,2},{2,4},{4,6},{6,0},{1,3},{3,5},{5,7},{7,1},{8,10},{10,12},{12... | collective-permute-start | bytes 1572872 | tf_op jit(solution)/shard_map/ppermute | solution.py:24
  42.5 23.4 %collective-permute-start = (f32[4,256]{1,0:T(4,128)S(1)}, f32[4,256]{1,0:T(4,128)S(1)}, u32[]{:S(2)}, u32[]{:S(2)}) collective-permute-start(f32[4,256]{1,0:T(4,128)S(1)} %select_maximum_fusion), channel_id=1, source_target_pairs={{0,1},{1,0},{2,3},{3,2},{4,5},{5,4},{6,7},{7,6},{8,9},{9,8},{10,11... | collective-permute-start | bytes 12296 | tf_op jit(solution)/shard_map/ppermute | solution.py:286
  65.9 76.9 %copy-start.8 = (f32[2,4,256]{2,1,0:T(4,128)}, f32[2,4,256]{2,1,0:T(4,128)S(1)}, u32[]{:S(2)}) copy-start(f32[2,4,256]{2,1,0:T(4,128)S(1)} %maximum_select_fusion) | copy-start | bytes 24580
  142.8 11.4 %collective-permute-start.5 = (bf16[2,4,160,128]{3,2,1,0:T(8,128)(2,1)}, bf16[2,4,160,128]{3,2,1,0:T(8,128)(2,1)S(1)}, u32[]{:S(2)}, u32[]{:S(2)}) collective-permute-start(bf16[2,4,160,128]{3,2,1,0:T(8,128)(2,1)} %get-tuple-element.28), channel_id=1, source_target_pairs={{0,1},{1,8},{8,9},{9,16},{16,17},{17,24},{24,25},{25,32},{32,33},{... | collective-permute-start | bytes 983048 | tf_op jit(solution)/shard_map/ppermute | solution.py:322
  151.5 18.9 %collective-permute-start.12 = (bf16[128,2048]{1,0:T(8,128)(2,1)}, bf16[128,2048]{1,0:T(8,128)(2,1)S(1)}, u32[]{:S(2)}, u32[]{:S(2)}) collective-permute-start(bf16[128,2048]{1,0:T(8,128)(2,1)} %get-tuple-element.36), channel_id=1, source_target_pairs={{0,6},{2,0},{4,2},{6,4},{1,7},{3,1},{5,3},{7,5},{8,14},{10,8},{12,... | collective-permute-start | bytes 1572872 | tf_op jit(solution)/shard_map/ppermute | solution.py:24
  154.2 26.2 %collective-permute-start.7 = (bf16[128,2048]{1,0:T(8,128)(2,1)}, bf16[128,2048]{1,0:T(8,128)(2,1)S(1)}, u32[]{:S(2)}, u32[]{:S(2)}) collective-permute-start(bf16[128,2048]{1,0:T(8,128)(2,1)} %get-tuple-element.30), channel_id=1, source_target_pairs={{0,2},{2,4},{4,6},{6,0},{1,3},{3,5},{5,7},{7,1},{8,10},{10,12},{12... | collective-permute-start | bytes 1572872 | tf_op jit(solution)/shard_map/ppermute | solution.py:24
  154.2 0.7 copy-start.1
  160.9 13.6 %collective-permute-start.8 = (bf16[64,2048]{1,0:T(8,128)(2,1)}, bf16[64,2048]{1,0:T(8,128)(2,1)S(1)}, u32[]{:S(2)}, u32[]{:S(2)}) collective-permute-start(bf16[64,2048]{1,0:T(8,128)(2,1)} %get-tuple-element.32), channel_id=1, source_target_pairs={{0,2},{2,4},{4,6},{6,0},{1,3},{3,5},{5,7},{7,1},{8,10},{10,12},{12... | collective-permute-start | bytes 786440 | tf_op jit(solution)/shard_map/ppermute | solution.py:24
  161.3 18.9 %collective-permute-start.10 = (bf16[64,2048]{1,0:T(8,128)(2,1)}, bf16[64,2048]{1,0:T(8,128)(2,1)S(1)}, u32[]{:S(2)}, u32[]{:S(2)}) collective-permute-start(bf16[64,2048]{1,0:T(8,128)(2,1)} %get-tuple-element.34), channel_id=1, source_target_pairs={{0,2},{2,4},{4,6},{6,0},{1,3},{3,5},{5,7},{7,1},{8,10},{10,12},{12... | collective-permute-start | bytes 786440 | tf_op jit(solution)/shard_map/ppermute | solution.py:24
  162.3 18.1 %collective-permute-start.6 = (bf16[128,2048]{1,0:T(8,128)(2,1)}, bf16[128,2048]{1,0:T(8,128)(2,1)S(1)}, u32[]{:S(2)}, u32[]{:S(2)}) collective-permute-start(bf16[128,2048]{1,0:T(8,128)(2,1)} %get-tuple-element.29), channel_id=1, source_target_pairs={{0,6},{2,0},{4,2},{6,4},{1,7},{3,1},{5,3},{7,5},{8,14},{10,8},{12,... | collective-permute-start | bytes 1572872 | tf_op jit(solution)/shard_map/ppermute | solution.py:24
  170.3 9.9 %copy-start.6 = (bf16[64,2048]{1,0:T(8,128)(2,1)S(1)}, bf16[64,2048]{1,0:T(8,128)(2,1)}, u32[]{:S(2)}) copy-start(bf16[64,2048]{1,0:T(8,128)(2,1)} %get-tuple-element.33) | copy-start | bytes 786436
  171.6 19.6 %collective-permute-start.13 = (bf16[128,2048]{1,0:T(8,128)(2,1)S(1)}, bf16[128,2048]{1,0:T(8,128)(2,1)S(1)}, u32[]{:S(2)}, u32[]{:S(2)}) collective-permute-start(bf16[128,2048]{1,0:T(8,128)(2,1)S(1)} %add_convert_fusion.1), channel_id=1, source_target_pairs={{0,6},{2,0},{4,2},{6,4},{1,7},{3,1},{5,3},{7,5},{8,14},{10,8},{12,... | collective-permute-start | bytes 1572872 | tf_op jit(solution)/shard_map/ppermute | solution.py:24
  175.6 13.0 %collective-permute-start.9 = (bf16[64,2048]{1,0:T(8,128)(2,1)S(1)}, bf16[64,2048]{1,0:T(8,128)(2,1)S(1)}, u32[]{:S(2)}, u32[]{:S(2)}) collective-permute-start(bf16[64,2048]{1,0:T(8,128)(2,1)S(1)} %add_convert_fusion.3), channel_id=1, source_target_pairs={{0,2},{2,4},{4,6},{6,0},{1,3},{3,5},{5,7},{7,1},{8,10},{10,12},{12... | collective-permute-start | bytes 786440 | tf_op jit(solution)/shard_map/ppermute | solution.py:24
  180.3 10.9 %collective-permute-start.11 = (bf16[64,2048]{1,0:T(8,128)(2,1)S(1)}, bf16[64,2048]{1,0:T(8,128)(2,1)S(1)}, u32[]{:S(2)}, u32[]{:S(2)}) collective-permute-start(bf16[64,2048]{1,0:T(8,128)(2,1)S(1)} %add_convert_fusion.2), channel_id=1, source_target_pairs={{0,2},{2,4},{4,6},{6,0},{1,3},{3,5},{5,7},{7,1},{8,10},{10,12},{12... | collective-permute-start | bytes 786440 | tf_op jit(solution)/shard_map/ppermute | solution.py:24
  180.4 0.8 copy-start.4
  181.2 0.8 copy-start.5
Sparse Core Ops, SparseCore 0:
  22.2 103.4 all-gather.1

commit v4 on v3

--- a/solution.py
+++ b/solution.py
@@ -12,6 +12,7 @@
 WINDOW = 128
 TAPS = 3
 EPSILON = 1e-06
+LOG2_E = 1.4426950408889634
 
 
 ANY = pl.BlockSpec(memory_space=pl.ANY)
@@ -24,24 +25,33 @@
     return lax.ppermute(array, axis, [(i, (i + by) % size) for i in range(size)])
 
 
-def pack_kernel(wq, wk, wv, conv_t, attn_t, wb, wc, wi, out):
-    fs = out.shape[0]
+def pack_kernel(group, wq, wk, wv, conv_t, attn_t, wb, wc, wi, *outs):
+    fs = len(outs)
     chans = wq.shape[1] // fs
-    for f in range(fs):
-        cut = slice(f * chans, (f + 1) * chans)
-        head = (f * wk.shape[1]) // (fs * HEAD) * HEAD
-        kv = jnp.concatenate([wk[:, head : head + HEAD], wv[:, head : head + HEAD]], axis=1)
+    for d, out in enumerate(outs):
+        to = lax.rem(group[0] + d, fs)
+        cut = pl.ds(pl.multiple_of(to * chans, chans), chans)
+        second = to >= fs // 2
+        kv = jnp.concatenate(
+            [jnp.where(second, w[:, HEAD : 2 * HEAD], w[:, :HEAD]) for w in (wk, wv)], axis=1
+        )
         at = 0
         for part in (wb[:, cut], wc[:, cut], wi[:, cut], wq[:, cut], kv, conv_t[:, cut], attn_t[:, cut]):
-            out[f, :, at : at + part.shape[1]] = part
+            out[:, at : at + part.shape[1]] = part
             at += part.shape[1]
 
 
-def turn_kernel(in_cols, mine, out):
+def turn_kernel(in_cols, group, *refs):
+    parts, out, squares = refs[:-2], refs[-2], refs[-1]
     block, width = out.shape
-    out[:, :in_cols] = mine[:, :in_cols]
-    for at in range(in_cols, width, block):
-        out[:, at : at + block] = mine[:, at : at + block].T
+    rows = parts[0].shape[0]
+    for d, part in enumerate(parts):
+        source = lax.rem(group[0] - d + len(parts), len(parts))
+        at = pl.ds(pl.multiple_of(source * rows, rows), rows)
+        out[at, :in_cols] = part[:, :in_cols]
+        squares[at, :] = part[:, in_cols:]
+    for at in range(0, width - in_cols, block):
+        out[:, in_cols + at : in_cols + at + block] = squares[:, at : at + block].T
 
 
 def project_kernel(wide, weights, *refs):
@@ -192,12 +202,12 @@
             for h in range(heads):
                 qh = jnp.where((lane >= h * HEAD) & (lane < (h + 1) * HEAD), q, jnp.zeros_like(q))
                 sc = jnp.dot(qh, keys, preferred_element_type=f32)
-                sc = jnp.where(allowed, sc * (1.0 / 8.0), -jnp.inf)
-                sink = sinks[side, h]
+                sc = jnp.where(allowed, sc * (LOG2_E / 8.0), -jnp.inf)
+                sink = sinks[side, h] * LOG2_E
                 m = jnp.maximum(jnp.max(sc, axis=1, keepdims=True), sink)
-                e = jnp.exp(sc - m).astype(bf16)
+                e = jnp.exp2(sc - m).astype(bf16)
                 o = jnp.dot(e, values, preferred_element_type=f32)
-                outs.append(o[:, :pair] / (o[:, pair:] + jnp.exp(sink - m)))
+                outs.append(o[:, :pair] / (o[:, pair:] + jnp.exp2(sink - m)))
             for j in range(heads // 2):
                 col = base + chans + j * pair
                 acts[to : to + WINDOW, col : col + pair] = jnp.where(
@@ -246,27 +256,28 @@
     b_width, out_cols = 3 * chans, 2 * chans
     in_cols = b_width + chans + 2 * HEAD
     width = in_cols + out_cols
+    core, place, group = lax.axis_index("tp"), lax.axis_index("sp"), lax.axis_index("fs")
+    idx = (place * tp + core).astype(jnp.int32).reshape(1)
+    member = group.astype(jnp.int32).reshape(1)
     packed = pl.pallas_call(
         pack_kernel,
-        out_shape=jax.ShapeDtypeStruct((fs, rows_in, width), bf16),
-        in_specs=[VMEM] * 8,
-        out_specs=VMEM,
+        out_shape=(jax.ShapeDtypeStruct((rows_in, width), bf16),) * fs,
+        in_specs=[SMEM] + [VMEM] * 8,
+        out_specs=(VMEM,) * fs,
         name="pack_weights",
-    )(w_query, w_key, w_value, conv_out_weight.T, attn_out_weight.T, w_bgate, w_cgate, w_conv_in)
-    mine = lax.all_to_all(packed, "fs", split_axis=0, concat_axis=0, tiled=True)
+    )(member, w_query, w_key, w_value, conv_out_weight.T, attn_out_weight.T, w_bgate, w_cgate, w_conv_in)
     mine = pl.pallas_call(
         functools.partial(turn_kernel, in_cols),
         out_shape=jax.ShapeDtypeStruct((block, width), bf16),
-        in_specs=[VMEM],
+        in_specs=[SMEM] + [VMEM] * fs,
         out_specs=VMEM,
+        scratch_shapes=[pltpu.VMEM((block, out_cols), bf16)],
         name="turn_weights",
-    )(mine.reshape(block, width))
+    )(member, packed[0], *(ring(p, "fs", d) for d, p in enumerate(packed) if d > 0))
     weights = lax.all_gather(mine, ("sp", "tp"), axis=0, tiled=True)
     weights = weights.reshape(sp, tp, block, width)
 
-    core, place, group = lax.axis_index("tp"), lax.axis_index("sp"), lax.axis_index("fs")
     heads = chans // HEAD
-    idx = jnp.stack([place * tp + core, place]).astype(jnp.int32)
     taps = lax.dynamic_slice_in_dim(conv_taps, group * chans, chans, 1).astype(f32)
     sinks = lax.dynamic_slice_in_dim(sink_logits, group * heads, heads, 0)
     small = jnp.concatenate([taps, jnp.pad(sinks[None], ((0, 0), (0, chans - heads)))], axis=0)

time: 201 us -> 200 us (level)
  blocking collectives: 11.6 us -> 0 us
  starting transfers between devices: 38 us -> 43.4 us
  waiting for transfers between devices: 80.9 us -> 83.6 us
  Pallas kernels: 45.5 us -> 48 us
    all_to_all x1 -> x0, blocking collectives: 11.6 us -> none  [layer(): mine = lax.all_to_all(packed, 'fs', split_axis=0, concat_axis=0, tiled=True)]
    ppermute x12 -> x15, starting transfers between devices: 12.8 us -> 18.1 us  [ring(): lax.ppermute(array, axis, [(i, (i + by) % size) for i in range(size)])]
    ppermute x12 -> x15, waiting for transfers between devices: 21.4 us -> 24.4 us  [ring(): lax.ppermute(array, axis, [(i, (i + by) % size) for i in range(size)])]
    pallas_call x4, Pallas kernels: 24.6 us -> 27 us  [mix(): pl.pallas_call(functools.partial(mix_kernel, blocks, pieces, b_width), ou...]
  transfers between devices with their start and end apart: 15 -> 18, of which waited for: 7 -> 8; matrix products, arithmetic and copies ran while one was open for 3% -> 3% of each run, Pallas kernels for 12% -> 14%
where the time goes in v4:
time: 200 us
  waiting for transfers between devices  83.6 us (42%)
  Pallas kernels  48 us (24%)
  starting transfers between devices  43.4 us (22%)
  between operations  13.7 us (7%)
  other arithmetic  6.19 us (3%)
  local copies, waits for them, and re-layouts  4.71 us (2%)
    all_gather x1, waiting for transfers between devices, layer(): weights = lax.all_gather(mine, ('sp', 'tp'), axis=0, tiled=True)  58.4 us
    pallas_call x4, Pallas kernels, mix(): pl.pallas_call(functools.partial(mix_kernel, blocks, pieces, b_width), ou...  27 us
    ppermute x15, waiting for transfers between devices, ring(): lax.ppermute(array, axis, [(i, (i + by) % size) for i in range(size)])  24.4 us
    ppermute x1, starting transfers between devices, layer(): theirs = lax.ppermute(small, 'tp', [(0, 1), (1, 0)])  22.6 us
    ppermute x15, starting transfers between devices, ring(): lax.ppermute(array, axis, [(i, (i + by) % size) for i in range(size)])  18.1 us
    pallas_call x1, Pallas kernels, layer(): pl.pallas_call(functools.partial(project_kernel, b_width), out_shape=(jax...  17 us
  transfers between devices with their start and end apart: 18, of which 8 were waited for; matrix products, arithmetic and copies ran while one was open for 3% of the time, Pallas kernels for 14%

profile of v4, /device:TPU:33, one launch (start us, length us, event | category | flops | bytes accessed | tf_op | source)
XLA Modules:
  0.0 199.5 jit_solution(102139979976154723)
XLA Ops:
  6.6 2.0 %pack_weights.1 = (bf16[32,1664]{1,0:T(8,128)(2,1)}, bf16[32,1664]{1,0:T(8,128)(2,1)}, bf16[32,1664]{1,0:T(8,128)(2,1)}, bf16[32,1664]{1,0:T(8,128)(2,1)}) custom-call(s32[1]{0:T(128)} %bitcast.group, bf16[32,1024]{1,0:T(8,128)(2,1)} %wq.1, bf16[32,128]{1,0:T(8,128)(2,1)} %wk.1, bf16[32,128]{1,0:T(8,128)(2,1)} %wv.1, bf16[32,1024]{1,0:T(8,128)(2,1)} %bitcast.22, ...), custom_call_target="tpu_custom_call" | custom-call | tf_op jit(solution)/shard_map/pack_weights/pallas_call | solution.py:262
  8.6 2.2 %collective-permute-start = (bf16[32,1664]{1,0:T(8,128)(2,1)}, bf16[32,1664]{1,0:T(8,128)(2,1)S(1)}, u32[]{:S(2)}, u32[]{:S(2)}) collective-permute-start(bf16[32,1664]{1,0:T(8,128)(2,1)} %get-tuple-element.26), channel_id=1, source_target_pairs={{0,2},{2,4},{4,6},{6,0},{1,3},{3,5},{5,7},{7,1},{8,10},{10,12},{12... | collective-permute-start | bytes 319496 | tf_op jit(solution)/shard_map/ppermute | solution.py:25
  10.7 2.7 %collective-permute-start.1 = (bf16[32,1664]{1,0:T(8,128)(2,1)}, bf16[32,1664]{1,0:T(8,128)(2,1)S(1)}, u32[]{:S(2)}, u32[]{:S(2)}) collective-permute-start(bf16[32,1664]{1,0:T(8,128)(2,1)} %get-tuple-element.27), channel_id=1, source_target_pairs={{0,4},{2,6},{4,0},{6,2},{1,5},{3,7},{5,1},{7,3},{8,12},{10,14},{12... | collective-permute-start | bytes 319496 | tf_op jit(solution)/shard_map/ppermute | solution.py:25
  13.5 1.0 collective-permute-start.2
  14.5 0.1 collective-permute-done.refs_1_
  14.6 3.5 %collective-permute-done.1.refs_2_ = bf16[32,1664]{1,0:T(8,128)(2,1)S(1)} collective-permute-done((bf16[32,1664]{1,0:T(8,128)(2,1)}, bf16[32,1664]{1,0:T(8,128)(2,1)S(1)}, u32[]{:S(2)}, u32[]{:S(2)}) %collective-permute-start.1) | collective-permute-done | bytes 106528 | tf_op jit(solution)/shard_map/ppermute | solution.py:25
  18.1 0.6 copy-done.10
  18.7 0.0 copy-done.11
  18.7 1.9 turn_weights.1
  20.7 0.1 all-gather.2.cloned.1.call-update
  20.7 0.3 fusion
  21.1 0.3 fusion.2.refs_4_
  21.4 1.5 collective-permute-start.6
  22.9 0.1 collective-permute-start.4
  23.0 13.9 %collective-permute-done.6.refs_2_ = bf16[256,2048]{1,0:T(8,128)(2,1)S(1)} collective-permute-done((bf16[256,2048]{1,0:T(8,128)(2,1)S(1)}, bf16[256,2048]{1,0:T(8,128)(2,1)S(1)}, u32[]{:S(2)}, u32[]{:S(2)}) %collective-permute-start.6) | collective-permute-done | bytes 1048608 | tf_op jit(solution)/shard_map/ppermute | solution.py:25
  36.9 3.2 %collective-permute-start.7 = (bf16[128,2048]{1,0:T(8,128)(2,1)S(1)}, bf16[128,2048]{1,0:T(8,128)(2,1)}, u32[]{:S(2)}, u32[]{:S(2)}) collective-permute-start(bf16[128,2048]{1,0:T(8,128)(2,1)S(1)} %slice.19), channel_id=1, source_target_pairs={{0,6},{2,0},{4,2},{6,4},{1,7},{3,1},{5,3},{7,5},{8,14},{10,8},{12,... | collective-permute-start | bytes 1572872 | tf_op jit(solution)/shard_map/ppermute | solution.py:25
  40.2 1.1 slice.18
  41.3 0.1 collective-permute-start.5
  41.4 0.1 dynamic-slice_bitcast_fusion
  41.5 0.7 dynamic-slice_convert_fusion
  42.2 22.6 %collective-permute-start.3 = (f32[4,256]{1,0:T(4,128)S(1)}, f32[4,256]{1,0:T(4,128)S(1)}, u32[]{:S(2)}, u32[]{:S(2)}) collective-permute-start(f32[4,256]{1,0:T(4,128)S(1)} %select_maximum_fusion), channel_id=1, source_target_pairs={{0,1},{1,0},{2,3},{3,2},{4,5},{5,4},{6,7},{7,6},{8,9},{9,8},{10,11... | collective-permute-start | bytes 12296 | tf_op jit(solution)/shard_map/ppermute | solution.py:297
  64.8 0.8 collective-permute-done.3
  65.6 0.5 slice.17
  66.1 58.4 %all-gather.2.cloned.1.call-done = bf16[4096,1664]{1,0:T(8,128)(2,1)} async-done(((bf16[128,1664]{1,0:T(8,128)(2,1)}), bf16[4096,1664]{1,0:T(8,128)(2,1)}) %all-gather.2.cloned.1.call-update) | async-done | bytes 13631504 | tf_op jit(solution)/shard_map/all_gather | solution.py:277
  124.5 0.0 collective-permute-done.5.refs_0_
  124.5 17.0 %project_rows.1 = (bf16[2,4,256,1024]{3,2,1,0:T(8,128)(2,1)}, bf16[4,256,256]{2,1,0:T(8,128)(2,1)}, bf16[2,4,160,128]{3,2,1,0:T(8,128)(2,1)}, bf16[1024,2048]{1,0:T(8,128)(2,1)}) custom-call(bf16[16,2,128,1664]{3,2,1,0:T(8,128)(2,1)} %bitcast.29, bf16[128,2048]{1,0:T(8,128)(2,1)} %collective-permute-done.5.refs_0_, ...), custom_call_target="tpu_custom_call" | custom-call | flops 9663676416 | bytes 25000000 | tf_op jit(solution)/shard_map/project_rows/pallas_call | solution.py:304
  141.6 2.6 %collective-permute-start.8 = (bf16[2,4,160,128]{3,2,1,0:T(8,128)(2,1)}, bf16[2,4,160,128]{3,2,1,0:T(8,128)(2,1)S(1)}, u32[]{:S(2)}, u32[]{:S(2)}) collective-permute-start(bf16[2,4,160,128]{3,2,1,0:T(8,128)(2,1)} %get-tuple-element.36), channel_id=1, source_target_pairs={{0,1},{1,8},{8,9},{9,16},{16,17},{17,24},{24,25},{25,32},{32,33},{... | collective-permute-start | bytes 983048 | tf_op jit(solution)/shard_map/ppermute | solution.py:333
  144.2 6.6 %shard_map.119 = (bf16[128,2048]{1,0:T(8,128)(2,1)}, bf16[128,2048]{1,0:T(8,128)(2,1)}) custom-call(s32[1]{0:T(128)} %bitcast.4.idx, f32[2,4]{1,0:T(2,128)} %bitcast.24, f32[2,3,256]{2,1,0:T(4,128)} %bitcast.18, bf16[1024,2048]{1,0:T(8,128)(2,1)} %get-tuple-element.33.wout, bf16[2,4,256,1024]{3,2,1,0:T(8,128)(2,1)} %get-tuple-element.34.refs_0_.refs_1_, ...), custom_call_target="tpu_custom_call" | custom-call | flops 1673741824 | bytes 8000000 | tf_op jit(solution)/shard_map/pallas_call | solution.py:342
  150.8 2.5 %collective-permute-start.15 = (bf16[128,2048]{1,0:T(8,128)(2,1)}, bf16[128,2048]{1,0:T(8,128)(2,1)S(1)}, u32[]{:S(2)}, u32[]{:S(2)}) collective-permute-start(bf16[128,2048]{1,0:T(8,128)(2,1)} %get-tuple-element.44), channel_id=1, source_target_pairs={{0,6},{2,0},{4,2},{6,4},{1,7},{3,1},{5,3},{7,5},{8,14},{10,8},{12,... | collective-permute-start | bytes 1572872 | tf_op jit(solution)/shard_map/ppermute | solution.py:25
  153.3 0.7 copy-done.1
  154.0 6.6 %shard_map.118 = (bf16[64,2048]{1,0:T(8,128)(2,1)}, bf16[64,2048]{1,0:T(8,128)(2,1)}, bf16[128,2048]{1,0:T(8,128)(2,1)}) custom-call(s32[1]{0:T(128)} %bitcast.4.idx, f32[2,4]{1,0:T(2,128)} %bitcast.25, f32[2,3,256]{2,1,0:T(4,128)} %bitcast.19, bf16[1024,2048]{1,0:T(8,128)(2,1)} %get-tuple-element.33.wout, ...), custom_call_target="tpu_custom_call" | custom-call | flops 1673741824 | bytes 8000000 | tf_op jit(solution)/shard_map/pallas_call | solution.py:342
  160.6 0.3 collective-permute-start.11
  161.0 1.2 collective-permute-start.13
  162.2 1.7 collective-permute-start.9
  163.9 6.6 %shard_map.121 = (bf16[64,2048]{1,0:T(8,128)(2,1)}, bf16[64,2048]{1,0:T(8,128)(2,1)}, bf16[128,2048]{1,0:T(8,128)(2,1)}) custom-call(s32[1]{0:T(128)} %bitcast.4.idx, f32[2,4]{1,0:T(2,128)} %bitcast.26, f32[2,3,256]{2,1,0:T(4,128)} %bitcast.20, bf16[1024,2048]{1,0:T(8,128)(2,1)} %get-tuple-element.33.wout, ...), custom_call_target="tpu_custom_call" | custom-call | flops 1673741824 | bytes 8000000 | tf_op jit(solution)/shard_map/pallas_call | solution.py:342
  170.6 1.2 add_convert_fusion.1
  171.8 1.2 collective-permute-start.16
  173.0 0.5 collective-permute-done.11
  173.5 1.0 add_convert_fusion.3
  174.5 0.1 collective-permute-start.12
  174.7 4.5 %collective-permute-done.13 = bf16[64,2048]{1,0:T(8,128)(2,1)S(1)} collective-permute-done((bf16[64,2048]{1,0:T(8,128)(2,1)}, bf16[64,2048]{1,0:T(8,128)(2,1)S(1)}, u32[]{:S(2)}, u32[]{:S(2)}) %collective-permute-start.13) | collective-permute-done | bytes 262176 | tf_op jit(solution)/shard_map/ppermute | solution.py:25
  179.1 0.1 add_convert_fusion.2
  179.2 0.1 collective-permute-start.14
  179.4 0.8 copy-done.4
  180.2 0.8 copy-done.5
  180.9 7.2 %shard_map.120 = bf16[256,2048]{1,0:T(8,128)(2,1)} custom-call(s32[1]{0:T(128)} %bitcast.4.idx, f32[2,4]{1,0:T(2,128)} %bitcast.27, f32[2,3,256]{2,1,0:T(4,128)} %bitcast.21, bf16[1024,2048]{1,0:T(8,128)(2,1)} %get-tuple-element.33.wout, bf16[2,4,256,1024]{3,2,1,0:T(8,128)(2,1)} %get-tuple-element.34.refs_0_.refs_1_, ...), custom_call_target="tpu_custom_call" | custom-call | flops 1673741824 | bytes 8000000 | tf_op jit(solution)/shard_map/pallas_call | solution.py:342
  188.2 1.9 collective-permute-done.14
  190.1 2.6 %fusion.3 = bf16[1,256,2048]{2,1,0:T(8,128)(2,1)} fusion(bf16[256,2048]{1,0:T(8,128)(2,1)} %shard_map.120, bf16[128,2048]{1,0:T(8,128)(2,1)S(1)} %collective-permute-done.16, bf16[64,2048]{1,0:T(8,128)(2,1)S(1)} %collective-permute-done.14, bf16[64,2048]{1,0:T(8,128)(2,1)S(1)} %collective-permute-done.12), kind=kLoop, calls=%fused_computation.6 | loop fusion | flops 4718592 | bytes 3145728 | tf_op jit(solution)/shard_map/broadcast_in_dim | solution.py:378
  (37 shorter events, 0.1 us)
Async XLA Ops:
  6.5 34.8 %copy-start = (f32[16]{0:T(128)S(1)}, f32[16]{0:T(128)}, u32[]{:S(2)}) copy-start(f32[16]{0:T(128)} %param.21) | copy-start | bytes 196
  6.6 14.2 %copy-start.2 = (bf16[1,256,2048]{2,1,0:T(8,128)(2,1)S(1)}, bf16[1,256,2048]{2,1,0:T(8,128)(2,1)}, u32[]{:S(2)}) copy-start(bf16[1,256,2048]{2,1,0:T(8,128)(2,1)} %param.12) | copy-start | bytes 3145732
  6.6 14.5 %copy-start.12 = (f32[2048]{0:T(1024)S(1)}, f32[2048]{0:T(1024)}, u32[]{:S(2)}) copy-start(f32[2048]{0:T(1024)} %param.13) | copy-start | bytes 24580
  6.6 117.9 %all-gather.2.cloned.1.call-start = ((), (), s32[]{:S(2)}) async-start(), calls=%async_computation | async-start | bytes 14057472 | tf_op jit(solution)/shard_map/all_gather | solution.py:277
  8.6 6.0 %collective-permute-start = (bf16[32,1664]{1,0:T(8,128)(2,1)}, bf16[32,1664]{1,0:T(8,128)(2,1)S(1)}, u32[]{:S(2)}, u32[]{:S(2)}) collective-permute-start(bf16[32,1664]{1,0:T(8,128)(2,1)} %get-tuple-element.26), channel_id=1, source_target_pairs={{0,2},{2,4},{4,6},{6,0},{1,3},{3,5},{5,7},{7,1},{8,10},{10,12},{12... | collective-permute-start | bytes 319496 | tf_op jit(solution)/shard_map/ppermute | solution.py:25
  10.7 7.3 %collective-permute-start.1 = (bf16[32,1664]{1,0:T(8,128)(2,1)}, bf16[32,1664]{1,0:T(8,128)(2,1)S(1)}, u32[]{:S(2)}, u32[]{:S(2)}) collective-permute-start(bf16[32,1664]{1,0:T(8,128)(2,1)} %get-tuple-element.27), channel_id=1, source_target_pairs={{0,4},{2,6},{4,0},{6,2},{1,5},{3,7},{5,1},{7,3},{8,12},{10,14},{12... | collective-permute-start | bytes 319496 | tf_op jit(solution)/shard_map/ppermute | solution.py:25
  13.5 4.6 %collective-permute-start.2 = (bf16[32,1664]{1,0:T(8,128)(2,1)}, bf16[32,1664]{1,0:T(8,128)(2,1)S(1)}, u32[]{:S(2)}, u32[]{:S(2)}) collective-permute-start(bf16[32,1664]{1,0:T(8,128)(2,1)} %get-tuple-element.28), channel_id=1, source_target_pairs={{0,6},{2,0},{4,2},{6,4},{1,7},{3,1},{5,3},{7,5},{8,14},{10,8},{12,... | collective-permute-start | bytes 319496 | tf_op jit(solution)/shard_map/ppermute | solution.py:25
  14.6 3.5 %copy-start.9 = (bf16[32,1664]{1,0:T(8,128)(2,1)}, bf16[32,1664]{1,0:T(8,128)(2,1)S(1)}, u32[]{:S(2)}) copy-start(bf16[32,1664]{1,0:T(8,128)(2,1)S(1)} %collective-permute-done.refs_1_) | copy-start | bytes 319492
  18.0 0.6 copy-start.10
  18.1 0.7 copy-start.11
  21.4 103.1 %copy-start.3 = (bf16[256,2048]{1,0:T(8,128)(2,1)}, bf16[256,2048]{1,0:T(8,128)(2,1)S(1)}, u32[]{:S(2)}) copy-start(bf16[256,2048]{1,0:T(8,128)(2,1)S(1)} %fusion.2.refs_4_) | copy-start | bytes 3145732
  21.4 15.5 %collective-permute-start.6 = (bf16[256,2048]{1,0:T(8,128)(2,1)S(1)}, bf16[256,2048]{1,0:T(8,128)(2,1)S(1)}, u32[]{:S(2)}, u32[]{:S(2)}) collective-permute-start(bf16[256,2048]{1,0:T(8,128)(2,1)S(1)} %fusion.2.refs_4_), channel_id=1, source_target_pairs={{0,6},{2,0},{4,2},{6,4},{1,7},{3,1},{5,3},{7,5},{8,14},{10,8},{12,... | collective-permute-start | bytes 3145736 | tf_op jit(solution)/shard_map/ppermute | solution.py:25
  22.9 17.3 %collective-permute-start.4 = (bf16[256,2048]{1,0:T(8,128)(2,1)S(1)}, bf16[256,2048]{1,0:T(8,128)(2,1)}, u32[]{:S(2)}, u32[]{:S(2)}) collective-permute-start(bf16[256,2048]{1,0:T(8,128)(2,1)S(1)} %fusion.2.refs_4_), channel_id=1, source_target_pairs={{0,2},{2,4},{4,6},{6,0},{1,3},{3,5},{5,7},{7,1},{8,10},{10,12},{12... | collective-permute-start | bytes 3145736 | tf_op jit(solution)/shard_map/ppermute | solution.py:25
  36.9 87.6 %copy-start.7 = (bf16[256,2048]{1,0:T(8,128)(2,1)}, bf16[256,2048]{1,0:T(8,128)(2,1)S(1)}, u32[]{:S(2)}) copy-start(bf16[256,2048]{1,0:T(8,128)(2,1)S(1)} %collective-permute-done.6.refs_2_) | copy-start | bytes 3145732
  36.9 87.6 %collective-permute-start.7 = (bf16[128,2048]{1,0:T(8,128)(2,1)S(1)}, bf16[128,2048]{1,0:T(8,128)(2,1)}, u32[]{:S(2)}, u32[]{:S(2)}) collective-permute-start(bf16[128,2048]{1,0:T(8,128)(2,1)S(1)} %slice.19), channel_id=1, source_target_pairs={{0,6},{2,0},{4,2},{6,4},{1,7},{3,1},{5,3},{7,5},{8,14},{10,8},{12,... | collective-permute-start | bytes 1572872 | tf_op jit(solution)/shard_map/ppermute | solution.py:25
  41.3 83.3 %collective-permute-start.5 = (bf16[128,2048]{1,0:T(8,128)(2,1)S(1)}, bf16[128,2048]{1,0:T(8,128)(2,1)}, u32[]{:S(2)}, u32[]{:S(2)}) collective-permute-start(bf16[128,2048]{1,0:T(8,128)(2,1)S(1)} %slice.18), channel_id=1, source_target_pairs={{0,2},{2,4},{4,6},{6,0},{1,3},{3,5},{5,7},{7,1},{8,10},{10,12},{12... | collective-permute-start | bytes 1572872 | tf_op jit(solution)/shard_map/ppermute | solution.py:25
  42.2 23.4 %collective-permute-start.3 = (f32[4,256]{1,0:T(4,128)S(1)}, f32[4,256]{1,0:T(4,128)S(1)}, u32[]{:S(2)}, u32[]{:S(2)}) collective-permute-start(f32[4,256]{1,0:T(4,128)S(1)} %select_maximum_fusion), channel_id=1, source_target_pairs={{0,1},{1,0},{2,3},{3,2},{4,5},{5,4},{6,7},{7,6},{8,9},{9,8},{10,11... | collective-permute-start | bytes 12296 | tf_op jit(solution)/shard_map/ppermute | solution.py:297
  65.6 76.0 %copy-start.8 = (f32[2,4,256]{2,1,0:T(4,128)}, f32[2,4,256]{2,1,0:T(4,128)S(1)}, u32[]{:S(2)}) copy-start(f32[2,4,256]{2,1,0:T(4,128)S(1)} %maximum_select_fusion) | copy-start | bytes 24580
  141.6 11.7 %collective-permute-start.8 = (bf16[2,4,160,128]{3,2,1,0:T(8,128)(2,1)}, bf16[2,4,160,128]{3,2,1,0:T(8,128)(2,1)S(1)}, u32[]{:S(2)}, u32[]{:S(2)}) collective-permute-start(bf16[2,4,160,128]{3,2,1,0:T(8,128)(2,1)} %get-tuple-element.36), channel_id=1, source_target_pairs={{0,1},{1,8},{8,9},{9,16},{16,17},{17,24},{24,25},{25,32},{32,33},{... | collective-permute-start | bytes 983048 | tf_op jit(solution)/shard_map/ppermute | solution.py:333
  150.8 19.8 %collective-permute-start.15 = (bf16[128,2048]{1,0:T(8,128)(2,1)}, bf16[128,2048]{1,0:T(8,128)(2,1)S(1)}, u32[]{:S(2)}, u32[]{:S(2)}) collective-permute-start(bf16[128,2048]{1,0:T(8,128)(2,1)} %get-tuple-element.44), channel_id=1, source_target_pairs={{0,6},{2,0},{4,2},{6,4},{1,7},{3,1},{5,3},{7,5},{8,14},{10,8},{12,... | collective-permute-start | bytes 1572872 | tf_op jit(solution)/shard_map/ppermute | solution.py:25
  153.3 26.1 %collective-permute-start.10 = (bf16[128,2048]{1,0:T(8,128)(2,1)}, bf16[128,2048]{1,0:T(8,128)(2,1)S(1)}, u32[]{:S(2)}, u32[]{:S(2)}) collective-permute-start(bf16[128,2048]{1,0:T(8,128)(2,1)} %get-tuple-element.38), channel_id=1, source_target_pairs={{0,2},{2,4},{4,6},{6,0},{1,3},{3,5},{5,7},{7,1},{8,10},{10,12},{12... | collective-permute-start | bytes 1572872 | tf_op jit(solution)/shard_map/ppermute | solution.py:25
  153.3 0.7 copy-start.1
  160.6 12.9 %collective-permute-start.11 = (bf16[64,2048]{1,0:T(8,128)(2,1)}, bf16[64,2048]{1,0:T(8,128)(2,1)S(1)}, u32[]{:S(2)}, u32[]{:S(2)}) collective-permute-start(bf16[64,2048]{1,0:T(8,128)(2,1)} %get-tuple-element.40), channel_id=1, source_target_pairs={{0,2},{2,4},{4,6},{6,0},{1,3},{3,5},{5,7},{7,1},{8,10},{10,12},{12... | collective-permute-start | bytes 786440 | tf_op jit(solution)/shard_map/ppermute | solution.py:25
  161.0 18.2 %collective-permute-start.13 = (bf16[64,2048]{1,0:T(8,128)(2,1)}, bf16[64,2048]{1,0:T(8,128)(2,1)S(1)}, u32[]{:S(2)}, u32[]{:S(2)}) collective-permute-start(bf16[64,2048]{1,0:T(8,128)(2,1)} %get-tuple-element.42), channel_id=1, source_target_pairs={{0,2},{2,4},{4,6},{6,0},{1,3},{3,5},{5,7},{7,1},{8,10},{10,12},{12... | collective-permute-start | bytes 786440 | tf_op jit(solution)/shard_map/ppermute | solution.py:25
  162.2 17.2 %collective-permute-start.9 = (bf16[128,2048]{1,0:T(8,128)(2,1)}, bf16[128,2048]{1,0:T(8,128)(2,1)S(1)}, u32[]{:S(2)}, u32[]{:S(2)}) collective-permute-start(bf16[128,2048]{1,0:T(8,128)(2,1)} %get-tuple-element.37), channel_id=1, source_target_pairs={{0,6},{2,0},{4,2},{6,4},{1,7},{3,1},{5,3},{7,5},{8,14},{10,8},{12,... | collective-permute-start | bytes 1572872 | tf_op jit(solution)/shard_map/ppermute | solution.py:25
  170.6 8.6 %copy-start.6 = (bf16[64,2048]{1,0:T(8,128)(2,1)S(1)}, bf16[64,2048]{1,0:T(8,128)(2,1)}, u32[]{:S(2)}) copy-start(bf16[64,2048]{1,0:T(8,128)(2,1)} %get-tuple-element.41) | copy-start | bytes 786436
  171.8 18.3 %collective-permute-start.16 = (bf16[128,2048]{1,0:T(8,128)(2,1)S(1)}, bf16[128,2048]{1,0:T(8,128)(2,1)S(1)}, u32[]{:S(2)}, u32[]{:S(2)}) collective-permute-start(bf16[128,2048]{1,0:T(8,128)(2,1)S(1)} %add_convert_fusion.1), channel_id=1, source_target_pairs={{0,6},{2,0},{4,2},{6,4},{1,7},{3,1},{5,3},{7,5},{8,14},{10,8},{12,... | collective-permute-start | bytes 1572872 | tf_op jit(solution)/shard_map/ppermute | solution.py:25
  174.5 13.6 %collective-permute-start.12 = (bf16[64,2048]{1,0:T(8,128)(2,1)S(1)}, bf16[64,2048]{1,0:T(8,128)(2,1)S(1)}, u32[]{:S(2)}, u32[]{:S(2)}) collective-permute-start(bf16[64,2048]{1,0:T(8,128)(2,1)S(1)} %add_convert_fusion.3), channel_id=1, source_target_pairs={{0,2},{2,4},{4,6},{6,0},{1,3},{3,5},{5,7},{7,1},{8,10},{10,12},{12... | collective-permute-start | bytes 786440 | tf_op jit(solution)/shard_map/ppermute | solution.py:25
  179.2 10.9 %collective-permute-start.14 = (bf16[64,2048]{1,0:T(8,128)(2,1)S(1)}, bf16[64,2048]{1,0:T(8,128)(2,1)S(1)}, u32[]{:S(2)}, u32[]{:S(2)}) collective-permute-start(bf16[64,2048]{1,0:T(8,128)(2,1)S(1)} %add_convert_fusion.2), channel_id=1, source_target_pairs={{0,2},{2,4},{4,6},{6,0},{1,3},{3,5},{5,7},{7,1},{8,10},{10,12},{12... | collective-permute-start | bytes 786440 | tf_op jit(solution)/shard_map/ppermute | solution.py:25
  179.4 0.8 copy-start.4
  180.2 0.8 copy-start.5
Sparse Core Ops, SparseCore 0:
  20.9 103.5 all-gather.1

commit v5 on v4

--- a/solution.py
+++ b/solution.py
@@ -12,7 +12,6 @@
 WINDOW = 128
 TAPS = 3
 EPSILON = 1e-06
-LOG2_E = 1.4426950408889634
 
 
 ANY = pl.BlockSpec(memory_space=pl.ANY)
@@ -202,12 +201,12 @@
             for h in range(heads):
                 qh = jnp.where((lane >= h * HEAD) & (lane < (h + 1) * HEAD), q, jnp.zeros_like(q))
                 sc = jnp.dot(qh, keys, preferred_element_type=f32)
-                sc = jnp.where(allowed, sc * (LOG2_E / 8.0), -jnp.inf)
-                sink = sinks[side, h] * LOG2_E
+                sc = jnp.where(allowed, sc * (1.0 / 8.0), -jnp.inf)
+                sink = sinks[side, h]
                 m = jnp.maximum(jnp.max(sc, axis=1, keepdims=True), sink)
-                e = jnp.exp2(sc - m).astype(bf16)
+                e = jnp.exp(sc - m).astype(bf16)
                 o = jnp.dot(e, values, preferred_element_type=f32)
-                outs.append(o[:, :pair] / (o[:, pair:] + jnp.exp2(sink - m)))
+                outs.append(o[:, :pair] / (o[:, pair:] + jnp.exp(sink - m)))
             for j in range(heads // 2):
                 col = base + chans + j * pair
                 acts[to : to + WINDOW, col : col + pair] = jnp.where(

time: 200 us -> 200 us (level)
  Pallas kernels: 48 us -> 45.7 us
    pallas_call x4, Pallas kernels: 27 us -> 24.7 us  [mix(): pl.pallas_call(functools.partial(mix_kernel, blocks, pieces, b_width), ou...]
  transfers between devices with their start and end apart: 18 -> 18, of which waited for: 8 -> 8; matrix products, arithmetic and copies ran while one was open for 3% -> 3% of each run, Pallas kernels for 14% -> 12%
where the time goes in v5:
time: 200 us; the launch traced here: 199 us
  waiting for transfers between devices  85.4 us (43%)
  Pallas kernels  45.7 us (23%)
  starting transfers between devices  43.4 us (22%)
  between operations  13.7 us (7%)
  other arithmetic  6.19 us (3%)
  local copies, waits for them, and re-layouts  4.71 us (2%)
    all_gather x1, waiting for transfers between devices, layer(): weights = lax.all_gather(mine, ('sp', 'tp'), axis=0, tiled=True)  58.4 us
    ppermute x15, waiting for transfers between devices, ring(): lax.ppermute(array, axis, [(i, (i + by) % size) for i in range(size)])  26.1 us
    pallas_call x4, Pallas kernels, mix(): pl.pallas_call(functools.partial(mix_kernel, blocks, pieces, b_width), ou...  24.7 us
    ppermute x1, starting transfers between devices, layer(): theirs = lax.ppermute(small, 'tp', [(0, 1), (1, 0)])  22.6 us
    ppermute x15, starting transfers between devices, ring(): lax.ppermute(array, axis, [(i, (i + by) % size) for i in range(size)])  18.1 us
    pallas_call x1, Pallas kernels, layer(): pl.pallas_call(functools.partial(project_kernel, b_width), out_shape=(jax...  17 us
  transfers between devices with their start and end apart: 18, of which 8 were waited for; matrix products, arithmetic and copies ran while one was open for 3% of the time, Pallas kernels for 12%

profile of v5, /device:TPU:33, one launch (start us, length us, event | category | flops | bytes accessed | tf_op | source)
XLA Modules:
  0.0 199.0 jit_solution(9192241536751008760)
XLA Ops:
  6.6 2.0 %pack_weights.1 = (bf16[32,1664]{1,0:T(8,128)(2,1)}, bf16[32,1664]{1,0:T(8,128)(2,1)}, bf16[32,1664]{1,0:T(8,128)(2,1)}, bf16[32,1664]{1,0:T(8,128)(2,1)}) custom-call(s32[1]{0:T(128)} %bitcast.group, bf16[32,1024]{1,0:T(8,128)(2,1)} %wq.1, bf16[32,128]{1,0:T(8,128)(2,1)} %wk.1, bf16[32,128]{1,0:T(8,128)(2,1)} %wv.1, bf16[32,1024]{1,0:T(8,128)(2,1)} %bitcast.22, ...), custom_call_target="tpu_custom_call" | custom-call | tf_op jit(solution)/shard_map/pack_weights/pallas_call | solution.py:261
  8.6 2.2 %collective-permute-start = (bf16[32,1664]{1,0:T(8,128)(2,1)}, bf16[32,1664]{1,0:T(8,128)(2,1)S(1)}, u32[]{:S(2)}, u32[]{:S(2)}) collective-permute-start(bf16[32,1664]{1,0:T(8,128)(2,1)} %get-tuple-element.26), channel_id=1, source_target_pairs={{0,2},{2,4},{4,6},{6,0},{1,3},{3,5},{5,7},{7,1},{8,10},{10,12},{12... | collective-permute-start | bytes 319496 | tf_op jit(solution)/shard_map/ppermute | solution.py:24
  10.7 2.7 %collective-permute-start.1 = (bf16[32,1664]{1,0:T(8,128)(2,1)}, bf16[32,1664]{1,0:T(8,128)(2,1)S(1)}, u32[]{:S(2)}, u32[]{:S(2)}) collective-permute-start(bf16[32,1664]{1,0:T(8,128)(2,1)} %get-tuple-element.27), channel_id=1, source_target_pairs={{0,4},{2,6},{4,0},{6,2},{1,5},{3,7},{5,1},{7,3},{8,12},{10,14},{12... | collective-permute-start | bytes 319496 | tf_op jit(solution)/shard_map/ppermute | solution.py:24
  13.5 1.0 collective-permute-start.2
  14.5 0.1 collective-permute-done.refs_1_
  14.6 3.5 %collective-permute-done.1.refs_2_ = bf16[32,1664]{1,0:T(8,128)(2,1)S(1)} collective-permute-done((bf16[32,1664]{1,0:T(8,128)(2,1)}, bf16[32,1664]{1,0:T(8,128)(2,1)S(1)}, u32[]{:S(2)}, u32[]{:S(2)}) %collective-permute-start.1) | collective-permute-done | bytes 106528 | tf_op jit(solution)/shard_map/ppermute | solution.py:24
  18.1 0.6 copy-done.10
  18.7 0.0 copy-done.11
  18.7 1.9 turn_weights.1
  20.7 0.1 all-gather.2.cloned.1.call-update
  20.7 0.3 fusion
  21.1 0.3 fusion.2.refs_4_
  21.4 1.5 collective-permute-start.6
  22.9 0.1 collective-permute-start.4
  23.0 13.9 %collective-permute-done.6.refs_2_ = bf16[256,2048]{1,0:T(8,128)(2,1)S(1)} collective-permute-done((bf16[256,2048]{1,0:T(8,128)(2,1)S(1)}, bf16[256,2048]{1,0:T(8,128)(2,1)S(1)}, u32[]{:S(2)}, u32[]{:S(2)}) %collective-permute-start.6) | collective-permute-done | bytes 1048608 | tf_op jit(solution)/shard_map/ppermute | solution.py:24
  36.9 3.2 %collective-permute-start.7 = (bf16[128,2048]{1,0:T(8,128)(2,1)S(1)}, bf16[128,2048]{1,0:T(8,128)(2,1)}, u32[]{:S(2)}, u32[]{:S(2)}) collective-permute-start(bf16[128,2048]{1,0:T(8,128)(2,1)S(1)} %slice.19), channel_id=1, source_target_pairs={{0,6},{2,0},{4,2},{6,4},{1,7},{3,1},{5,3},{7,5},{8,14},{10,8},{12,... | collective-permute-start | bytes 1572872 | tf_op jit(solution)/shard_map/ppermute | solution.py:24
  40.2 1.1 slice.18
  41.3 0.1 collective-permute-start.5
  41.4 0.1 dynamic-slice_bitcast_fusion
  41.5 0.7 dynamic-slice_convert_fusion
  42.2 22.6 %collective-permute-start.3 = (f32[4,256]{1,0:T(4,128)S(1)}, f32[4,256]{1,0:T(4,128)S(1)}, u32[]{:S(2)}, u32[]{:S(2)}) collective-permute-start(f32[4,256]{1,0:T(4,128)S(1)} %select_maximum_fusion), channel_id=1, source_target_pairs={{0,1},{1,0},{2,3},{3,2},{4,5},{5,4},{6,7},{7,6},{8,9},{9,8},{10,11... | collective-permute-start | bytes 12296 | tf_op jit(solution)/shard_map/ppermute | solution.py:296
  64.8 0.8 collective-permute-done.3
  65.6 0.5 slice.17
  66.1 58.4 %all-gather.2.cloned.1.call-done = bf16[4096,1664]{1,0:T(8,128)(2,1)} async-done(((bf16[128,1664]{1,0:T(8,128)(2,1)}), bf16[4096,1664]{1,0:T(8,128)(2,1)}) %all-gather.2.cloned.1.call-update) | async-done | bytes 13631504 | tf_op jit(solution)/shard_map/all_gather | solution.py:276
  124.5 0.0 collective-permute-done.5.refs_0_
  124.5 17.0 %project_rows.1 = (bf16[2,4,256,1024]{3,2,1,0:T(8,128)(2,1)}, bf16[4,256,256]{2,1,0:T(8,128)(2,1)}, bf16[2,4,160,128]{3,2,1,0:T(8,128)(2,1)}, bf16[1024,2048]{1,0:T(8,128)(2,1)}) custom-call(bf16[16,2,128,1664]{3,2,1,0:T(8,128)(2,1)} %bitcast.29, bf16[128,2048]{1,0:T(8,128)(2,1)} %collective-permute-done.5.refs_0_, ...), custom_call_target="tpu_custom_call" | custom-call | flops 9663676416 | bytes 25000000 | tf_op jit(solution)/shard_map/project_rows/pallas_call | solution.py:303
  141.6 2.6 %collective-permute-start.8 = (bf16[2,4,160,128]{3,2,1,0:T(8,128)(2,1)}, bf16[2,4,160,128]{3,2,1,0:T(8,128)(2,1)S(1)}, u32[]{:S(2)}, u32[]{:S(2)}) collective-permute-start(bf16[2,4,160,128]{3,2,1,0:T(8,128)(2,1)} %get-tuple-element.36), channel_id=1, source_target_pairs={{0,1},{1,8},{8,9},{9,16},{16,17},{17,24},{24,25},{25,32},{32,33},{... | collective-permute-start | bytes 983048 | tf_op jit(solution)/shard_map/ppermute | solution.py:332
  144.2 6.0 %shard_map.119 = (bf16[128,2048]{1,0:T(8,128)(2,1)}, bf16[128,2048]{1,0:T(8,128)(2,1)}) custom-call(s32[1]{0:T(128)} %bitcast.4.idx, f32[2,4]{1,0:T(2,128)} %bitcast.24, f32[2,3,256]{2,1,0:T(4,128)} %bitcast.18, bf16[1024,2048]{1,0:T(8,128)(2,1)} %get-tuple-element.33.wout, bf16[2,4,256,1024]{3,2,1,0:T(8,128)(2,1)} %get-tuple-element.34.refs_0_.refs_1_, ...), custom_call_target="tpu_custom_call" | custom-call | flops 1673741824 | bytes 8000000 | tf_op jit(solution)/shard_map/pallas_call | solution.py:341
  150.2 2.5 %collective-permute-start.15 = (bf16[128,2048]{1,0:T(8,128)(2,1)}, bf16[128,2048]{1,0:T(8,128)(2,1)S(1)}, u32[]{:S(2)}, u32[]{:S(2)}) collective-permute-start(bf16[128,2048]{1,0:T(8,128)(2,1)} %get-tuple-element.44), channel_id=1, source_target_pairs={{0,6},{2,0},{4,2},{6,4},{1,7},{3,1},{5,3},{7,5},{8,14},{10,8},{12,... | collective-permute-start | bytes 1572872 | tf_op jit(solution)/shard_map/ppermute | solution.py:24
  152.8 0.7 copy-done.1
  153.5 6.0 %shard_map.118 = (bf16[64,2048]{1,0:T(8,128)(2,1)}, bf16[64,2048]{1,0:T(8,128)(2,1)}, bf16[128,2048]{1,0:T(8,128)(2,1)}) custom-call(s32[1]{0:T(128)} %bitcast.4.idx, f32[2,4]{1,0:T(2,128)} %bitcast.25, f32[2,3,256]{2,1,0:T(4,128)} %bitcast.19, bf16[1024,2048]{1,0:T(8,128)(2,1)} %get-tuple-element.33.wout, ...), custom_call_target="tpu_custom_call" | custom-call | flops 1673741824 | bytes 8000000 | tf_op jit(solution)/shard_map/pallas_call | solution.py:341
  159.5 0.3 collective-permute-start.11
  159.8 1.2 collective-permute-start.13
  161.0 1.7 collective-permute-start.9
  162.8 6.0 %shard_map.121 = (bf16[64,2048]{1,0:T(8,128)(2,1)}, bf16[64,2048]{1,0:T(8,128)(2,1)}, bf16[128,2048]{1,0:T(8,128)(2,1)}) custom-call(s32[1]{0:T(128)} %bitcast.4.idx, f32[2,4]{1,0:T(2,128)} %bitcast.26, f32[2,3,256]{2,1,0:T(4,128)} %bitcast.20, bf16[1024,2048]{1,0:T(8,128)(2,1)} %get-tuple-element.33.wout, ...), custom_call_target="tpu_custom_call" | custom-call | flops 1673741824 | bytes 8000000 | tf_op jit(solution)/shard_map/pallas_call | solution.py:341
  168.8 1.2 add_convert_fusion.1
  170.1 1.2 collective-permute-start.16
  171.3 1.7 collective-permute-done.11
  173.0 1.0 add_convert_fusion.3
  174.0 0.1 collective-permute-start.12
  174.1 4.5 %collective-permute-done.13 = bf16[64,2048]{1,0:T(8,128)(2,1)S(1)} collective-permute-done((bf16[64,2048]{1,0:T(8,128)(2,1)}, bf16[64,2048]{1,0:T(8,128)(2,1)S(1)}, u32[]{:S(2)}, u32[]{:S(2)}) %collective-permute-start.13) | collective-permute-done | bytes 262176 | tf_op jit(solution)/shard_map/ppermute | solution.py:24
  178.6 0.1 add_convert_fusion.2
  178.7 0.1 collective-permute-start.14
  178.8 0.8 copy-done.4
  179.6 0.8 copy-done.5
  180.4 6.6 %shard_map.120 = bf16[256,2048]{1,0:T(8,128)(2,1)} custom-call(s32[1]{0:T(128)} %bitcast.4.idx, f32[2,4]{1,0:T(2,128)} %bitcast.27, f32[2,3,256]{2,1,0:T(4,128)} %bitcast.21, bf16[1024,2048]{1,0:T(8,128)(2,1)} %get-tuple-element.33.wout, bf16[2,4,256,1024]{3,2,1,0:T(8,128)(2,1)} %get-tuple-element.34.refs_0_.refs_1_, ...), custom_call_target="tpu_custom_call" | custom-call | flops 1673741824 | bytes 8000000 | tf_op jit(solution)/shard_map/pallas_call | solution.py:341
  187.0 2.5 %collective-permute-done.14 = bf16[64,2048]{1,0:T(8,128)(2,1)S(1)} collective-permute-done((bf16[64,2048]{1,0:T(8,128)(2,1)S(1)}, bf16[64,2048]{1,0:T(8,128)(2,1)S(1)}, u32[]{:S(2)}, u32[]{:S(2)}) %collective-permute-start.14) | collective-permute-done | bytes 262176 | tf_op jit(solution)/shard_map/ppermute | solution.py:24
  189.5 2.6 %fusion.3 = bf16[1,256,2048]{2,1,0:T(8,128)(2,1)} fusion(bf16[256,2048]{1,0:T(8,128)(2,1)} %shard_map.120, bf16[128,2048]{1,0:T(8,128)(2,1)S(1)} %collective-permute-done.16, bf16[64,2048]{1,0:T(8,128)(2,1)S(1)} %collective-permute-done.14, bf16[64,2048]{1,0:T(8,128)(2,1)S(1)} %collective-permute-done.12), kind=kLoop, calls=%fused_computation.6 | loop fusion | flops 4718592 | bytes 3145728 | tf_op jit(solution)/shard_map/broadcast_in_dim | solution.py:377
  (37 shorter events, 0.1 us)
Async XLA Ops:
  6.5 34.8 %copy-start = (f32[16]{0:T(128)S(1)}, f32[16]{0:T(128)}, u32[]{:S(2)}) copy-start(f32[16]{0:T(128)} %param.21) | copy-start | bytes 196
  6.6 14.2 %copy-start.2 = (bf16[1,256,2048]{2,1,0:T(8,128)(2,1)S(1)}, bf16[1,256,2048]{2,1,0:T(8,128)(2,1)}, u32[]{:S(2)}) copy-start(bf16[1,256,2048]{2,1,0:T(8,128)(2,1)} %param.12) | copy-start | bytes 3145732
  6.6 14.5 %copy-start.12 = (f32[2048]{0:T(1024)S(1)}, f32[2048]{0:T(1024)}, u32[]{:S(2)}) copy-start(f32[2048]{0:T(1024)} %param.13) | copy-start | bytes 24580
  6.6 117.9 %all-gather.2.cloned.1.call-start = ((), (), s32[]{:S(2)}) async-start(), calls=%async_computation | async-start | bytes 14057472 | tf_op jit(solution)/shard_map/all_gather | solution.py:276
  8.6 6.0 %collective-permute-start = (bf16[32,1664]{1,0:T(8,128)(2,1)}, bf16[32,1664]{1,0:T(8,128)(2,1)S(1)}, u32[]{:S(2)}, u32[]{:S(2)}) collective-permute-start(bf16[32,1664]{1,0:T(8,128)(2,1)} %get-tuple-element.26), channel_id=1, source_target_pairs={{0,2},{2,4},{4,6},{6,0},{1,3},{3,5},{5,7},{7,1},{8,10},{10,12},{12... | collective-permute-start | bytes 319496 | tf_op jit(solution)/shard_map/ppermute | solution.py:24
  10.7 7.3 %collective-permute-start.1 = (bf16[32,1664]{1,0:T(8,128)(2,1)}, bf16[32,1664]{1,0:T(8,128)(2,1)S(1)}, u32[]{:S(2)}, u32[]{:S(2)}) collective-permute-start(bf16[32,1664]{1,0:T(8,128)(2,1)} %get-tuple-element.27), channel_id=1, source_target_pairs={{0,4},{2,6},{4,0},{6,2},{1,5},{3,7},{5,1},{7,3},{8,12},{10,14},{12... | collective-permute-start | bytes 319496 | tf_op jit(solution)/shard_map/ppermute | solution.py:24
  13.5 4.6 %collective-permute-start.2 = (bf16[32,1664]{1,0:T(8,128)(2,1)}, bf16[32,1664]{1,0:T(8,128)(2,1)S(1)}, u32[]{:S(2)}, u32[]{:S(2)}) collective-permute-start(bf16[32,1664]{1,0:T(8,128)(2,1)} %get-tuple-element.28), channel_id=1, source_target_pairs={{0,6},{2,0},{4,2},{6,4},{1,7},{3,1},{5,3},{7,5},{8,14},{10,8},{12,... | collective-permute-start | bytes 319496 | tf_op jit(solution)/shard_map/ppermute | solution.py:24
  14.6 3.5 %copy-start.9 = (bf16[32,1664]{1,0:T(8,128)(2,1)}, bf16[32,1664]{1,0:T(8,128)(2,1)S(1)}, u32[]{:S(2)}) copy-start(bf16[32,1664]{1,0:T(8,128)(2,1)S(1)} %collective-permute-done.refs_1_) | copy-start | bytes 319492
  18.0 0.6 copy-start.10
  18.1 0.7 copy-start.11
  21.4 103.1 %copy-start.3 = (bf16[256,2048]{1,0:T(8,128)(2,1)}, bf16[256,2048]{1,0:T(8,128)(2,1)S(1)}, u32[]{:S(2)}) copy-start(bf16[256,2048]{1,0:T(8,128)(2,1)S(1)} %fusion.2.refs_4_) | copy-start | bytes 3145732
  21.4 15.5 %collective-permute-start.6 = (bf16[256,2048]{1,0:T(8,128)(2,1)S(1)}, bf16[256,2048]{1,0:T(8,128)(2,1)S(1)}, u32[]{:S(2)}, u32[]{:S(2)}) collective-permute-start(bf16[256,2048]{1,0:T(8,128)(2,1)S(1)} %fusion.2.refs_4_), channel_id=1, source_target_pairs={{0,6},{2,0},{4,2},{6,4},{1,7},{3,1},{5,3},{7,5},{8,14},{10,8},{12,... | collective-permute-start | bytes 3145736 | tf_op jit(solution)/shard_map/ppermute | solution.py:24
  22.9 17.3 %collective-permute-start.4 = (bf16[256,2048]{1,0:T(8,128)(2,1)S(1)}, bf16[256,2048]{1,0:T(8,128)(2,1)}, u32[]{:S(2)}, u32[]{:S(2)}) collective-permute-start(bf16[256,2048]{1,0:T(8,128)(2,1)S(1)} %fusion.2.refs_4_), channel_id=1, source_target_pairs={{0,2},{2,4},{4,6},{6,0},{1,3},{3,5},{5,7},{7,1},{8,10},{10,12},{12... | collective-permute-start | bytes 3145736 | tf_op jit(solution)/shard_map/ppermute | solution.py:24
  36.9 87.6 %copy-start.7 = (bf16[256,2048]{1,0:T(8,128)(2,1)}, bf16[256,2048]{1,0:T(8,128)(2,1)S(1)}, u32[]{:S(2)}) copy-start(bf16[256,2048]{1,0:T(8,128)(2,1)S(1)} %collective-permute-done.6.refs_2_) | copy-start | bytes 3145732
  36.9 87.6 %collective-permute-start.7 = (bf16[128,2048]{1,0:T(8,128)(2,1)S(1)}, bf16[128,2048]{1,0:T(8,128)(2,1)}, u32[]{:S(2)}, u32[]{:S(2)}) collective-permute-start(bf16[128,2048]{1,0:T(8,128)(2,1)S(1)} %slice.19), channel_id=1, source_target_pairs={{0,6},{2,0},{4,2},{6,4},{1,7},{3,1},{5,3},{7,5},{8,14},{10,8},{12,... | collective-permute-start | bytes 1572872 | tf_op jit(solution)/shard_map/ppermute | solution.py:24
  41.3 83.3 %collective-permute-start.5 = (bf16[128,2048]{1,0:T(8,128)(2,1)S(1)}, bf16[128,2048]{1,0:T(8,128)(2,1)}, u32[]{:S(2)}, u32[]{:S(2)}) collective-permute-start(bf16[128,2048]{1,0:T(8,128)(2,1)S(1)} %slice.18), channel_id=1, source_target_pairs={{0,2},{2,4},{4,6},{6,0},{1,3},{3,5},{5,7},{7,1},{8,10},{10,12},{12... | collective-permute-start | bytes 1572872 | tf_op jit(solution)/shard_map/ppermute | solution.py:24
  42.2 23.4 %collective-permute-start.3 = (f32[4,256]{1,0:T(4,128)S(1)}, f32[4,256]{1,0:T(4,128)S(1)}, u32[]{:S(2)}, u32[]{:S(2)}) collective-permute-start(f32[4,256]{1,0:T(4,128)S(1)} %select_maximum_fusion), channel_id=1, source_target_pairs={{0,1},{1,0},{2,3},{3,2},{4,5},{5,4},{6,7},{7,6},{8,9},{9,8},{10,11... | collective-permute-start | bytes 12296 | tf_op jit(solution)/shard_map/ppermute | solution.py:296
  65.6 76.0 %copy-start.8 = (f32[2,4,256]{2,1,0:T(4,128)}, f32[2,4,256]{2,1,0:T(4,128)S(1)}, u32[]{:S(2)}) copy-start(f32[2,4,256]{2,1,0:T(4,128)S(1)} %maximum_select_fusion) | copy-start | bytes 24580
  141.6 11.2 %collective-permute-start.8 = (bf16[2,4,160,128]{3,2,1,0:T(8,128)(2,1)}, bf16[2,4,160,128]{3,2,1,0:T(8,128)(2,1)S(1)}, u32[]{:S(2)}, u32[]{:S(2)}) collective-permute-start(bf16[2,4,160,128]{3,2,1,0:T(8,128)(2,1)} %get-tuple-element.36), channel_id=1, source_target_pairs={{0,1},{1,8},{8,9},{9,16},{16,17},{17,24},{24,25},{25,32},{32,33},{... | collective-permute-start | bytes 983048 | tf_op jit(solution)/shard_map/ppermute | solution.py:332
  150.2 18.6 %collective-permute-start.15 = (bf16[128,2048]{1,0:T(8,128)(2,1)}, bf16[128,2048]{1,0:T(8,128)(2,1)S(1)}, u32[]{:S(2)}, u32[]{:S(2)}) collective-permute-start(bf16[128,2048]{1,0:T(8,128)(2,1)} %get-tuple-element.44), channel_id=1, source_target_pairs={{0,6},{2,0},{4,2},{6,4},{1,7},{3,1},{5,3},{7,5},{8,14},{10,8},{12,... | collective-permute-start | bytes 1572872 | tf_op jit(solution)/shard_map/ppermute | solution.py:24
  152.7 26.1 %collective-permute-start.10 = (bf16[128,2048]{1,0:T(8,128)(2,1)}, bf16[128,2048]{1,0:T(8,128)(2,1)S(1)}, u32[]{:S(2)}, u32[]{:S(2)}) collective-permute-start(bf16[128,2048]{1,0:T(8,128)(2,1)} %get-tuple-element.38), channel_id=1, source_target_pairs={{0,2},{2,4},{4,6},{6,0},{1,3},{3,5},{5,7},{7,1},{8,10},{10,12},{12... | collective-permute-start | bytes 1572872 | tf_op jit(solution)/shard_map/ppermute | solution.py:24
  152.7 0.7 copy-start.1
  159.5 13.5 %collective-permute-start.11 = (bf16[64,2048]{1,0:T(8,128)(2,1)}, bf16[64,2048]{1,0:T(8,128)(2,1)S(1)}, u32[]{:S(2)}, u32[]{:S(2)}) collective-permute-start(bf16[64,2048]{1,0:T(8,128)(2,1)} %get-tuple-element.40), channel_id=1, source_target_pairs={{0,2},{2,4},{4,6},{6,0},{1,3},{3,5},{5,7},{7,1},{8,10},{10,12},{12... | collective-permute-start | bytes 786440 | tf_op jit(solution)/shard_map/ppermute | solution.py:24
  159.8 18.7 %collective-permute-start.13 = (bf16[64,2048]{1,0:T(8,128)(2,1)}, bf16[64,2048]{1,0:T(8,128)(2,1)S(1)}, u32[]{:S(2)}, u32[]{:S(2)}) collective-permute-start(bf16[64,2048]{1,0:T(8,128)(2,1)} %get-tuple-element.42), channel_id=1, source_target_pairs={{0,2},{2,4},{4,6},{6,0},{1,3},{3,5},{5,7},{7,1},{8,10},{10,12},{12... | collective-permute-start | bytes 786440 | tf_op jit(solution)/shard_map/ppermute | solution.py:24
  161.0 17.8 %collective-permute-start.9 = (bf16[128,2048]{1,0:T(8,128)(2,1)}, bf16[128,2048]{1,0:T(8,128)(2,1)S(1)}, u32[]{:S(2)}, u32[]{:S(2)}) collective-permute-start(bf16[128,2048]{1,0:T(8,128)(2,1)} %get-tuple-element.37), channel_id=1, source_target_pairs={{0,6},{2,0},{4,2},{6,4},{1,7},{3,1},{5,3},{7,5},{8,14},{10,8},{12,... | collective-permute-start | bytes 1572872 | tf_op jit(solution)/shard_map/ppermute | solution.py:24
  168.8 9.7 %copy-start.6 = (bf16[64,2048]{1,0:T(8,128)(2,1)S(1)}, bf16[64,2048]{1,0:T(8,128)(2,1)}, u32[]{:S(2)}) copy-start(bf16[64,2048]{1,0:T(8,128)(2,1)} %get-tuple-element.41) | copy-start | bytes 786436
  170.1 19.5 %collective-permute-start.16 = (bf16[128,2048]{1,0:T(8,128)(2,1)S(1)}, bf16[128,2048]{1,0:T(8,128)(2,1)S(1)}, u32[]{:S(2)}, u32[]{:S(2)}) collective-permute-start(bf16[128,2048]{1,0:T(8,128)(2,1)S(1)} %add_convert_fusion.1), channel_id=1, source_target_pairs={{0,6},{2,0},{4,2},{6,4},{1,7},{3,1},{5,3},{7,5},{8,14},{10,8},{12,... | collective-permute-start | bytes 1572872 | tf_op jit(solution)/shard_map/ppermute | solution.py:24
  174.0 13.0 %collective-permute-start.12 = (bf16[64,2048]{1,0:T(8,128)(2,1)S(1)}, bf16[64,2048]{1,0:T(8,128)(2,1)S(1)}, u32[]{:S(2)}, u32[]{:S(2)}) collective-permute-start(bf16[64,2048]{1,0:T(8,128)(2,1)S(1)} %add_convert_fusion.3), channel_id=1, source_target_pairs={{0,2},{2,4},{4,6},{6,0},{1,3},{3,5},{5,7},{7,1},{8,10},{10,12},{12... | collective-permute-start | bytes 786440 | tf_op jit(solution)/shard_map/ppermute | solution.py:24
  178.7 10.9 %collective-permute-start.14 = (bf16[64,2048]{1,0:T(8,128)(2,1)S(1)}, bf16[64,2048]{1,0:T(8,128)(2,1)S(1)}, u32[]{:S(2)}, u32[]{:S(2)}) collective-permute-start(bf16[64,2048]{1,0:T(8,128)(2,1)S(1)} %add_convert_fusion.2), channel_id=1, source_target_pairs={{0,2},{2,4},{4,6},{6,0},{1,3},{3,5},{5,7},{7,1},{8,10},{10,12},{12... | collective-permute-start | bytes 786440 | tf_op jit(solution)/shard_map/ppermute | solution.py:24
  178.8 0.8 copy-start.4
  179.6 0.8 copy-start.5
Sparse Core Ops, SparseCore 0:
  20.9 103.5 all-gather.1

commit v6 on v5

--- a/solution.py
+++ b/solution.py
@@ -265,6 +265,9 @@
         out_specs=(VMEM,) * fs,
         name="pack_weights",
     )(member, w_query, w_key, w_value, conv_out_weight.T, attn_out_weight.T, w_bgate, w_cgate, w_conv_in)
+    exchanged = []
+    for d in range(1, fs):
+        exchanged.append(ring(packed[d], "fs", d))
     mine = pl.pallas_call(
         functools.partial(turn_kernel, in_cols),
         out_shape=jax.ShapeDtypeStruct((block, width), bf16),
@@ -272,7 +275,7 @@
         out_specs=VMEM,
         scratch_shapes=[pltpu.VMEM((block, out_cols), bf16)],
         name="turn_weights",
-    )(member, packed[0], *(ring(p, "fs", d) for d, p in enumerate(packed) if d > 0))
+    )(member, packed[0], *exchanged)
     weights = lax.all_gather(mine, ("sp", "tp"), axis=0, tiled=True)
     weights = weights.reshape(sp, tp, block, width)
 

time: 200 us -> 200 us (level)
  no operation moved by 1% of the time
where the time goes in v6:
time: 200 us; the launch traced here: 199 us
  waiting for transfers between devices  85.4 us (43%)
  Pallas kernels  45.7 us (23%)
  starting transfers between devices  43.4 us (22%)
  between operations  13.7 us (7%)
  other arithmetic  6.19 us (3%)
  local copies, waits for them, and re-layouts  4.71 us (2%)
    all_gather x1, waiting for transfers between devices, layer(): weights = lax.all_gather(mine, ('sp', 'tp'), axis=0, tiled=True)  58.4 us
    ppermute x15, waiting for transfers between devices, ring(): lax.ppermute(array, axis, [(i, (i + by) % size) for i in range(size)])  26.1 us
    pallas_call x4, Pallas kernels, mix(): pl.pallas_call(functools.partial(mix_kernel, blocks, pieces, b_width), ou...  24.7 us
    ppermute x1, starting transfers between devices, layer(): theirs = lax.ppermute(small, 'tp', [(0, 1), (1, 0)])  22.6 us
    ppermute x15, starting transfers between devices, ring(): lax.ppermute(array, axis, [(i, (i + by) % size) for i in range(size)])  18.1 us
    pallas_call x1, Pallas kernels, layer(): pl.pallas_call(functools.partial(project_kernel, b_width), out_shape=(jax...  17 us
  transfers between devices with their start and end apart: 18, of which 8 were waited for; matrix products, arithmetic and copies ran while one was open for 3% of the time, Pallas kernels for 12%

profile of v6, /device:TPU:33, one launch (start us, length us, event | category | flops | bytes accessed | tf_op | source)
XLA Modules:
  0.0 199.0 jit_solution(9192241536751008760)
XLA Ops:
  6.6 2.0 %pack_weights.1 = (bf16[32,1664]{1,0:T(8,128)(2,1)}, bf16[32,1664]{1,0:T(8,128)(2,1)}, bf16[32,1664]{1,0:T(8,128)(2,1)}, bf16[32,1664]{1,0:T(8,128)(2,1)}) custom-call(s32[1]{0:T(128)} %bitcast.group, bf16[32,1024]{1,0:T(8,128)(2,1)} %wq.1, bf16[32,128]{1,0:T(8,128)(2,1)} %wk.1, bf16[32,128]{1,0:T(8,128)(2,1)} %wv.1, bf16[32,1024]{1,0:T(8,128)(2,1)} %bitcast.22, ...), custom_call_target="tpu_custom_call" | custom-call | tf_op jit(solution)/shard_map/pack_weights/pallas_call | solution.py:261
  8.6 2.2 %collective-permute-start = (bf16[32,1664]{1,0:T(8,128)(2,1)}, bf16[32,1664]{1,0:T(8,128)(2,1)S(1)}, u32[]{:S(2)}, u32[]{:S(2)}) collective-permute-start(bf16[32,1664]{1,0:T(8,128)(2,1)} %get-tuple-element.26), channel_id=1, source_target_pairs={{0,2},{2,4},{4,6},{6,0},{1,3},{3,5},{5,7},{7,1},{8,10},{10,12},{12... | collective-permute-start | bytes 319496 | tf_op jit(solution)/shard_map/ppermute | solution.py:24
  10.7 2.7 %collective-permute-start.1 = (bf16[32,1664]{1,0:T(8,128)(2,1)}, bf16[32,1664]{1,0:T(8,128)(2,1)S(1)}, u32[]{:S(2)}, u32[]{:S(2)}) collective-permute-start(bf16[32,1664]{1,0:T(8,128)(2,1)} %get-tuple-element.27), channel_id=1, source_target_pairs={{0,4},{2,6},{4,0},{6,2},{1,5},{3,7},{5,1},{7,3},{8,12},{10,14},{12... | collective-permute-start | bytes 319496 | tf_op jit(solution)/shard_map/ppermute | solution.py:24
  13.5 1.0 collective-permute-start.2
  14.5 0.1 collective-permute-done.refs_1_
  14.6 3.5 %collective-permute-done.1.refs_2_ = bf16[32,1664]{1,0:T(8,128)(2,1)S(1)} collective-permute-done((bf16[32,1664]{1,0:T(8,128)(2,1)}, bf16[32,1664]{1,0:T(8,128)(2,1)S(1)}, u32[]{:S(2)}, u32[]{:S(2)}) %collective-permute-start.1) | collective-permute-done | bytes 106528 | tf_op jit(solution)/shard_map/ppermute | solution.py:24
  18.1 0.6 copy-done.10
  18.7 0.0 copy-done.11
  18.7 1.9 turn_weights.1
  20.7 0.1 all-gather.2.cloned.1.call-update
  20.7 0.3 fusion
  21.1 0.3 fusion.2.refs_4_
  21.4 1.5 collective-permute-start.6
  22.9 0.1 collective-permute-start.4
  23.0 13.9 %collective-permute-done.6.refs_2_ = bf16[256,2048]{1,0:T(8,128)(2,1)S(1)} collective-permute-done((bf16[256,2048]{1,0:T(8,128)(2,1)S(1)}, bf16[256,2048]{1,0:T(8,128)(2,1)S(1)}, u32[]{:S(2)}, u32[]{:S(2)}) %collective-permute-start.6) | collective-permute-done | bytes 1048608 | tf_op jit(solution)/shard_map/ppermute | solution.py:24
  36.9 3.2 %collective-permute-start.7 = (bf16[128,2048]{1,0:T(8,128)(2,1)S(1)}, bf16[128,2048]{1,0:T(8,128)(2,1)}, u32[]{:S(2)}, u32[]{:S(2)}) collective-permute-start(bf16[128,2048]{1,0:T(8,128)(2,1)S(1)} %slice.19), channel_id=1, source_target_pairs={{0,6},{2,0},{4,2},{6,4},{1,7},{3,1},{5,3},{7,5},{8,14},{10,8},{12,... | collective-permute-start | bytes 1572872 | tf_op jit(solution)/shard_map/ppermute | solution.py:24
  40.2 1.1 slice.18
  41.3 0.1 collective-permute-start.5
  41.4 0.1 dynamic-slice_bitcast_fusion
  41.5 0.7 dynamic-slice_convert_fusion
  42.2 22.6 %collective-permute-start.3 = (f32[4,256]{1,0:T(4,128)S(1)}, f32[4,256]{1,0:T(4,128)S(1)}, u32[]{:S(2)}, u32[]{:S(2)}) collective-permute-start(f32[4,256]{1,0:T(4,128)S(1)} %select_maximum_fusion), channel_id=1, source_target_pairs={{0,1},{1,0},{2,3},{3,2},{4,5},{5,4},{6,7},{7,6},{8,9},{9,8},{10,11... | collective-permute-start | bytes 12296 | tf_op jit(solution)/shard_map/ppermute | solution.py:299
  64.8 0.8 collective-permute-done.3
  65.6 0.5 slice.17
  66.1 58.4 %all-gather.2.cloned.1.call-done = bf16[4096,1664]{1,0:T(8,128)(2,1)} async-done(((bf16[128,1664]{1,0:T(8,128)(2,1)}), bf16[4096,1664]{1,0:T(8,128)(2,1)}) %all-gather.2.cloned.1.call-update) | async-done | bytes 13631504 | tf_op jit(solution)/shard_map/all_gather | solution.py:279
  124.5 0.0 collective-permute-done.5.refs_0_
  124.5 17.0 %project_rows.1 = (bf16[2,4,256,1024]{3,2,1,0:T(8,128)(2,1)}, bf16[4,256,256]{2,1,0:T(8,128)(2,1)}, bf16[2,4,160,128]{3,2,1,0:T(8,128)(2,1)}, bf16[1024,2048]{1,0:T(8,128)(2,1)}) custom-call(bf16[16,2,128,1664]{3,2,1,0:T(8,128)(2,1)} %bitcast.29, bf16[128,2048]{1,0:T(8,128)(2,1)} %collective-permute-done.5.refs_0_, ...), custom_call_target="tpu_custom_call" | custom-call | flops 9663676416 | bytes 25000000 | tf_op jit(solution)/shard_map/project_rows/pallas_call | solution.py:306
  141.6 2.6 %collective-permute-start.8 = (bf16[2,4,160,128]{3,2,1,0:T(8,128)(2,1)}, bf16[2,4,160,128]{3,2,1,0:T(8,128)(2,1)S(1)}, u32[]{:S(2)}, u32[]{:S(2)}) collective-permute-start(bf16[2,4,160,128]{3,2,1,0:T(8,128)(2,1)} %get-tuple-element.36), channel_id=1, source_target_pairs={{0,1},{1,8},{8,9},{9,16},{16,17},{17,24},{24,25},{25,32},{32,33},{... | collective-permute-start | bytes 983048 | tf_op jit(solution)/shard_map/ppermute | solution.py:335
  144.2 6.0 %shard_map.119 = (bf16[128,2048]{1,0:T(8,128)(2,1)}, bf16[128,2048]{1,0:T(8,128)(2,1)}) custom-call(s32[1]{0:T(128)} %bitcast.4.idx, f32[2,4]{1,0:T(2,128)} %bitcast.24, f32[2,3,256]{2,1,0:T(4,128)} %bitcast.18, bf16[1024,2048]{1,0:T(8,128)(2,1)} %get-tuple-element.33.wout, bf16[2,4,256,1024]{3,2,1,0:T(8,128)(2,1)} %get-tuple-element.34.refs_0_.refs_1_, ...), custom_call_target="tpu_custom_call" | custom-call | flops 1673741824 | bytes 8000000 | tf_op jit(solution)/shard_map/pallas_call | solution.py:344
  150.2 2.5 %collective-permute-start.15 = (bf16[128,2048]{1,0:T(8,128)(2,1)}, bf16[128,2048]{1,0:T(8,128)(2,1)S(1)}, u32[]{:S(2)}, u32[]{:S(2)}) collective-permute-start(bf16[128,2048]{1,0:T(8,128)(2,1)} %get-tuple-element.44), channel_id=1, source_target_pairs={{0,6},{2,0},{4,2},{6,4},{1,7},{3,1},{5,3},{7,5},{8,14},{10,8},{12,... | collective-permute-start | bytes 1572872 | tf_op jit(solution)/shard_map/ppermute | solution.py:24
  152.8 0.7 copy-done.1
  153.5 6.0 %shard_map.118 = (bf16[64,2048]{1,0:T(8,128)(2,1)}, bf16[64,2048]{1,0:T(8,128)(2,1)}, bf16[128,2048]{1,0:T(8,128)(2,1)}) custom-call(s32[1]{0:T(128)} %bitcast.4.idx, f32[2,4]{1,0:T(2,128)} %bitcast.25, f32[2,3,256]{2,1,0:T(4,128)} %bitcast.19, bf16[1024,2048]{1,0:T(8,128)(2,1)} %get-tuple-element.33.wout, ...), custom_call_target="tpu_custom_call" | custom-call | flops 1673741824 | bytes 8000000 | tf_op jit(solution)/shard_map/pallas_call | solution.py:344
  159.5 0.3 collective-permute-start.11
  159.8 1.2 collective-permute-start.13
  161.0 1.7 collective-permute-start.9
  162.8 6.0 %shard_map.121 = (bf16[64,2048]{1,0:T(8,128)(2,1)}, bf16[64,2048]{1,0:T(8,128)(2,1)}, bf16[128,2048]{1,0:T(8,128)(2,1)}) custom-call(s32[1]{0:T(128)} %bitcast.4.idx, f32[2,4]{1,0:T(2,128)} %bitcast.26, f32[2,3,256]{2,1,0:T(4,128)} %bitcast.20, bf16[1024,2048]{1,0:T(8,128)(2,1)} %get-tuple-element.33.wout, ...), custom_call_target="tpu_custom_call" | custom-call | flops 1673741824 | bytes 8000000 | tf_op jit(solution)/shard_map/pallas_call | solution.py:344
  168.8 1.2 add_convert_fusion.1
  170.1 1.2 collective-permute-start.16
  171.3 1.7 collective-permute-done.11
  173.0 1.0 add_convert_fusion.3
  174.0 0.1 collective-permute-start.12
  174.1 4.5 %collective-permute-done.13 = bf16[64,2048]{1,0:T(8,128)(2,1)S(1)} collective-permute-done((bf16[64,2048]{1,0:T(8,128)(2,1)}, bf16[64,2048]{1,0:T(8,128)(2,1)S(1)}, u32[]{:S(2)}, u32[]{:S(2)}) %collective-permute-start.13) | collective-permute-done | bytes 262176 | tf_op jit(solution)/shard_map/ppermute | solution.py:24
  178.6 0.1 add_convert_fusion.2
  178.7 0.1 collective-permute-start.14
  178.8 0.8 copy-done.4
  179.6 0.8 copy-done.5
  180.4 6.6 %shard_map.120 = bf16[256,2048]{1,0:T(8,128)(2,1)} custom-call(s32[1]{0:T(128)} %bitcast.4.idx, f32[2,4]{1,0:T(2,128)} %bitcast.27, f32[2,3,256]{2,1,0:T(4,128)} %bitcast.21, bf16[1024,2048]{1,0:T(8,128)(2,1)} %get-tuple-element.33.wout, bf16[2,4,256,1024]{3,2,1,0:T(8,128)(2,1)} %get-tuple-element.34.refs_0_.refs_1_, ...), custom_call_target="tpu_custom_call" | custom-call | flops 1673741824 | bytes 8000000 | tf_op jit(solution)/shard_map/pallas_call | solution.py:344
  187.0 2.5 %collective-permute-done.14 = bf16[64,2048]{1,0:T(8,128)(2,1)S(1)} collective-permute-done((bf16[64,2048]{1,0:T(8,128)(2,1)S(1)}, bf16[64,2048]{1,0:T(8,128)(2,1)S(1)}, u32[]{:S(2)}, u32[]{:S(2)}) %collective-permute-start.14) | collective-permute-done | bytes 262176 | tf_op jit(solution)/shard_map/ppermute | solution.py:24
  189.5 2.6 %fusion.3 = bf16[1,256,2048]{2,1,0:T(8,128)(2,1)} fusion(bf16[256,2048]{1,0:T(8,128)(2,1)} %shard_map.120, bf16[128,2048]{1,0:T(8,128)(2,1)S(1)} %collective-permute-done.16, bf16[64,2048]{1,0:T(8,128)(2,1)S(1)} %collective-permute-done.14, bf16[64,2048]{1,0:T(8,128)(2,1)S(1)} %collective-permute-done.12), kind=kLoop, calls=%fused_computation.6 | loop fusion | flops 4718592 | bytes 3145728 | tf_op jit(solution)/shard_map/broadcast_in_dim | solution.py:380
  (37 shorter events, 0.1 us)
Async XLA Ops:
  6.5 34.8 %copy-start = (f32[16]{0:T(128)S(1)}, f32[16]{0:T(128)}, u32[]{:S(2)}) copy-start(f32[16]{0:T(128)} %param.21) | copy-start | bytes 196
  6.6 14.2 %copy-start.2 = (bf16[1,256,2048]{2,1,0:T(8,128)(2,1)S(1)}, bf16[1,256,2048]{2,1,0:T(8,128)(2,1)}, u32[]{:S(2)}) copy-start(bf16[1,256,2048]{2,1,0:T(8,128)(2,1)} %param.12) | copy-start | bytes 3145732
  6.6 14.5 %copy-start.12 = (f32[2048]{0:T(1024)S(1)}, f32[2048]{0:T(1024)}, u32[]{:S(2)}) copy-start(f32[2048]{0:T(1024)} %param.13) | copy-start | bytes 24580
  6.6 117.9 %all-gather.2.cloned.1.call-start = ((), (), s32[]{:S(2)}) async-start(), calls=%async_computation | async-start | bytes 14057472 | tf_op jit(solution)/shard_map/all_gather | solution.py:279
  8.6 6.0 %collective-permute-start = (bf16[32,1664]{1,0:T(8,128)(2,1)}, bf16[32,1664]{1,0:T(8,128)(2,1)S(1)}, u32[]{:S(2)}, u32[]{:S(2)}) collective-permute-start(bf16[32,1664]{1,0:T(8,128)(2,1)} %get-tuple-element.26), channel_id=1, source_target_pairs={{0,2},{2,4},{4,6},{6,0},{1,3},{3,5},{5,7},{7,1},{8,10},{10,12},{12... | collective-permute-start | bytes 319496 | tf_op jit(solution)/shard_map/ppermute | solution.py:24
  10.7 7.3 %collective-permute-start.1 = (bf16[32,1664]{1,0:T(8,128)(2,1)}, bf16[32,1664]{1,0:T(8,128)(2,1)S(1)}, u32[]{:S(2)}, u32[]{:S(2)}) collective-permute-start(bf16[32,1664]{1,0:T(8,128)(2,1)} %get-tuple-element.27), channel_id=1, source_target_pairs={{0,4},{2,6},{4,0},{6,2},{1,5},{3,7},{5,1},{7,3},{8,12},{10,14},{12... | collective-permute-start | bytes 319496 | tf_op jit(solution)/shard_map/ppermute | solution.py:24
  13.5 4.6 %collective-permute-start.2 = (bf16[32,1664]{1,0:T(8,128)(2,1)}, bf16[32,1664]{1,0:T(8,128)(2,1)S(1)}, u32[]{:S(2)}, u32[]{:S(2)}) collective-permute-start(bf16[32,1664]{1,0:T(8,128)(2,1)} %get-tuple-element.28), channel_id=1, source_target_pairs={{0,6},{2,0},{4,2},{6,4},{1,7},{3,1},{5,3},{7,5},{8,14},{10,8},{12,... | collective-permute-start | bytes 319496 | tf_op jit(solution)/shard_map/ppermute | solution.py:24
  14.6 3.5 %copy-start.9 = (bf16[32,1664]{1,0:T(8,128)(2,1)}, bf16[32,1664]{1,0:T(8,128)(2,1)S(1)}, u32[]{:S(2)}) copy-start(bf16[32,1664]{1,0:T(8,128)(2,1)S(1)} %collective-permute-done.refs_1_) | copy-start | bytes 319492
  18.0 0.6 copy-start.10
  18.1 0.7 copy-start.11
  21.4 103.1 %copy-start.3 = (bf16[256,2048]{1,0:T(8,128)(2,1)}, bf16[256,2048]{1,0:T(8,128)(2,1)S(1)}, u32[]{:S(2)}) copy-start(bf16[256,2048]{1,0:T(8,128)(2,1)S(1)} %fusion.2.refs_4_) | copy-start | bytes 3145732
  21.4 15.5 %collective-permute-start.6 = (bf16[256,2048]{1,0:T(8,128)(2,1)S(1)}, bf16[256,2048]{1,0:T(8,128)(2,1)S(1)}, u32[]{:S(2)}, u32[]{:S(2)}) collective-permute-start(bf16[256,2048]{1,0:T(8,128)(2,1)S(1)} %fusion.2.refs_4_), channel_id=1, source_target_pairs={{0,6},{2,0},{4,2},{6,4},{1,7},{3,1},{5,3},{7,5},{8,14},{10,8},{12,... | collective-permute-start | bytes 3145736 | tf_op jit(solution)/shard_map/ppermute | solution.py:24
  22.9 17.3 %collective-permute-start.4 = (bf16[256,2048]{1,0:T(8,128)(2,1)S(1)}, bf16[256,2048]{1,0:T(8,128)(2,1)}, u32[]{:S(2)}, u32[]{:S(2)}) collective-permute-start(bf16[256,2048]{1,0:T(8,128)(2,1)S(1)} %fusion.2.refs_4_), channel_id=1, source_target_pairs={{0,2},{2,4},{4,6},{6,0},{1,3},{3,5},{5,7},{7,1},{8,10},{10,12},{12... | collective-permute-start | bytes 3145736 | tf_op jit(solution)/shard_map/ppermute | solution.py:24
  36.9 87.6 %copy-start.7 = (bf16[256,2048]{1,0:T(8,128)(2,1)}, bf16[256,2048]{1,0:T(8,128)(2,1)S(1)}, u32[]{:S(2)}) copy-start(bf16[256,2048]{1,0:T(8,128)(2,1)S(1)} %collective-permute-done.6.refs_2_) | copy-start | bytes 3145732
  36.9 87.6 %collective-permute-start.7 = (bf16[128,2048]{1,0:T(8,128)(2,1)S(1)}, bf16[128,2048]{1,0:T(8,128)(2,1)}, u32[]{:S(2)}, u32[]{:S(2)}) collective-permute-start(bf16[128,2048]{1,0:T(8,128)(2,1)S(1)} %slice.19), channel_id=1, source_target_pairs={{0,6},{2,0},{4,2},{6,4},{1,7},{3,1},{5,3},{7,5},{8,14},{10,8},{12,... | collective-permute-start | bytes 1572872 | tf_op jit(solution)/shard_map/ppermute | solution.py:24
  41.3 83.3 %collective-permute-start.5 = (bf16[128,2048]{1,0:T(8,128)(2,1)S(1)}, bf16[128,2048]{1,0:T(8,128)(2,1)}, u32[]{:S(2)}, u32[]{:S(2)}) collective-permute-start(bf16[128,2048]{1,0:T(8,128)(2,1)S(1)} %slice.18), channel_id=1, source_target_pairs={{0,2},{2,4},{4,6},{6,0},{1,3},{3,5},{5,7},{7,1},{8,10},{10,12},{12... | collective-permute-start | bytes 1572872 | tf_op jit(solution)/shard_map/ppermute | solution.py:24
  42.2 23.4 %collective-permute-start.3 = (f32[4,256]{1,0:T(4,128)S(1)}, f32[4,256]{1,0:T(4,128)S(1)}, u32[]{:S(2)}, u32[]{:S(2)}) collective-permute-start(f32[4,256]{1,0:T(4,128)S(1)} %select_maximum_fusion), channel_id=1, source_target_pairs={{0,1},{1,0},{2,3},{3,2},{4,5},{5,4},{6,7},{7,6},{8,9},{9,8},{10,11... | collective-permute-start | bytes 12296 | tf_op jit(solution)/shard_map/ppermute | solution.py:299
  65.6 76.0 %copy-start.8 = (f32[2,4,256]{2,1,0:T(4,128)}, f32[2,4,256]{2,1,0:T(4,128)S(1)}, u32[]{:S(2)}) copy-start(f32[2,4,256]{2,1,0:T(4,128)S(1)} %maximum_select_fusion) | copy-start | bytes 24580
  141.6 11.2 %collective-permute-start.8 = (bf16[2,4,160,128]{3,2,1,0:T(8,128)(2,1)}, bf16[2,4,160,128]{3,2,1,0:T(8,128)(2,1)S(1)}, u32[]{:S(2)}, u32[]{:S(2)}) collective-permute-start(bf16[2,4,160,128]{3,2,1,0:T(8,128)(2,1)} %get-tuple-element.36), channel_id=1, source_target_pairs={{0,1},{1,8},{8,9},{9,16},{16,17},{17,24},{24,25},{25,32},{32,33},{... | collective-permute-start | bytes 983048 | tf_op jit(solution)/shard_map/ppermute | solution.py:335
  150.2 18.6 %collective-permute-start.15 = (bf16[128,2048]{1,0:T(8,128)(2,1)}, bf16[128,2048]{1,0:T(8,128)(2,1)S(1)}, u32[]{:S(2)}, u32[]{:S(2)}) collective-permute-start(bf16[128,2048]{1,0:T(8,128)(2,1)} %get-tuple-element.44), channel_id=1, source_target_pairs={{0,6},{2,0},{4,2},{6,4},{1,7},{3,1},{5,3},{7,5},{8,14},{10,8},{12,... | collective-permute-start | bytes 1572872 | tf_op jit(solution)/shard_map/ppermute | solution.py:24
  152.7 26.1 %collective-permute-start.10 = (bf16[128,2048]{1,0:T(8,128)(2,1)}, bf16[128,2048]{1,0:T(8,128)(2,1)S(1)}, u32[]{:S(2)}, u32[]{:S(2)}) collective-permute-start(bf16[128,2048]{1,0:T(8,128)(2,1)} %get-tuple-element.38), channel_id=1, source_target_pairs={{0,2},{2,4},{4,6},{6,0},{1,3},{3,5},{5,7},{7,1},{8,10},{10,12},{12... | collective-permute-start | bytes 1572872 | tf_op jit(solution)/shard_map/ppermute | solution.py:24
  152.7 0.7 copy-start.1
  159.5 13.5 %collective-permute-start.11 = (bf16[64,2048]{1,0:T(8,128)(2,1)}, bf16[64,2048]{1,0:T(8,128)(2,1)S(1)}, u32[]{:S(2)}, u32[]{:S(2)}) collective-permute-start(bf16[64,2048]{1,0:T(8,128)(2,1)} %get-tuple-element.40), channel_id=1, source_target_pairs={{0,2},{2,4},{4,6},{6,0},{1,3},{3,5},{5,7},{7,1},{8,10},{10,12},{12... | collective-permute-start | bytes 786440 | tf_op jit(solution)/shard_map/ppermute | solution.py:24
  159.8 18.7 %collective-permute-start.13 = (bf16[64,2048]{1,0:T(8,128)(2,1)}, bf16[64,2048]{1,0:T(8,128)(2,1)S(1)}, u32[]{:S(2)}, u32[]{:S(2)}) collective-permute-start(bf16[64,2048]{1,0:T(8,128)(2,1)} %get-tuple-element.42), channel_id=1, source_target_pairs={{0,2},{2,4},{4,6},{6,0},{1,3},{3,5},{5,7},{7,1},{8,10},{10,12},{12... | collective-permute-start | bytes 786440 | tf_op jit(solution)/shard_map/ppermute | solution.py:24
  161.0 17.8 %collective-permute-start.9 = (bf16[128,2048]{1,0:T(8,128)(2,1)}, bf16[128,2048]{1,0:T(8,128)(2,1)S(1)}, u32[]{:S(2)}, u32[]{:S(2)}) collective-permute-start(bf16[128,2048]{1,0:T(8,128)(2,1)} %get-tuple-element.37), channel_id=1, source_target_pairs={{0,6},{2,0},{4,2},{6,4},{1,7},{3,1},{5,3},{7,5},{8,14},{10,8},{12,... | collective-permute-start | bytes 1572872 | tf_op jit(solution)/shard_map/ppermute | solution.py:24
  168.8 9.7 %copy-start.6 = (bf16[64,2048]{1,0:T(8,128)(2,1)S(1)}, bf16[64,2048]{1,0:T(8,128)(2,1)}, u32[]{:S(2)}) copy-start(bf16[64,2048]{1,0:T(8,128)(2,1)} %get-tuple-element.41) | copy-start | bytes 786436
  170.1 19.5 %collective-permute-start.16 = (bf16[128,2048]{1,0:T(8,128)(2,1)S(1)}, bf16[128,2048]{1,0:T(8,128)(2,1)S(1)}, u32[]{:S(2)}, u32[]{:S(2)}) collective-permute-start(bf16[128,2048]{1,0:T(8,128)(2,1)S(1)} %add_convert_fusion.1), channel_id=1, source_target_pairs={{0,6},{2,0},{4,2},{6,4},{1,7},{3,1},{5,3},{7,5},{8,14},{10,8},{12,... | collective-permute-start | bytes 1572872 | tf_op jit(solution)/shard_map/ppermute | solution.py:24
  174.0 13.0 %collective-permute-start.12 = (bf16[64,2048]{1,0:T(8,128)(2,1)S(1)}, bf16[64,2048]{1,0:T(8,128)(2,1)S(1)}, u32[]{:S(2)}, u32[]{:S(2)}) collective-permute-start(bf16[64,2048]{1,0:T(8,128)(2,1)S(1)} %add_convert_fusion.3), channel_id=1, source_target_pairs={{0,2},{2,4},{4,6},{6,0},{1,3},{3,5},{5,7},{7,1},{8,10},{10,12},{12... | collective-permute-start | bytes 786440 | tf_op jit(solution)/shard_map/ppermute | solution.py:24
  178.7 10.9 %collective-permute-start.14 = (bf16[64,2048]{1,0:T(8,128)(2,1)S(1)}, bf16[64,2048]{1,0:T(8,128)(2,1)S(1)}, u32[]{:S(2)}, u32[]{:S(2)}) collective-permute-start(bf16[64,2048]{1,0:T(8,128)(2,1)S(1)} %add_convert_fusion.2), channel_id=1, source_target_pairs={{0,2},{2,4},{4,6},{6,0},{1,3},{3,5},{5,7},{7,1},{8,10},{10,12},{12... | collective-permute-start | bytes 786440 | tf_op jit(solution)/shard_map/ppermute | solution.py:24
  178.8 0.8 copy-start.4
  179.6 0.8 copy-start.5
Sparse Core Ops, SparseCore 0:
  20.9 103.5 all-gather.1
